TPU v7x, 256 devices: a whole 4x4x8 slice. The times are simulated.
256 devices in a mesh: ep: 32 (over z, x), tp: 8 (over y, core).
Axes of the slice: x: 4, y: 4, z: 8, core: 2. Of those that a mesh axis runs over, the one named last changes fastest.
Arguments:
- tokens: bfloat16 [2048, 2048], P('ep'), may hold values from -6 to 6
- norm_gain: float32 [2048], replicated, may hold values from 0.1 to 1.9
- norm_shift: float32 [2048], replicated, may hold values from -3 to 3
- expert_ids: int32 [2048, 4], P('ep'), may hold values from 0 to 63, as said below
- gate_weights: float32 [2048, 4], P('ep'), may hold values from 0.1 to 1
- expert_gate: bfloat16 [64, 2048, 512], P('ep', None, 'tp'), may hold values from -0.125 to 0.125
- expert_up: bfloat16 [64, 2048, 512], P('ep', None, 'tp'), may hold values from -0.125 to 0.125
- expert_down: bfloat16 [64, 512, 2048], P('ep', 'tp'), may hold values from -0.25 to 0.25
Outputs:
- mixed_out: bfloat16 [2048, 2048], P('ep', 'tp')
Inputs may be any that keep to these rules, and one draw needn't show every extreme that they name: `expert_ids`: each row names 4 distinct experts that all lie in one group of 16 consecutive expert numbers. In the rows of one index of ep (aligned blocks of 64 rows) no expert is named by more than 8 rows, and in every block some expert is named by exactly 8 rows.
All inputs are finite; a program needn't handle non-finite values.
Results may differ from a plain program's by a relative error of at most 0.002.
Values may be sent and summed in bfloat16 or wider, within the bound.
No kernel may reach another device: no remote copies, remote signals or barrier semaphores. Data moves between devices by JAX's collectives and lax.ppermute only.
A program may use at most 64 MiB of HBM per device.

v0:
```python
import functools

import jax
import jax.numpy as jnp
from jax import lax
from jax.experimental import pallas as pl
from jax.experimental.pallas import tpu as pltpu
from jax.sharding import PartitionSpec as P


GROUPS = 4
CORES = 2
EPSILON = 1e-05

VMEM = pl.BlockSpec(memory_space=pltpu.VMEM)
PARAMS = pltpu.CompilerParams(vmem_limit_bytes=20 * 1024 * 1024)


def on_chip(*arrays):
    return [pltpu.with_memory_space_constraint(a, pltpu.VMEM) for a in arrays]


def off_chip(*arrays):
    return [pltpu.with_memory_space_constraint(a, pltpu.HBM) for a in arrays]


def position():
    index = lax.axis_index("tp")
    return lax.shift_right_logical(index, 1), lax.bitwise_and(index, 1)


def dot_nn(a, b):
    return lax.dot_general(a, b, (((1,), (0,)), ((), ())), preferred_element_type=jnp.float32)


def dot_nt(a, b):
    return lax.dot_general(a, b, (((1,), (1,)), ((), ())), preferred_element_type=jnp.float32)


def dot_tn(a, b):
    return lax.dot_general(a, b, (((0,), (0,)), ((), ())), preferred_element_type=jnp.float32)


def part(y):
    high = lax.shift_right_logical(y, 1)
    return high, lax.bitwise_and(lax.bitwise_xor(y, high), 1)


def iota(shape, dimension):
    return lax.broadcasted_iota(jnp.int32, shape, dimension)


def copy_all(pairs, sems):
    copies = [pltpu.make_async_copy(src, dst, sems.at[i]) for i, (src, dst) in enumerate(pairs)]
    for copy in copies:
        copy.start()
    return copies


def weights_kernel(gate, up, mine, giving, sems):
    _, core = position()
    pairs = [(ref.at[core], mine.at[i]) for i, ref in enumerate((gate, up))]
    pairs += [(ref.at[1 - core], giving.at[i]) for i, ref in enumerate((gate, up))]
    for copy in copy_all(pairs, sems):
        copy.wait()


def pack_kernel(tokens, gain, shift, ids, weights, packed, select_hi, select_lo, *, slots):
    y, core = position()
    row_half, feature_half = part(y)
    top_count, rows = ids.shape
    total = packed.shape[0]
    experts = total // slots
    width = packed.shape[1]
    share = 2 * width
    values = tokens[...].astype(jnp.float32)
    centre = jnp.mean(values, axis=-1, keepdims=True)
    spread = jnp.mean(jnp.square(values - centre), axis=-1, keepdims=True)
    columns = pl.ds(pl.multiple_of(feature_half * share, share), share)
    own = tokens[:, columns].astype(jnp.float32)
    scaled = (own - centre) * lax.rsqrt(spread + EPSILON) * gain[:, columns] + shift[:, columns]
    normed = scaled.astype(jnp.bfloat16)
    expert = CORES * iota((experts, rows), 0) + core
    named = jnp.zeros((experts, rows), jnp.float32)
    weight = jnp.zeros((experts, rows), jnp.float32)
    for k in range(top_count):
        hit = ids[k : k + 1, :] == expert
        named = jnp.where(hit, 1.0, named)
        weight = jnp.where(hit, weights[k : k + 1, :], weight)
    earlier = jnp.where(iota((rows, rows), 0) < iota((rows, rows), 1), 1.0, 0.0)
    rank = dot_nn(named.astype(jnp.bfloat16), earlier.astype(jnp.bfloat16))
    slot = jnp.where(named > 0.0, rank, -1.0)
    cube = (experts, slots, rows)
    slot = jnp.broadcast_to(slot[:, None, :], cube)
    place = iota(cube, 1)
    sent = row_half * (slots // 2) + lax.rem(place, slots // 2)
    one_hot = jnp.where(slot == sent.astype(jnp.float32), 1.0, 0.0)
    one_hot = one_hot.reshape(total, rows).astype(jnp.bfloat16)
    first = dot_nn(one_hot, normed[:, :width])
    second = dot_nn(one_hot, normed[:, width:])
    front = lax.rem(iota((total, width), 0), slots) < slots // 2
    packed[...] = jnp.where(front, first, second).astype(jnp.bfloat16)
    factor = jnp.where(
        slot == place.astype(jnp.float32), jnp.broadcast_to(weight[:, None, :], cube), 0.0
    ).reshape(total, rows)
    high = factor.astype(jnp.bfloat16)
    select_hi[...] = high
    select_lo[...] = (factor - high.astype(jnp.float32)).astype(jnp.bfloat16)


def pieces_kernel(down, own, first, second, third, sems):
    y, _ = position()
    share = own.shape[-1]
    pairs = []
    for chip, piece in zip((y, *others(y)), (own, first, second, third)):
        columns = pl.ds(pl.multiple_of(chip * share, share), share)
        pairs.append((down.at[:, :, columns], piece))
    for copy in copy_all(pairs, sems):
        copy.wait()


def others(y):
    return lax.bitwise_xor(y, 1), 3 - y, lax.bitwise_xor(y, 2)


def hidden_kernel(own, near, mine, swapped, same, cross, hidden, *, slots):
    y, _ = position()
    _, half = part(y)
    rows, width = own.shape
    kept = rows // 2
    count = slots // 2
    i, j = iota((kept, rows), 0), iota((kept, rows), 1)
    source = (i // count) * slots + i % count
    total = None
    for tokens, at in ((own, half), (near, 1 - half)):
        values = tokens[...]
        for q in range(2):
            pick = jnp.where(j == source + q * count, 1.0, 0.0).astype(jnp.bfloat16)
            x = dot_nn(pick, values).astype(jnp.bfloat16)
            columns = pl.ds(pl.multiple_of((2 * at + q) * width, width), width)
            w = jnp.concatenate(
                [ref[m, :, columns] for m in range(2) for ref in (mine, swapped, same, cross)]
            )
            product = dot_nt(x, w)
            total = product if total is None else total + product
    units = total.shape[1] // 2
    value = total[:, :units]
    result = value / (1.0 + jnp.exp(-value)) * total[:, units:]
    hidden[...] = result.astype(jnp.bfloat16)


def give_kernel(own, first, second, third, giving):
    _, core = position()
    for i, ref in enumerate((own, first, second, third)):
        giving[i] = ref[1 - core]


def down_kernel(h_own, h_first, h_second, h_third, own, first, second, third, other, out, *, slots):
    y, core = position()
    row_half, _ = part(y)
    rows = out.shape[0]
    kept = h_own.shape[0]
    count = slots // 2
    units = h_own.shape[1] // 2
    r, j = iota((rows, 2 * kept), 0), iota((rows, 2 * kept), 1)
    i = lax.rem(j, kept)
    half = jnp.where(j < kept, row_half, 1 - row_half)
    place = (i // count) * slots + half * count + i % count
    spread = jnp.where(r == place, 1.0, 0.0).astype(jnp.bfloat16)
    total = None
    for a, b, w0, o0, w1, o1 in (
        (h_own, h_second, own, 0, second, 2),
        (h_first, h_third, first, 1, third, 3),
    ):
        across = jnp.concatenate([b[:, units:], b[:, :units]], axis=1)
        h = dot_nn(spread, jnp.concatenate([a[...], across])).astype(jnp.bfloat16)
        w = jnp.concatenate([w0[core], other[o0], w1[core], other[o1]])
        product = dot_nn(h, w)
        total = product if total is None else total + product
    out[...] = total


def combine_kernel(select_hi, select_lo, returned, kept, sent):
    _, core = position()
    values = returned[...]
    high = values.astype(jnp.bfloat16)
    low = (values - high.astype(jnp.float32)).astype(jnp.bfloat16)
    total = dot_tn(select_hi[...], high) + dot_tn(select_lo[...], high)
    total = total + dot_tn(select_hi[...], low)
    half = kept.shape[1]
    first, second = total[:, :half], total[:, half:]
    kept[...] = jnp.where(core == 0, first, second)
    sent[...] = jnp.where(core == 0, second, first)


def per_device(
    tokens, norm_gain, norm_shift, expert_ids, gate_weights, expert_gate, expert_up, expert_down
):
    tok_rows, features = tokens.shape
    top_count = expert_ids.shape[1]
    ep_size = lax.axis_size("ep")
    tp_size = lax.axis_size("tp")
    chips = tp_size // CORES
    total_experts = expert_gate.shape[0] * ep_size
    group_size = total_experts // GROUPS
    slots = tok_rows // 2 * top_count // group_size
    rows = ep_size * slots
    share = features // chips
    units = expert_gate.shape[2]
    swap = [(i, i ^ 1) for i in range(tp_size)]
    near = [(i, i ^ 2) for i in range(tp_size)]
    same = [(i, 6 - i // 2 * 2 + i % 2) for i in range(tp_size)]
    cross = [(i, 7 - i // 2 * 2 - i % 2) for i in range(tp_size)]
    across = [(i, i ^ 4) for i in range(tp_size)]
    anywhere = pl.BlockSpec(memory_space=pl.ANY)

    def ppermute(array, pairs):
        return lax.ppermute(array, "tp", pairs)

    mine, giving = pl.pallas_call(
        weights_kernel,
        out_shape=(pltpu.VMEM((2, units, features), jnp.bfloat16),) * 2,
        in_specs=[anywhere] * 2,
        out_specs=(VMEM,) * 2,
        scratch_shapes=[pltpu.SemaphoreType.DMA((4,))],
        compiler_params=PARAMS,
        name="split",
    )(*off_chip(expert_gate.transpose(0, 2, 1), expert_up.transpose(0, 2, 1)))
    w_same, w_cross = ppermute(mine, same), ppermute(giving, cross)
    w_swapped = ppermute(giving, swap)

    packed, select_hi, select_lo = pl.pallas_call(
        functools.partial(pack_kernel, slots=slots),
        out_shape=(
            pltpu.VMEM((rows, share), jnp.bfloat16),
            pltpu.VMEM((rows, tok_rows), jnp.bfloat16),
            pltpu.VMEM((rows, tok_rows), jnp.bfloat16),
        ),
        in_specs=[VMEM] * 5,
        out_specs=(VMEM,) * 3,
        compiler_params=PARAMS,
        name="pack",
    )(
        tokens,
        norm_gain.reshape(1, features),
        norm_shift.reshape(1, features),
        expert_ids.T,
        gate_weights.T,
    )
    arrived = lax.all_to_all(
        packed.reshape(ep_size, slots, share), "ep", split_axis=0, concat_axis=0, tiled=True
    ).reshape(rows, share)
    neighbour = ppermute(arrived, near)

    pieces = pl.pallas_call(
        pieces_kernel,
        out_shape=(pltpu.VMEM((2, units, share), jnp.bfloat16),) * chips,
        in_specs=[anywhere],
        out_specs=(VMEM,) * chips,
        scratch_shapes=[pltpu.SemaphoreType.DMA((chips,))],
        compiler_params=PARAMS,
        name="pieces",
    )(*off_chip(expert_down))
    downs = [ppermute(p, pairs) for p, pairs in zip(pieces[1:], (near, same, across))]
    downs = on_chip(pieces[0], *downs)

    hidden = pl.pallas_call(
        functools.partial(hidden_kernel, slots=slots),
        out_shape=pltpu.VMEM((rows // 2, 2 * CORES * units), jnp.bfloat16),
        in_specs=[VMEM] * 6,
        out_specs=VMEM,
        compiler_params=PARAMS,
        name="hidden",
    )(*on_chip(arrived, neighbour, mine, w_swapped, w_same, w_cross))
    hiddens = [hidden] + [ppermute(hidden, pairs) for pairs in (near, same, across)]
    d_giving = pl.pallas_call(
        give_kernel,
        out_shape=pltpu.VMEM((chips, units, share), jnp.bfloat16),
        in_specs=[VMEM] * chips,
        out_specs=VMEM,
        compiler_params=PARAMS,
        name="give",
    )(*downs)
    d_other = ppermute(d_giving, swap)
    result = pl.pallas_call(
        functools.partial(down_kernel, slots=slots),
        out_shape=pltpu.VMEM((rows, share), jnp.float32),
        in_specs=[VMEM] * (2 * chips + 1),
        out_specs=VMEM,
        compiler_params=PARAMS,
        name="down",
    )(*on_chip(*hiddens), *downs, *on_chip(d_other))
    returned = lax.all_to_all(
        result.reshape(ep_size, slots, share), "ep", split_axis=0, concat_axis=0, tiled=True
    ).reshape(rows, share)
    half = pltpu.VMEM((tok_rows, share // CORES), jnp.float32)
    kept, sent = pl.pallas_call(
        combine_kernel,
        out_shape=(half, half),
        in_specs=[VMEM] * 3,
        out_specs=(VMEM, VMEM),
        compiler_params=PARAMS,
        name="combine",
    )(*on_chip(select_hi, select_lo, returned))
    mixed_out = kept + lax.ppermute(sent, "tp", swap)
    return mixed_out.astype(jnp.bfloat16)


def solution(mesh):
    return jax.shard_map(
        per_device,
        mesh=mesh,
        in_specs=(
            P("ep", None),
            P(),
            P(),
            P("ep", None),
            P("ep", None),
            P("ep", None, "tp"),
            P("ep", None, "tp"),
            P("ep", "tp", None),
        ),
        out_specs=P("ep", "tp"),
        check_vma=False,
    )
```

profile of v0, /device:TPU:1, one launch (start us, length us, event | category | flops | bytes accessed | tf_op | source)
XLA Modules:
  0.0 96.7 jit_solution(15171696877377924228)
XLA Ops:
  0.0 0.0 copy-start.4
  0.0 0.0 copy-start.3
  0.0 0.7 copy-done.4
  0.7 0.0 copy-done.3
  0.7 0.0 copy-start
  0.7 0.9 copy-done
  1.6 0.0 copy-start.1
  1.7 0.7 copy-done.1
  2.3 0.0 copy-start.2
  2.3 0.7 copy-done.2
  3.0 1.2 %pack.1 = (bf16[256,512]{1,0:T(8,128)(2,1)}, bf16[256,64]{1,0:T(8,128)(2,1)S(1)}, bf16[256,64]{1,0:T(8,128)(2,1)S(1)}) custom-call(bf16[64,2048]{1,0:T(8,128)(2,1)S(1)} %copy-done, f32[1,2048]{1,0:T(1,128)S(1)} %bitcast.14, f32[1,2048]{1,0:T(1,128)S(1)} %bitcast.15, s32[4,64]{1,0:T(4,128)S(1)} %bitcast.16, f32[4,64]{1,0:T(4,128)S(1)} %bitcast.17), custom_call_target="tpu_custom_call" | custom-call | tf_op jit(solution)/shard_map/pack/pallas_call | solution.py:232
  4.3 11.9 %all-to-all-start = ((bf16[32,8,512]{2,1,0:T(8,128)(2,1)}), bf16[32,8,512]{2,1,0:T(8,128)(2,1)S(1)}, u32[]{:S(2)}, u32[]{:S(2)}) async-start(bf16[32,8,512]{2,1,0:T(8,128)(2,1)} %bitcast.4), calls=%async_computation | async-start | bytes 524288 | tf_op jit(solution)/shard_map/all_to_all | solution.py:250
  16.1 1.2 %split.1 = (bf16[2,64,2048]{2,1,0:T(8,128)(2,1)S(1)}, bf16[2,64,2048]{2,1,0:T(8,128)(2,1)S(1)}) custom-call(bf16[2,64,2048]{2,1,0:T(8,128)(2,1)} %bitcast.18, bf16[2,64,2048]{2,1,0:T(8,128)(2,1)} %bitcast.19), custom_call_target="tpu_custom_call" | custom-call | tf_op jit(solution)/shard_map/split/pallas_call | solution.py:220
  17.4 1.0 %collective-permute-start.1 = (bf16[2,64,2048]{2,1,0:T(8,128)(2,1)S(1)}, bf16[2,64,2048]{2,1,0:T(8,128)(2,1)S(1)}, u32[]{:S(2)}, u32[]{:S(2)}) collective-permute-start(bf16[2,64,2048]{2,1,0:T(8,128)(2,1)S(1)} %get-tuple-element.20), channel_id=1, source_target_pairs={{0,1},{1,0},{2,3},{3,2},{4,5},{5,4},{6,7},{7,6},{8,9},{9,8},{10,11... | collective-permute-start | bytes 1572872 | tf_op jit(solution)/shard_map/ppermute | solution.py:218
  18.4 2.7 %collective-permute-start.2 = (bf16[2,64,2048]{2,1,0:T(8,128)(2,1)S(1)}, bf16[2,64,2048]{2,1,0:T(8,128)(2,1)S(1)}, u32[]{:S(2)}, u32[]{:S(2)}) collective-permute-start(bf16[2,64,2048]{2,1,0:T(8,128)(2,1)S(1)} %get-tuple-element.19.mine), channel_id=1, source_target_pairs={{0,6},{1,7},{2,4},{3,5},{4,2},{5,3},{6,0},{7,1},{8,14},{9,15},{10,... | collective-permute-start | bytes 1572872 | tf_op jit(solution)/shard_map/ppermute | solution.py:218
  21.2 0.2 collective-permute-start.3
  21.4 1.8 %pieces.1 = (bf16[2,64,512]{2,1,0:T(8,128)(2,1)S(1)}, bf16[2,64,512]{2,1,0:T(8,128)(2,1)S(1)}, bf16[2,64,512]{2,1,0:T(8,128)(2,1)S(1)}, bf16[2,64,512]{2,1,0:T(8,128)(2,1)}) custom-call(bf16[2,64,2048]{2,1,0:T(8,128)(2,1)} %down.2), custom_call_target="tpu_custom_call" | custom-call | tf_op jit(solution)/shard_map/pieces/pallas_call | solution.py:255
  23.1 0.2 collective-permute-start.7
  23.3 2.7 %collective-permute-start.8 = (bf16[2,64,512]{2,1,0:T(8,128)(2,1)S(1)}, bf16[2,64,512]{2,1,0:T(8,128)(2,1)S(1)}, u32[]{:S(2)}, u32[]{:S(2)}) collective-permute-start(bf16[2,64,512]{2,1,0:T(8,128)(2,1)S(1)} %get-tuple-element.23), channel_id=1, source_target_pairs={{0,6},{1,7},{2,4},{3,5},{4,2},{5,3},{6,0},{7,1},{8,14},{9,15},{10,... | collective-permute-start | bytes 393224 | tf_op jit(solution)/shard_map/ppermute | solution.py:218
  26.1 2.0 %collective-permute-done.7.first = bf16[2,64,512]{2,1,0:T(8,128)(2,1)S(1)} collective-permute-done((bf16[2,64,512]{2,1,0:T(8,128)(2,1)S(1)}, bf16[2,64,512]{2,1,0:T(8,128)(2,1)S(1)}, u32[]{:S(2)}, u32[]{:S(2)}) %collective-permute-start.7) | collective-permute-done | bytes 131104 | tf_op jit(solution)/shard_map/ppermute | solution.py:218
  28.1 2.8 %collective-permute-start.9 = (bf16[2,64,512]{2,1,0:T(8,128)(2,1)}, bf16[2,64,512]{2,1,0:T(8,128)(2,1)S(1)}, u32[]{:S(2)}, u32[]{:S(2)}) collective-permute-start(bf16[2,64,512]{2,1,0:T(8,128)(2,1)} %get-tuple-element.24), channel_id=1, source_target_pairs={{0,4},{1,5},{2,6},{3,7},{4,0},{5,1},{6,2},{7,3},{8,12},{9,13},{10,... | collective-permute-start | bytes 393224 | tf_op jit(solution)/shard_map/ppermute | solution.py:218
  30.9 19.1 %collective-permute-done.8.second = bf16[2,64,512]{2,1,0:T(8,128)(2,1)S(1)} collective-permute-done((bf16[2,64,512]{2,1,0:T(8,128)(2,1)S(1)}, bf16[2,64,512]{2,1,0:T(8,128)(2,1)S(1)}, u32[]{:S(2)}, u32[]{:S(2)}) %collective-permute-start.8) | collective-permute-done | bytes 131104 | tf_op jit(solution)/shard_map/ppermute | solution.py:218
  50.0 0.0 all-to-all-done
  50.0 0.0 collective-permute-start
  50.0 0.0 collective-permute-done.9.third
  50.0 1.3 %collective-permute-start.10 = (bf16[4,64,512]{2,1,0:T(8,128)(2,1)S(1)}, bf16[4,64,512]{2,1,0:T(8,128)(2,1)S(1)}, u32[]{:S(2)}, u32[]{:S(2)}) collective-permute-start(bf16[4,64,512]{2,1,0:T(8,128)(2,1)S(1)} %give.1), channel_id=1, source_target_pairs={{0,1},{1,0},{2,3},{3,2},{4,5},{5,4},{6,7},{7,6},{8,9},{9,8},{10,11... | collective-permute-start | bytes 786440 | tf_op jit(solution)/shard_map/ppermute | solution.py:218
  51.3 0.0 collective-permute-done.1.swapped
  51.3 0.0 collective-permute-done.2.same
  51.3 0.0 collective-permute-done.3.cross
  51.3 5.6 %collective-permute-done.near = bf16[256,512]{1,0:T(8,128)(2,1)S(1)} collective-permute-done((bf16[256,512]{1,0:T(8,128)(2,1)S(1)}, bf16[256,512]{1,0:T(8,128)(2,1)S(1)}, u32[]{:S(2)}, u32[]{:S(2)}) %collective-permute-start) | collective-permute-done | bytes 262176 | tf_op jit(solution)/shard_map/ppermute | solution.py:218
  57.0 1.1 %hidden.1.h_own = bf16[128,256]{1,0:T(8,128)(2,1)S(1)} custom-call(bf16[256,512]{1,0:T(8,128)(2,1)S(1)} %bitcast.13, bf16[256,512]{1,0:T(8,128)(2,1)S(1)} %collective-permute-done.near, bf16[2,64,2048]{2,1,0:T(8,128)(2,1)S(1)} %get-tuple-element.19.mine, bf16[2,64,2048]{2,1,0:T(8,128)(2,1)S(1)} %collective-permute-done.1.swapped, ...), custom_call_target="tpu_custom_call" | custom-call | tf_op jit(solution)/shard_map/hidden/pallas_call | solution.py:267
  58.1 0.1 collective-permute-start.4
  58.2 2.8 %collective-permute-start.5 = (bf16[128,256]{1,0:T(8,128)(2,1)S(1)}, bf16[128,256]{1,0:T(8,128)(2,1)S(1)}, u32[]{:S(2)}, u32[]{:S(2)}) collective-permute-start(bf16[128,256]{1,0:T(8,128)(2,1)S(1)} %hidden.1.h_own), channel_id=1, source_target_pairs={{0,6},{1,7},{2,4},{3,5},{4,2},{5,3},{6,0},{7,1},{8,14},{9,15},{10,... | collective-permute-start | bytes 196616 | tf_op jit(solution)/shard_map/ppermute | solution.py:218
  61.0 0.9 collective-permute-start.6
  61.9 0.0 collective-permute-done.10.other
  61.9 0.0 collective-permute-done.4.h_first
  61.9 0.8 collective-permute-done.5.h_second
  62.7 3.4 %collective-permute-done.6.h_third = bf16[128,256]{1,0:T(8,128)(2,1)S(1)} collective-permute-done((bf16[128,256]{1,0:T(8,128)(2,1)S(1)}, bf16[128,256]{1,0:T(8,128)(2,1)S(1)}, u32[]{:S(2)}, u32[]{:S(2)}) %collective-permute-start.6) | collective-permute-done | bytes 65568 | tf_op jit(solution)/shard_map/ppermute | solution.py:218
  66.1 0.4 down.3
  66.6 23.3 %all_to_all.10 = f32[32,8,512]{2,1,0:T(8,128)S(1)} all-to-all(f32[32,8,512]{2,1,0:T(8,128)S(1)} %bitcast.10), channel_id=1, replica_groups=mesh['ep'=32,'tp'=8] {'ep'}, dimensions={0} | all-to-all | bytes 1048576 | tf_op jit(solution)/shard_map/all_to_all | solution.py:293
  89.8 0.3 combine.1
  90.1 5.1 %collective-permute-start.11 = (f32[64,256]{1,0:T(8,128)S(1)}, f32[64,256]{1,0:T(8,128)S(1)}, u32[]{:S(2)}, u32[]{:S(2)}) collective-permute-start(f32[64,256]{1,0:T(8,128)S(1)} %get-tuple-element.26), channel_id=1, source_target_pairs={{0,1},{1,0},{2,3},{3,2},{4,5},{5,4},{6,7},{7,6},{8,9},{9,8},{10,11... | collective-permute-start | bytes 196616 | tf_op jit(solution)/shard_map/ppermute | solution.py:305
  95.2 0.9 collective-permute-done.11
  96.1 0.6 add_convert_fusion
  (1 shorter events, 0.0 us)
Async XLA Ops:
  0.0 0.7 copy-start.4
  0.0 0.7 copy-start.3
  0.7 0.9 copy-start
  1.6 0.7 copy-start.1
  2.3 0.7 copy-start.2
  4.3 45.7 %all-to-all-start = ((bf16[32,8,512]{2,1,0:T(8,128)(2,1)}), bf16[32,8,512]{2,1,0:T(8,128)(2,1)S(1)}, u32[]{:S(2)}, u32[]{:S(2)}) async-start(bf16[32,8,512]{2,1,0:T(8,128)(2,1)} %bitcast.4), calls=%async_computation | async-start | bytes 524288 | tf_op jit(solution)/shard_map/all_to_all | solution.py:250
  17.4 33.9 %collective-permute-start.1 = (bf16[2,64,2048]{2,1,0:T(8,128)(2,1)S(1)}, bf16[2,64,2048]{2,1,0:T(8,128)(2,1)S(1)}, u32[]{:S(2)}, u32[]{:S(2)}) collective-permute-start(bf16[2,64,2048]{2,1,0:T(8,128)(2,1)S(1)} %get-tuple-element.20), channel_id=1, source_target_pairs={{0,1},{1,0},{2,3},{3,2},{4,5},{5,4},{6,7},{7,6},{8,9},{9,8},{10,11... | collective-permute-start | bytes 1572872 | tf_op jit(solution)/shard_map/ppermute | solution.py:218
  18.4 32.9 %collective-permute-start.2 = (bf16[2,64,2048]{2,1,0:T(8,128)(2,1)S(1)}, bf16[2,64,2048]{2,1,0:T(8,128)(2,1)S(1)}, u32[]{:S(2)}, u32[]{:S(2)}) collective-permute-start(bf16[2,64,2048]{2,1,0:T(8,128)(2,1)S(1)} %get-tuple-element.19.mine), channel_id=1, source_target_pairs={{0,6},{1,7},{2,4},{3,5},{4,2},{5,3},{6,0},{7,1},{8,14},{9,15},{10,... | collective-permute-start | bytes 1572872 | tf_op jit(solution)/shard_map/ppermute | solution.py:218
  21.2 30.2 %collective-permute-start.3 = (bf16[2,64,2048]{2,1,0:T(8,128)(2,1)S(1)}, bf16[2,64,2048]{2,1,0:T(8,128)(2,1)S(1)}, u32[]{:S(2)}, u32[]{:S(2)}) collective-permute-start(bf16[2,64,2048]{2,1,0:T(8,128)(2,1)S(1)} %get-tuple-element.20), channel_id=1, source_target_pairs={{0,7},{1,6},{2,5},{3,4},{4,3},{5,2},{6,1},{7,0},{8,15},{9,14},{10,... | collective-permute-start | bytes 1572872 | tf_op jit(solution)/shard_map/ppermute | solution.py:218
  23.1 5.0 %collective-permute-start.7 = (bf16[2,64,512]{2,1,0:T(8,128)(2,1)S(1)}, bf16[2,64,512]{2,1,0:T(8,128)(2,1)S(1)}, u32[]{:S(2)}, u32[]{:S(2)}) collective-permute-start(bf16[2,64,512]{2,1,0:T(8,128)(2,1)S(1)} %get-tuple-element.22), channel_id=1, source_target_pairs={{0,2},{1,3},{2,0},{3,1},{4,6},{5,7},{6,4},{7,5},{8,10},{9,11},{10,... | collective-permute-start | bytes 393224 | tf_op jit(solution)/shard_map/ppermute | solution.py:218
  23.3 26.7 %collective-permute-start.8 = (bf16[2,64,512]{2,1,0:T(8,128)(2,1)S(1)}, bf16[2,64,512]{2,1,0:T(8,128)(2,1)S(1)}, u32[]{:S(2)}, u32[]{:S(2)}) collective-permute-start(bf16[2,64,512]{2,1,0:T(8,128)(2,1)S(1)} %get-tuple-element.23), channel_id=1, source_target_pairs={{0,6},{1,7},{2,4},{3,5},{4,2},{5,3},{6,0},{7,1},{8,14},{9,15},{10,... | collective-permute-start | bytes 393224 | tf_op jit(solution)/shard_map/ppermute | solution.py:218
  28.1 21.9 %collective-permute-start.9 = (bf16[2,64,512]{2,1,0:T(8,128)(2,1)}, bf16[2,64,512]{2,1,0:T(8,128)(2,1)S(1)}, u32[]{:S(2)}, u32[]{:S(2)}) collective-permute-start(bf16[2,64,512]{2,1,0:T(8,128)(2,1)} %get-tuple-element.24), channel_id=1, source_target_pairs={{0,4},{1,5},{2,6},{3,7},{4,0},{5,1},{6,2},{7,3},{8,12},{9,13},{10,... | collective-permute-start | bytes 393224 | tf_op jit(solution)/shard_map/ppermute | solution.py:218
  50.0 7.0 %collective-permute-start = (bf16[256,512]{1,0:T(8,128)(2,1)S(1)}, bf16[256,512]{1,0:T(8,128)(2,1)S(1)}, u32[]{:S(2)}, u32[]{:S(2)}) collective-permute-start(bf16[256,512]{1,0:T(8,128)(2,1)S(1)} %bitcast.12), channel_id=1, source_target_pairs={{0,2},{1,3},{2,0},{3,1},{4,6},{5,7},{6,4},{7,5},{8,10},{9,11},{10,... | collective-permute-start | bytes 786440 | tf_op jit(solution)/shard_map/ppermute | solution.py:218
  50.0 11.9 %collective-permute-start.10 = (bf16[4,64,512]{2,1,0:T(8,128)(2,1)S(1)}, bf16[4,64,512]{2,1,0:T(8,128)(2,1)S(1)}, u32[]{:S(2)}, u32[]{:S(2)}) collective-permute-start(bf16[4,64,512]{2,1,0:T(8,128)(2,1)S(1)} %give.1), channel_id=1, source_target_pairs={{0,1},{1,0},{2,3},{3,2},{4,5},{5,4},{6,7},{7,6},{8,9},{9,8},{10,11... | collective-permute-start | bytes 786440 | tf_op jit(solution)/shard_map/ppermute | solution.py:218
  58.1 3.8 %collective-permute-start.4 = (bf16[128,256]{1,0:T(8,128)(2,1)S(1)}, bf16[128,256]{1,0:T(8,128)(2,1)S(1)}, u32[]{:S(2)}, u32[]{:S(2)}) collective-permute-start(bf16[128,256]{1,0:T(8,128)(2,1)S(1)} %hidden.1.h_own), channel_id=1, source_target_pairs={{0,2},{1,3},{2,0},{3,1},{4,6},{5,7},{6,4},{7,5},{8,10},{9,11},{10,... | collective-permute-start | bytes 196616 | tf_op jit(solution)/shard_map/ppermute | solution.py:218
  58.2 4.5 %collective-permute-start.5 = (bf16[128,256]{1,0:T(8,128)(2,1)S(1)}, bf16[128,256]{1,0:T(8,128)(2,1)S(1)}, u32[]{:S(2)}, u32[]{:S(2)}) collective-permute-start(bf16[128,256]{1,0:T(8,128)(2,1)S(1)} %hidden.1.h_own), channel_id=1, source_target_pairs={{0,6},{1,7},{2,4},{3,5},{4,2},{5,3},{6,0},{7,1},{8,14},{9,15},{10,... | collective-permute-start | bytes 196616 | tf_op jit(solution)/shard_map/ppermute | solution.py:218
  61.0 5.1 %collective-permute-start.6 = (bf16[128,256]{1,0:T(8,128)(2,1)S(1)}, bf16[128,256]{1,0:T(8,128)(2,1)S(1)}, u32[]{:S(2)}, u32[]{:S(2)}) collective-permute-start(bf16[128,256]{1,0:T(8,128)(2,1)S(1)} %hidden.1.h_own), channel_id=1, source_target_pairs={{0,4},{1,5},{2,6},{3,7},{4,0},{5,1},{6,2},{7,3},{8,12},{9,13},{10,... | collective-permute-start | bytes 196616 | tf_op jit(solution)/shard_map/ppermute | solution.py:218
  90.1 6.0 %collective-permute-start.11 = (f32[64,256]{1,0:T(8,128)S(1)}, f32[64,256]{1,0:T(8,128)S(1)}, u32[]{:S(2)}, u32[]{:S(2)}) collective-permute-start(f32[64,256]{1,0:T(8,128)S(1)} %get-tuple-element.26), channel_id=1, source_target_pairs={{0,1},{1,0},{2,3},{3,2},{4,5},{5,4},{6,7},{7,6},{8,9},{9,8},{10,11... | collective-permute-start | bytes 196616 | tf_op jit(solution)/shard_map/ppermute | solution.py:305
where the time goes:
time: 97.1 us; the launch traced here: 96.7 us
  waiting for transfers between devices  31.9 us (33%)
  starting transfers between devices  31.7 us (33%)
  blocking collectives  23.3 us (24%)
  Pallas kernels  6.11 us (6%)
  local copies, waits for them, and re-layouts  3.04 us (3%)
    ppermute x11, waiting for transfers between devices, ppermute(): return lax.ppermute(array, 'tp', pairs)  31 us
    all_to_all x1, blocking collectives, per_device(): lax.all_to_all(result.reshape(ep_size, slots, share), 'ep', split_axis=0,...  23.3 us
    ppermute x11, starting transfers between devices, ppermute(): return lax.ppermute(array, 'tp', pairs)  14.8 us
    all_to_all x1, starting transfers between devices, per_device(): lax.all_to_all(packed.reshape(ep_size, slots, share), 'ep', split_axis=0,...  11.9 us
    ppermute x1, starting transfers between devices, per_device(): mixed_out = kept + lax.ppermute(sent, 'tp', swap)  5.08 us
    unnamed x10, local copies, waits for them, and re-layouts  3.04 us
  transfers between devices with their start and end apart: 13, of which 6 were waited for; matrix products, arithmetic and copies ran while one was open for 0% of the time, Pallas kernels for 4%

commit v1 on v0

--- a/solution.py
+++ b/solution.py
@@ -57,16 +57,13 @@
     return copies
 
 
-def weights_kernel(gate, up, mine, giving, sems):
-    _, core = position()
+def pack_kernel(
+    tokens, gain, shift, ids, weights, gate, up, packed, select_hi, select_lo, mine, giving, sems, *, slots
+):
+    y, core = position()
     pairs = [(ref.at[core], mine.at[i]) for i, ref in enumerate((gate, up))]
     pairs += [(ref.at[1 - core], giving.at[i]) for i, ref in enumerate((gate, up))]
-    for copy in copy_all(pairs, sems):
-        copy.wait()
-
-
-def pack_kernel(tokens, gain, shift, ids, weights, packed, select_hi, select_lo, *, slots):
-    y, core = position()
+    copies = copy_all(pairs, sems)
     row_half, feature_half = part(y)
     top_count, rows = ids.shape
     total = packed.shape[0]
@@ -106,6 +103,8 @@
     high = factor.astype(jnp.bfloat16)
     select_hi[...] = high
     select_lo[...] = (factor - high.astype(jnp.float32)).astype(jnp.bfloat16)
+    for copy in copies:
+        copy.wait()
 
 
 def pieces_kernel(down, own, first, second, third, sems):
@@ -217,36 +216,33 @@
     def ppermute(array, pairs):
         return lax.ppermute(array, "tp", pairs)
 
-    mine, giving = pl.pallas_call(
-        weights_kernel,
-        out_shape=(pltpu.VMEM((2, units, features), jnp.bfloat16),) * 2,
-        in_specs=[anywhere] * 2,
-        out_specs=(VMEM,) * 2,
-        scratch_shapes=[pltpu.SemaphoreType.DMA((4,))],
-        compiler_params=PARAMS,
-        name="split",
-    )(*off_chip(expert_gate.transpose(0, 2, 1), expert_up.transpose(0, 2, 1)))
-    w_same, w_cross = ppermute(mine, same), ppermute(giving, cross)
-    w_swapped = ppermute(giving, swap)
-
-    packed, select_hi, select_lo = pl.pallas_call(
+    packed, select_hi, select_lo, mine, giving = pl.pallas_call(
         functools.partial(pack_kernel, slots=slots),
         out_shape=(
             pltpu.VMEM((rows, share), jnp.bfloat16),
             pltpu.VMEM((rows, tok_rows), jnp.bfloat16),
             pltpu.VMEM((rows, tok_rows), jnp.bfloat16),
+            pltpu.VMEM((2, units, features), jnp.bfloat16),
+            pltpu.VMEM((2, units, features), jnp.bfloat16),
         ),
-        in_specs=[VMEM] * 5,
-        out_specs=(VMEM,) * 3,
+        in_specs=[VMEM] * 5 + [anywhere] * 2,
+        out_specs=(VMEM,) * 5,
+        scratch_shapes=[pltpu.SemaphoreType.DMA((4,))],
         compiler_params=PARAMS,
         name="pack",
     )(
-        tokens,
-        norm_gain.reshape(1, features),
-        norm_shift.reshape(1, features),
-        expert_ids.T,
-        gate_weights.T,
+        *off_chip(
+            tokens,
+            norm_gain.reshape(1, features),
+            norm_shift.reshape(1, features),
+            expert_ids.T,
+            gate_weights.T,
+            expert_gate.transpose(0, 2, 1),
+            expert_up.transpose(0, 2, 1),
+        )
     )
+    w_same, w_cross = ppermute(mine, same), ppermute(giving, cross)
+    w_swapped = ppermute(giving, swap)
     arrived = lax.all_to_all(
         packed.reshape(ep_size, slots, share), "ep", split_axis=0, concat_axis=0, tiled=True
     ).reshape(rows, share)

time: 97.1 us -> 94.6 us (0.974)
  local copies, waits for them, and re-layouts: 3.04 us -> 0 us
    unnamed x10 -> x0, local copies, waits for them, and re-layouts: 3.04 us -> none
    pallas_call x1, Pallas kernels: 1.24 us -> 3.15 us  [per_device(): pl.pallas_call(functools.partial(pack_kernel, slots=slots), out_shape=(pl...]
    pallas_call x1 -> x0, Pallas kernels: 1.23 us -> none  [per_device(): pl.pallas_call(weights_kernel, out_shape=(pltpu.VMEM((2, units, features)...]
  transfers between devices with their start and end apart: 13 -> 13, of which waited for: 6 -> 6; matrix products, arithmetic and copies ran while one was open for 0% -> 0% of each run, Pallas kernels for 4% -> 3%
where the time goes in v1:
time: 94.6 us; the launch traced here: 94.4 us
  waiting for transfers between devices  31.9 us (34%)
  starting transfers between devices  31.7 us (34%)
  blocking collectives  23.3 us (25%)
  Pallas kernels  6.79 us (7%)
    ppermute x11, waiting for transfers between devices, ppermute(): return lax.ppermute(array, 'tp', pairs)  31 us
    all_to_all x1, blocking collectives, per_device(): lax.all_to_all(result.reshape(ep_size, slots, share), 'ep', split_axis=0,...  23.3 us
    ppermute x11, starting transfers between devices, ppermute(): return lax.ppermute(array, 'tp', pairs)  14.8 us
    all_to_all x1, starting transfers between devices, per_device(): lax.all_to_all(packed.reshape(ep_size, slots, share), 'ep', split_axis=0,...  11.9 us
    ppermute x1, starting transfers between devices, per_device(): mixed_out = kept + lax.ppermute(sent, 'tp', swap)  5.08 us
    pallas_call x1, Pallas kernels, per_device(): pl.pallas_call(functools.partial(pack_kernel, slots=slots), out_shape=(pl...  3.15 us
  transfers between devices with their start and end apart: 13, of which 6 were waited for; matrix products, arithmetic and copies ran while one was open for 0% of the time, Pallas kernels for 3%

profile of v1, /device:TPU:1, one launch (start us, length us, event | category | flops | bytes accessed | tf_op | source)
XLA Modules:
  0.0 94.4 jit_solution(11563547898992504470)
XLA Ops:
  0.0 3.1 %pack.1 = (bf16[256,512]{1,0:T(8,128)(2,1)}, bf16[256,64]{1,0:T(8,128)(2,1)S(1)}, bf16[256,64]{1,0:T(8,128)(2,1)S(1)}, bf16[2,64,2048]{2,1,0:T(8,128)(2,1)S(1)}, bf16[2,64,2048]{2,1,0:T(8,128)(2,1)S(1)}) custom-call(bf16[64,2048]{1,0:T(8,128)(2,1)} %tokens.1, f32[1,2048]{1,0:T(1,128)} %bitcast.16, f32[1,2048]{1,0:T(1,128)} %bitcast.17, s32[4,64]{1,0:T(4,128)} %bitcast.18, ...), custom_call_target="tpu_custom_call" | custom-call | tf_op jit(solution)/shard_map/pack/pallas_call | solution.py:219
  3.2 11.9 %all-to-all-start = ((bf16[32,8,512]{2,1,0:T(8,128)(2,1)}), bf16[32,8,512]{2,1,0:T(8,128)(2,1)S(1)}, u32[]{:S(2)}, u32[]{:S(2)}) async-start(bf16[32,8,512]{2,1,0:T(8,128)(2,1)} %bitcast.6), calls=%async_computation | async-start | bytes 524288 | tf_op jit(solution)/shard_map/all_to_all | solution.py:246
  15.0 1.0 %collective-permute-start.1 = (bf16[2,64,2048]{2,1,0:T(8,128)(2,1)S(1)}, bf16[2,64,2048]{2,1,0:T(8,128)(2,1)S(1)}, u32[]{:S(2)}, u32[]{:S(2)}) collective-permute-start(bf16[2,64,2048]{2,1,0:T(8,128)(2,1)S(1)} %get-tuple-element.20), channel_id=1, source_target_pairs={{0,1},{1,0},{2,3},{3,2},{4,5},{5,4},{6,7},{7,6},{8,9},{9,8},{10,11... | collective-permute-start | bytes 1572872 | tf_op jit(solution)/shard_map/ppermute | solution.py:217
  16.1 2.7 %collective-permute-start.2 = (bf16[2,64,2048]{2,1,0:T(8,128)(2,1)S(1)}, bf16[2,64,2048]{2,1,0:T(8,128)(2,1)S(1)}, u32[]{:S(2)}, u32[]{:S(2)}) collective-permute-start(bf16[2,64,2048]{2,1,0:T(8,128)(2,1)S(1)} %get-tuple-element.19.mine), channel_id=1, source_target_pairs={{0,6},{1,7},{2,4},{3,5},{4,2},{5,3},{6,0},{7,1},{8,14},{9,15},{10,... | collective-permute-start | bytes 1572872 | tf_op jit(solution)/shard_map/ppermute | solution.py:217
  18.8 0.2 collective-permute-start.3
  19.0 1.8 %pieces.1 = (bf16[2,64,512]{2,1,0:T(8,128)(2,1)S(1)}, bf16[2,64,512]{2,1,0:T(8,128)(2,1)S(1)}, bf16[2,64,512]{2,1,0:T(8,128)(2,1)S(1)}, bf16[2,64,512]{2,1,0:T(8,128)(2,1)}) custom-call(bf16[2,64,2048]{2,1,0:T(8,128)(2,1)} %down.2), custom_call_target="tpu_custom_call" | custom-call | tf_op jit(solution)/shard_map/pieces/pallas_call | solution.py:251
  20.8 0.2 collective-permute-start.7
  21.0 2.7 %collective-permute-start.8 = (bf16[2,64,512]{2,1,0:T(8,128)(2,1)S(1)}, bf16[2,64,512]{2,1,0:T(8,128)(2,1)S(1)}, u32[]{:S(2)}, u32[]{:S(2)}) collective-permute-start(bf16[2,64,512]{2,1,0:T(8,128)(2,1)S(1)} %get-tuple-element.23), channel_id=1, source_target_pairs={{0,6},{1,7},{2,4},{3,5},{4,2},{5,3},{6,0},{7,1},{8,14},{9,15},{10,... | collective-permute-start | bytes 393224 | tf_op jit(solution)/shard_map/ppermute | solution.py:217
  23.7 2.0 %collective-permute-done.7.first = bf16[2,64,512]{2,1,0:T(8,128)(2,1)S(1)} collective-permute-done((bf16[2,64,512]{2,1,0:T(8,128)(2,1)S(1)}, bf16[2,64,512]{2,1,0:T(8,128)(2,1)S(1)}, u32[]{:S(2)}, u32[]{:S(2)}) %collective-permute-start.7) | collective-permute-done | bytes 131104 | tf_op jit(solution)/shard_map/ppermute | solution.py:217
  25.8 2.8 %collective-permute-start.9 = (bf16[2,64,512]{2,1,0:T(8,128)(2,1)}, bf16[2,64,512]{2,1,0:T(8,128)(2,1)S(1)}, u32[]{:S(2)}, u32[]{:S(2)}) collective-permute-start(bf16[2,64,512]{2,1,0:T(8,128)(2,1)} %get-tuple-element.24), channel_id=1, source_target_pairs={{0,4},{1,5},{2,6},{3,7},{4,0},{5,1},{6,2},{7,3},{8,12},{9,13},{10,... | collective-permute-start | bytes 393224 | tf_op jit(solution)/shard_map/ppermute | solution.py:217
  28.6 19.1 %collective-permute-done.8.second = bf16[2,64,512]{2,1,0:T(8,128)(2,1)S(1)} collective-permute-done((bf16[2,64,512]{2,1,0:T(8,128)(2,1)S(1)}, bf16[2,64,512]{2,1,0:T(8,128)(2,1)S(1)}, u32[]{:S(2)}, u32[]{:S(2)}) %collective-permute-start.8) | collective-permute-done | bytes 131104 | tf_op jit(solution)/shard_map/ppermute | solution.py:217
  47.6 0.0 all-to-all-done
  47.6 0.0 collective-permute-start
  47.6 0.0 collective-permute-done.9.third
  47.7 1.3 %collective-permute-start.10 = (bf16[4,64,512]{2,1,0:T(8,128)(2,1)S(1)}, bf16[4,64,512]{2,1,0:T(8,128)(2,1)S(1)}, u32[]{:S(2)}, u32[]{:S(2)}) collective-permute-start(bf16[4,64,512]{2,1,0:T(8,128)(2,1)S(1)} %give.1), channel_id=1, source_target_pairs={{0,1},{1,0},{2,3},{3,2},{4,5},{5,4},{6,7},{7,6},{8,9},{9,8},{10,11... | collective-permute-start | bytes 786440 | tf_op jit(solution)/shard_map/ppermute | solution.py:217
  49.0 0.0 collective-permute-done.1.swapped
  49.0 0.0 collective-permute-done.2.same
  49.0 0.0 collective-permute-done.3.cross
  49.0 5.6 %collective-permute-done.near = bf16[256,512]{1,0:T(8,128)(2,1)S(1)} collective-permute-done((bf16[256,512]{1,0:T(8,128)(2,1)S(1)}, bf16[256,512]{1,0:T(8,128)(2,1)S(1)}, u32[]{:S(2)}, u32[]{:S(2)}) %collective-permute-start) | collective-permute-done | bytes 262176 | tf_op jit(solution)/shard_map/ppermute | solution.py:217
  54.6 1.1 %hidden.1.h_own = bf16[128,256]{1,0:T(8,128)(2,1)S(1)} custom-call(bf16[256,512]{1,0:T(8,128)(2,1)S(1)} %bitcast.13, bf16[256,512]{1,0:T(8,128)(2,1)S(1)} %collective-permute-done.near, bf16[2,64,2048]{2,1,0:T(8,128)(2,1)S(1)} %get-tuple-element.19.mine, bf16[2,64,2048]{2,1,0:T(8,128)(2,1)S(1)} %collective-permute-done.1.swapped, ...), custom_call_target="tpu_custom_call" | custom-call | tf_op jit(solution)/shard_map/hidden/pallas_call | solution.py:263
  55.7 0.1 collective-permute-start.4
  55.8 2.8 %collective-permute-start.5 = (bf16[128,256]{1,0:T(8,128)(2,1)S(1)}, bf16[128,256]{1,0:T(8,128)(2,1)S(1)}, u32[]{:S(2)}, u32[]{:S(2)}) collective-permute-start(bf16[128,256]{1,0:T(8,128)(2,1)S(1)} %hidden.1.h_own), channel_id=1, source_target_pairs={{0,6},{1,7},{2,4},{3,5},{4,2},{5,3},{6,0},{7,1},{8,14},{9,15},{10,... | collective-permute-start | bytes 196616 | tf_op jit(solution)/shard_map/ppermute | solution.py:217
  58.7 0.9 collective-permute-start.6
  59.6 0.0 collective-permute-done.10.other
  59.6 0.0 collective-permute-done.4.h_first
  59.6 0.8 collective-permute-done.5.h_second
  60.4 3.4 %collective-permute-done.6.h_third = bf16[128,256]{1,0:T(8,128)(2,1)S(1)} collective-permute-done((bf16[128,256]{1,0:T(8,128)(2,1)S(1)}, bf16[128,256]{1,0:T(8,128)(2,1)S(1)}, u32[]{:S(2)}, u32[]{:S(2)}) %collective-permute-start.6) | collective-permute-done | bytes 65568 | tf_op jit(solution)/shard_map/ppermute | solution.py:217
  63.8 0.4 down.3
  64.2 23.3 %all_to_all.10 = f32[32,8,512]{2,1,0:T(8,128)S(1)} all-to-all(f32[32,8,512]{2,1,0:T(8,128)S(1)} %bitcast.10), channel_id=1, replica_groups=mesh['ep'=32,'tp'=8] {'ep'}, dimensions={0} | all-to-all | bytes 1048576 | tf_op jit(solution)/shard_map/all_to_all | solution.py:289
  87.5 0.3 combine.1
  87.8 5.1 %collective-permute-start.11 = (f32[64,256]{1,0:T(8,128)S(1)}, f32[64,256]{1,0:T(8,128)S(1)}, u32[]{:S(2)}, u32[]{:S(2)}) collective-permute-start(f32[64,256]{1,0:T(8,128)S(1)} %get-tuple-element.26), channel_id=1, source_target_pairs={{0,1},{1,0},{2,3},{3,2},{4,5},{5,4},{6,7},{7,6},{8,9},{9,8},{10,11... | collective-permute-start | bytes 196616 | tf_op jit(solution)/shard_map/ppermute | solution.py:301
  92.8 0.9 collective-permute-done.11
  93.7 0.6 add_convert_fusion
  (1 shorter events, 0.0 us)
Async XLA Ops:
  3.2 44.5 %all-to-all-start = ((bf16[32,8,512]{2,1,0:T(8,128)(2,1)}), bf16[32,8,512]{2,1,0:T(8,128)(2,1)S(1)}, u32[]{:S(2)}, u32[]{:S(2)}) async-start(bf16[32,8,512]{2,1,0:T(8,128)(2,1)} %bitcast.6), calls=%async_computation | async-start | bytes 524288 | tf_op jit(solution)/shard_map/all_to_all | solution.py:246
  15.0 33.9 %collective-permute-start.1 = (bf16[2,64,2048]{2,1,0:T(8,128)(2,1)S(1)}, bf16[2,64,2048]{2,1,0:T(8,128)(2,1)S(1)}, u32[]{:S(2)}, u32[]{:S(2)}) collective-permute-start(bf16[2,64,2048]{2,1,0:T(8,128)(2,1)S(1)} %get-tuple-element.20), channel_id=1, source_target_pairs={{0,1},{1,0},{2,3},{3,2},{4,5},{5,4},{6,7},{7,6},{8,9},{9,8},{10,11... | collective-permute-start | bytes 1572872 | tf_op jit(solution)/shard_map/ppermute | solution.py:217
  16.1 32.9 %collective-permute-start.2 = (bf16[2,64,2048]{2,1,0:T(8,128)(2,1)S(1)}, bf16[2,64,2048]{2,1,0:T(8,128)(2,1)S(1)}, u32[]{:S(2)}, u32[]{:S(2)}) collective-permute-start(bf16[2,64,2048]{2,1,0:T(8,128)(2,1)S(1)} %get-tuple-element.19.mine), channel_id=1, source_target_pairs={{0,6},{1,7},{2,4},{3,5},{4,2},{5,3},{6,0},{7,1},{8,14},{9,15},{10,... | collective-permute-start | bytes 1572872 | tf_op jit(solution)/shard_map/ppermute | solution.py:217
  18.8 30.2 %collective-permute-start.3 = (bf16[2,64,2048]{2,1,0:T(8,128)(2,1)S(1)}, bf16[2,64,2048]{2,1,0:T(8,128)(2,1)S(1)}, u32[]{:S(2)}, u32[]{:S(2)}) collective-permute-start(bf16[2,64,2048]{2,1,0:T(8,128)(2,1)S(1)} %get-tuple-element.20), channel_id=1, source_target_pairs={{0,7},{1,6},{2,5},{3,4},{4,3},{5,2},{6,1},{7,0},{8,15},{9,14},{10,... | collective-permute-start | bytes 1572872 | tf_op jit(solution)/shard_map/ppermute | solution.py:217
  20.8 5.0 %collective-permute-start.7 = (bf16[2,64,512]{2,1,0:T(8,128)(2,1)S(1)}, bf16[2,64,512]{2,1,0:T(8,128)(2,1)S(1)}, u32[]{:S(2)}, u32[]{:S(2)}) collective-permute-start(bf16[2,64,512]{2,1,0:T(8,128)(2,1)S(1)} %get-tuple-element.22), channel_id=1, source_target_pairs={{0,2},{1,3},{2,0},{3,1},{4,6},{5,7},{6,4},{7,5},{8,10},{9,11},{10,... | collective-permute-start | bytes 393224 | tf_op jit(solution)/shard_map/ppermute | solution.py:217
  21.0 26.7 %collective-permute-start.8 = (bf16[2,64,512]{2,1,0:T(8,128)(2,1)S(1)}, bf16[2,64,512]{2,1,0:T(8,128)(2,1)S(1)}, u32[]{:S(2)}, u32[]{:S(2)}) collective-permute-start(bf16[2,64,512]{2,1,0:T(8,128)(2,1)S(1)} %get-tuple-element.23), channel_id=1, source_target_pairs={{0,6},{1,7},{2,4},{3,5},{4,2},{5,3},{6,0},{7,1},{8,14},{9,15},{10,... | collective-permute-start | bytes 393224 | tf_op jit(solution)/shard_map/ppermute | solution.py:217
  25.8 21.9 %collective-permute-start.9 = (bf16[2,64,512]{2,1,0:T(8,128)(2,1)}, bf16[2,64,512]{2,1,0:T(8,128)(2,1)S(1)}, u32[]{:S(2)}, u32[]{:S(2)}) collective-permute-start(bf16[2,64,512]{2,1,0:T(8,128)(2,1)} %get-tuple-element.24), channel_id=1, source_target_pairs={{0,4},{1,5},{2,6},{3,7},{4,0},{5,1},{6,2},{7,3},{8,12},{9,13},{10,... | collective-permute-start | bytes 393224 | tf_op jit(solution)/shard_map/ppermute | solution.py:217
  47.6 7.0 %collective-permute-start = (bf16[256,512]{1,0:T(8,128)(2,1)S(1)}, bf16[256,512]{1,0:T(8,128)(2,1)S(1)}, u32[]{:S(2)}, u32[]{:S(2)}) collective-permute-start(bf16[256,512]{1,0:T(8,128)(2,1)S(1)} %bitcast.12), channel_id=1, source_target_pairs={{0,2},{1,3},{2,0},{3,1},{4,6},{5,7},{6,4},{7,5},{8,10},{9,11},{10,... | collective-permute-start | bytes 786440 | tf_op jit(solution)/shard_map/ppermute | solution.py:217
  47.7 11.9 %collective-permute-start.10 = (bf16[4,64,512]{2,1,0:T(8,128)(2,1)S(1)}, bf16[4,64,512]{2,1,0:T(8,128)(2,1)S(1)}, u32[]{:S(2)}, u32[]{:S(2)}) collective-permute-start(bf16[4,64,512]{2,1,0:T(8,128)(2,1)S(1)} %give.1), channel_id=1, source_target_pairs={{0,1},{1,0},{2,3},{3,2},{4,5},{5,4},{6,7},{7,6},{8,9},{9,8},{10,11... | collective-permute-start | bytes 786440 | tf_op jit(solution)/shard_map/ppermute | solution.py:217
  55.7 3.8 %collective-permute-start.4 = (bf16[128,256]{1,0:T(8,128)(2,1)S(1)}, bf16[128,256]{1,0:T(8,128)(2,1)S(1)}, u32[]{:S(2)}, u32[]{:S(2)}) collective-permute-start(bf16[128,256]{1,0:T(8,128)(2,1)S(1)} %hidden.1.h_own), channel_id=1, source_target_pairs={{0,2},{1,3},{2,0},{3,1},{4,6},{5,7},{6,4},{7,5},{8,10},{9,11},{10,... | collective-permute-start | bytes 196616 | tf_op jit(solution)/shard_map/ppermute | solution.py:217
  55.8 4.6 %collective-permute-start.5 = (bf16[128,256]{1,0:T(8,128)(2,1)S(1)}, bf16[128,256]{1,0:T(8,128)(2,1)S(1)}, u32[]{:S(2)}, u32[]{:S(2)}) collective-permute-start(bf16[128,256]{1,0:T(8,128)(2,1)S(1)} %hidden.1.h_own), channel_id=1, source_target_pairs={{0,6},{1,7},{2,4},{3,5},{4,2},{5,3},{6,0},{7,1},{8,14},{9,15},{10,... | collective-permute-start | bytes 196616 | tf_op jit(solution)/shard_map/ppermute | solution.py:217
  58.7 5.1 %collective-permute-start.6 = (bf16[128,256]{1,0:T(8,128)(2,1)S(1)}, bf16[128,256]{1,0:T(8,128)(2,1)S(1)}, u32[]{:S(2)}, u32[]{:S(2)}) collective-permute-start(bf16[128,256]{1,0:T(8,128)(2,1)S(1)} %hidden.1.h_own), channel_id=1, source_target_pairs={{0,4},{1,5},{2,6},{3,7},{4,0},{5,1},{6,2},{7,3},{8,12},{9,13},{10,... | collective-permute-start | bytes 196616 | tf_op jit(solution)/shard_map/ppermute | solution.py:217
  87.8 6.0 %collective-permute-start.11 = (f32[64,256]{1,0:T(8,128)S(1)}, f32[64,256]{1,0:T(8,128)S(1)}, u32[]{:S(2)}, u32[]{:S(2)}) collective-permute-start(f32[64,256]{1,0:T(8,128)S(1)} %get-tuple-element.26), channel_id=1, source_target_pairs={{0,1},{1,0},{2,3},{3,2},{4,5},{5,4},{6,7},{7,6},{8,9},{9,8},{10,11... | collective-permute-start | bytes 196616 | tf_op jit(solution)/shard_map/ppermute | solution.py:301

commit v2 on v0

--- a/solution.py
+++ b/solution.py
@@ -13,7 +13,7 @@
 EPSILON = 1e-05
 
 VMEM = pl.BlockSpec(memory_space=pltpu.VMEM)
-PARAMS = pltpu.CompilerParams(vmem_limit_bytes=20 * 1024 * 1024)
+PARAMS = pltpu.CompilerParams(vmem_limit_bytes=12 * 1024 * 1024)
 
 
 def on_chip(*arrays):
@@ -57,7 +57,7 @@
     return copies
 
 
-def weights_kernel(gate, up, mine, giving, sems):
+def ours_kernel(gate, up, mine, giving, sems):
     _, core = position()
     pairs = [(ref.at[core], mine.at[i]) for i, ref in enumerate((gate, up))]
     pairs += [(ref.at[1 - core], giving.at[i]) for i, ref in enumerate((gate, up))]
@@ -65,20 +65,22 @@
         copy.wait()
 
 
+def pick_kernel(both, giving):
+    _, core = position()
+    giving[...] = both[1 - core]
+
+
 def pack_kernel(tokens, gain, shift, ids, weights, packed, select_hi, select_lo, *, slots):
     y, core = position()
-    row_half, feature_half = part(y)
+    row_half, _ = part(y)
     top_count, rows = ids.shape
     total = packed.shape[0]
     experts = total // slots
     width = packed.shape[1]
-    share = 2 * width
     values = tokens[...].astype(jnp.float32)
     centre = jnp.mean(values, axis=-1, keepdims=True)
     spread = jnp.mean(jnp.square(values - centre), axis=-1, keepdims=True)
-    columns = pl.ds(pl.multiple_of(feature_half * share, share), share)
-    own = tokens[:, columns].astype(jnp.float32)
-    scaled = (own - centre) * lax.rsqrt(spread + EPSILON) * gain[:, columns] + shift[:, columns]
+    scaled = (values - centre) * lax.rsqrt(spread + EPSILON) * gain[...] + shift[...]
     normed = scaled.astype(jnp.bfloat16)
     expert = CORES * iota((experts, rows), 0) + core
     named = jnp.zeros((experts, rows), jnp.float32)
@@ -123,26 +125,25 @@
     return lax.bitwise_xor(y, 1), 3 - y, lax.bitwise_xor(y, 2)
 
 
-def hidden_kernel(own, near, mine, swapped, same, cross, hidden, *, slots):
-    y, _ = position()
-    _, half = part(y)
-    rows, width = own.shape
+def hidden_kernel(arrived, mine, swapped, gate, gate_swapped, up, up_swapped, hidden, *, slots):
+    _, core = position()
+    rows, width = arrived.shape
     kept = rows // 2
     count = slots // 2
     i, j = iota((kept, rows), 0), iota((kept, rows), 1)
     source = (i // count) * slots + i % count
     total = None
-    for tokens, at in ((own, half), (near, 1 - half)):
-        values = tokens[...]
-        for q in range(2):
-            pick = jnp.where(j == source + q * count, 1.0, 0.0).astype(jnp.bfloat16)
-            x = dot_nn(pick, values).astype(jnp.bfloat16)
-            columns = pl.ds(pl.multiple_of((2 * at + q) * width, width), width)
-            w = jnp.concatenate(
-                [ref[m, :, columns] for m in range(2) for ref in (mine, swapped, same, cross)]
-            )
-            product = dot_nt(x, w)
-            total = product if total is None else total + product
+    values = arrived[...]
+    for q in range(2):
+        pick = jnp.where(j == source + q * count, 1.0, 0.0).astype(jnp.bfloat16)
+        x = dot_nn(pick, values).astype(jnp.bfloat16)
+        at = slice(q * width, (q + 1) * width)
+        w = jnp.concatenate(
+            [mine[0, :, at], swapped[0, :, at], gate[core, :, at], gate_swapped[:, at]]
+            + [mine[1, :, at], swapped[1, :, at], up[core, :, at], up_swapped[:, at]]
+        )
+        product = dot_nt(x, w)
+        total = product if total is None else total + product
     units = total.shape[1] // 2
     value = total[:, :units]
     result = value / (1.0 + jnp.exp(-value)) * total[:, units:]
@@ -210,29 +211,20 @@
     swap = [(i, i ^ 1) for i in range(tp_size)]
     near = [(i, i ^ 2) for i in range(tp_size)]
     same = [(i, 6 - i // 2 * 2 + i % 2) for i in range(tp_size)]
-    cross = [(i, 7 - i // 2 * 2 - i % 2) for i in range(tp_size)]
     across = [(i, i ^ 4) for i in range(tp_size)]
     anywhere = pl.BlockSpec(memory_space=pl.ANY)
 
     def ppermute(array, pairs):
         return lax.ppermute(array, "tp", pairs)
 
-    mine, giving = pl.pallas_call(
-        weights_kernel,
-        out_shape=(pltpu.VMEM((2, units, features), jnp.bfloat16),) * 2,
-        in_specs=[anywhere] * 2,
-        out_specs=(VMEM,) * 2,
-        scratch_shapes=[pltpu.SemaphoreType.DMA((4,))],
-        compiler_params=PARAMS,
-        name="split",
-    )(*off_chip(expert_gate.transpose(0, 2, 1), expert_up.transpose(0, 2, 1)))
-    w_same, w_cross = ppermute(mine, same), ppermute(giving, cross)
-    w_swapped = ppermute(giving, swap)
+    gate_t, up_t = off_chip(expert_gate.transpose(0, 2, 1), expert_up.transpose(0, 2, 1))
+    gate_both = ppermute(expert_gate.transpose(0, 2, 1), same)
+    up_both = ppermute(expert_up.transpose(0, 2, 1), same)
 
     packed, select_hi, select_lo = pl.pallas_call(
         functools.partial(pack_kernel, slots=slots),
         out_shape=(
-            pltpu.VMEM((rows, share), jnp.bfloat16),
+            pltpu.VMEM((rows, features // 2), jnp.bfloat16),
             pltpu.VMEM((rows, tok_rows), jnp.bfloat16),
             pltpu.VMEM((rows, tok_rows), jnp.bfloat16),
         ),
@@ -241,16 +233,40 @@
         compiler_params=PARAMS,
         name="pack",
     )(
-        tokens,
-        norm_gain.reshape(1, features),
-        norm_shift.reshape(1, features),
-        expert_ids.T,
-        gate_weights.T,
+        *off_chip(
+            tokens,
+            norm_gain.reshape(1, features),
+            norm_shift.reshape(1, features),
+            expert_ids.T,
+            gate_weights.T,
+        )
     )
     arrived = lax.all_to_all(
-        packed.reshape(ep_size, slots, share), "ep", split_axis=0, concat_axis=0, tiled=True
-    ).reshape(rows, share)
-    neighbour = ppermute(arrived, near)
+        packed.reshape(ep_size, slots, features // 2), "ep", split_axis=0, concat_axis=0, tiled=True
+    ).reshape(rows, features // 2)
+
+    mine, giving = pl.pallas_call(
+        ours_kernel,
+        out_shape=(pltpu.VMEM((2, units, features), jnp.bfloat16),) * 2,
+        in_specs=[anywhere] * 2,
+        out_specs=(VMEM,) * 2,
+        scratch_shapes=[pltpu.SemaphoreType.DMA((4,))],
+        compiler_params=PARAMS,
+        name="ours",
+    )(gate_t, up_t)
+    swapped = ppermute(giving, swap)
+
+    def passed_on(both):
+        picked = pl.pallas_call(
+            pick_kernel,
+            out_shape=pltpu.VMEM((units, features), jnp.bfloat16),
+            in_specs=[VMEM],
+            out_specs=VMEM,
+            compiler_params=PARAMS,
+        )(*on_chip(both))
+        return ppermute(picked, swap)
+
+    gate_swapped, up_swapped = passed_on(gate_both), passed_on(up_both)
 
     pieces = pl.pallas_call(
         pieces_kernel,
@@ -267,11 +283,11 @@
     hidden = pl.pallas_call(
         functools.partial(hidden_kernel, slots=slots),
         out_shape=pltpu.VMEM((rows // 2, 2 * CORES * units), jnp.bfloat16),
-        in_specs=[VMEM] * 6,
+        in_specs=[VMEM] * 7,
         out_specs=VMEM,
         compiler_params=PARAMS,
         name="hidden",
-    )(*on_chip(arrived, neighbour, mine, w_swapped, w_same, w_cross))
+    )(*on_chip(arrived, mine, swapped, gate_both, gate_swapped, up_both, up_swapped))
     hiddens = [hidden] + [ppermute(hidden, pairs) for pairs in (near, same, across)]
     d_giving = pl.pallas_call(
         give_kernel,

time: 97.1 us -> 89.4 us (0.921)
  waiting for transfers between devices: 31.9 us -> 21.4 us
  Pallas kernels: 6.11 us -> 8.23 us
  local copies, waits for them, and re-layouts: 3.04 us -> 1.66 us
  blocking collectives: 23.3 us -> 24.4 us
  starting transfers between devices: 31.7 us -> 32.7 us
    ppermute x11 -> x12, waiting for transfers between devices: 31 us -> 20.5 us  [ppermute(): return lax.ppermute(array, 'tp', pairs)]
    ppermute x11 -> x12, starting transfers between devices: 14.8 us -> 17.3 us  [ppermute(): return lax.ppermute(array, 'tp', pairs)]
    ppermute x1, starting transfers between devices: 5.08 us -> 3.51 us  [per_device(): mixed_out = kept + lax.ppermute(sent, 'tp', swap)]
    unnamed x10 -> x4, local copies, waits for them, and re-layouts: 3.04 us -> 1.66 us
    pallas_call x1, Pallas kernels: 1.24 us -> 2.45 us  [per_device(): pl.pallas_call(functools.partial(pack_kernel, slots=slots), out_shape=(pl...]
    all_to_all x1, blocking collectives: 23.3 us -> 24.4 us  [per_device(): lax.all_to_all(result.reshape(ep_size, slots, share), 'ep', split_axis=0,...]
  transfers between devices with their start and end apart: 13 -> 14, of which waited for: 6 -> 5; matrix products, arithmetic and copies ran while one was open for 0% -> 0% of each run, Pallas kernels for 4% -> 5%
where the time goes in v2:
time: 89.4 us; the launch traced here: 89.1 us
  starting transfers between devices  32.7 us (37%)
  blocking collectives  24.4 us (27%)
  waiting for transfers between devices  21.4 us (24%)
  Pallas kernels  8.23 us (9%)
  local copies, waits for them, and re-layouts  1.66 us (2%)
    all_to_all x1, blocking collectives, per_device(): lax.all_to_all(result.reshape(ep_size, slots, share), 'ep', split_axis=0,...  24.4 us
    ppermute x12, waiting for transfers between devices, ppermute(): return lax.ppermute(array, 'tp', pairs)  20.5 us
    ppermute x12, starting transfers between devices, ppermute(): return lax.ppermute(array, 'tp', pairs)  17.3 us
    all_to_all x1, starting transfers between devices, per_device(): lax.all_to_all(packed.reshape(ep_size, slots, features // 2), 'ep', split...  11.9 us
    ppermute x1, starting transfers between devices, per_device(): mixed_out = kept + lax.ppermute(sent, 'tp', swap)  3.51 us
    pallas_call x1, Pallas kernels, per_device(): pl.pallas_call(functools.partial(pack_kernel, slots=slots), out_shape=(pl...  2.45 us
  transfers between devices with their start and end apart: 14, of which 5 were waited for; matrix products, arithmetic and copies ran while one was open for 0% of the time, Pallas kernels for 5%

profile of v2, /device:TPU:1, one launch (start us, length us, event | category | flops | bytes accessed | tf_op | source)
XLA Modules:
  0.0 89.1 jit_solution(4117249875072816203)
XLA Ops:
  0.0 2.5 %pack.1 = (bf16[256,1024]{1,0:T(8,128)(2,1)}, bf16[256,64]{1,0:T(8,128)(2,1)S(1)}, bf16[256,64]{1,0:T(8,128)(2,1)S(1)}) custom-call(bf16[64,2048]{1,0:T(8,128)(2,1)} %tokens.1, f32[1,2048]{1,0:T(1,128)} %bitcast.13, f32[1,2048]{1,0:T(1,128)} %bitcast.14, s32[4,64]{1,0:T(4,128)} %bitcast.15, f32[4,64]{1,0:T(4,128)} %bitcast.16), custom_call_target="tpu_custom_call" | custom-call | tf_op jit(solution)/shard_map/pack/pallas_call | solution.py:224
  2.5 11.9 %all-to-all-start = ((bf16[32,8,1024]{2,1,0:T(8,128)(2,1)}), bf16[32,8,1024]{2,1,0:T(8,128)(2,1)S(1)}, u32[]{:S(2)}, u32[]{:S(2)}) async-start(bf16[32,8,1024]{2,1,0:T(8,128)(2,1)} %bitcast.4), calls=%async_computation | async-start | bytes 1048576 | tf_op jit(solution)/shard_map/all_to_all | solution.py:244
  14.3 2.8 %collective-permute-start.1 = (bf16[2,64,2048]{2,1,0:T(8,128)(2,1)}, bf16[2,64,2048]{2,1,0:T(8,128)(2,1)S(1)}, u32[]{:S(2)}, u32[]{:S(2)}) collective-permute-start(bf16[2,64,2048]{2,1,0:T(8,128)(2,1)} %bitcast.6.gate), channel_id=1, source_target_pairs={{0,6},{1,7},{2,4},{3,5},{4,2},{5,3},{6,0},{7,1},{8,14},{9,15},{10,... | collective-permute-start | bytes 1572872 | tf_op jit(solution)/shard_map/ppermute | solution.py:218
  17.1 0.1 collective-permute-start.3
  17.2 1.2 %ours.1 = (bf16[2,64,2048]{2,1,0:T(8,128)(2,1)S(1)}, bf16[2,64,2048]{2,1,0:T(8,128)(2,1)S(1)}) custom-call(bf16[2,64,2048]{2,1,0:T(8,128)(2,1)} %bitcast.6.gate, bf16[2,64,2048]{2,1,0:T(8,128)(2,1)} %bitcast.7.up), custom_call_target="tpu_custom_call" | custom-call | tf_op jit(solution)/shard_map/ours/pallas_call | solution.py:248
  18.5 1.4 %collective-permute-start = (bf16[2,64,2048]{2,1,0:T(8,128)(2,1)S(1)}, bf16[2,64,2048]{2,1,0:T(8,128)(2,1)S(1)}, u32[]{:S(2)}, u32[]{:S(2)}) collective-permute-start(bf16[2,64,2048]{2,1,0:T(8,128)(2,1)S(1)} %get-tuple-element.20), channel_id=1, source_target_pairs={{0,1},{1,0},{2,3},{3,2},{4,5},{5,4},{6,7},{7,6},{8,9},{9,8},{10,11... | collective-permute-start | bytes 1572872 | tf_op jit(solution)/shard_map/ppermute | solution.py:218
  19.9 1.1 %pieces.1 = (bf16[2,64,512]{2,1,0:T(8,128)(2,1)S(1)}, bf16[2,64,512]{2,1,0:T(8,128)(2,1)S(1)}, bf16[2,64,512]{2,1,0:T(8,128)(2,1)S(1)}, bf16[2,64,512]{2,1,0:T(8,128)(2,1)S(1)}) custom-call(bf16[2,64,2048]{2,1,0:T(8,128)(2,1)} %down.2), custom_call_target="tpu_custom_call" | custom-call | tf_op jit(solution)/shard_map/pieces/pallas_call | solution.py:271
  21.0 0.2 collective-permute-start.8
  21.2 2.7 %collective-permute-start.9 = (bf16[2,64,512]{2,1,0:T(8,128)(2,1)S(1)}, bf16[2,64,512]{2,1,0:T(8,128)(2,1)S(1)}, u32[]{:S(2)}, u32[]{:S(2)}) collective-permute-start(bf16[2,64,512]{2,1,0:T(8,128)(2,1)S(1)} %get-tuple-element.23), channel_id=1, source_target_pairs={{0,6},{1,7},{2,4},{3,5},{4,2},{5,3},{6,0},{7,1},{8,14},{9,15},{10,... | collective-permute-start | bytes 393224 | tf_op jit(solution)/shard_map/ppermute | solution.py:218
  24.0 4.5 %collective-permute-done.1.both.gate = bf16[2,64,2048]{2,1,0:T(8,128)(2,1)S(1)} collective-permute-done((bf16[2,64,2048]{2,1,0:T(8,128)(2,1)}, bf16[2,64,2048]{2,1,0:T(8,128)(2,1)S(1)}, u32[]{:S(2)}, u32[]{:S(2)}) %collective-permute-start.1) | collective-permute-done | bytes 524320 | tf_op jit(solution)/shard_map/ppermute | solution.py:218
  28.5 1.6 %collective-permute-start.10 = (bf16[2,64,512]{2,1,0:T(8,128)(2,1)S(1)}, bf16[2,64,512]{2,1,0:T(8,128)(2,1)S(1)}, u32[]{:S(2)}, u32[]{:S(2)}) collective-permute-start(bf16[2,64,512]{2,1,0:T(8,128)(2,1)S(1)} %get-tuple-element.24), channel_id=1, source_target_pairs={{0,4},{1,5},{2,6},{3,7},{4,0},{5,1},{6,2},{7,3},{8,12},{9,13},{10,... | collective-permute-start | bytes 393224 | tf_op jit(solution)/shard_map/ppermute | solution.py:218
  30.1 12.4 %collective-permute-done.3.both.up = bf16[2,64,2048]{2,1,0:T(8,128)(2,1)S(1)} collective-permute-done((bf16[2,64,2048]{2,1,0:T(8,128)(2,1)}, bf16[2,64,2048]{2,1,0:T(8,128)(2,1)S(1)}, u32[]{:S(2)}, u32[]{:S(2)}) %collective-permute-start.3) | collective-permute-done | bytes 524320 | tf_op jit(solution)/shard_map/ppermute | solution.py:218
  42.5 3.1 %collective-permute-start.2 = (bf16[64,2048]{1,0:T(8,128)(2,1)S(1)}, bf16[64,2048]{1,0:T(8,128)(2,1)S(1)}, u32[]{:S(2)}, u32[]{:S(2)}) collective-permute-start(bf16[64,2048]{1,0:T(8,128)(2,1)S(1)} %shard_map.82), channel_id=1, source_target_pairs={{0,1},{1,0},{2,3},{3,2},{4,5},{5,4},{6,7},{7,6},{8,9},{9,8},{10,11... | collective-permute-start | bytes 786440 | tf_op jit(solution)/shard_map/ppermute | solution.py:218
  45.6 0.0 collective-permute-done.8.first
  45.7 0.1 collective-permute-start.4
  45.8 0.0 collective-permute-done.9.second
  45.8 0.0 collective-permute-done.10.third
  45.8 0.7 give.1
  46.5 1.3 %collective-permute-start.11 = (bf16[4,64,512]{2,1,0:T(8,128)(2,1)}, bf16[4,64,512]{2,1,0:T(8,128)(2,1)}, u32[]{:S(2)}, u32[]{:S(2)}) collective-permute-start(bf16[4,64,512]{2,1,0:T(8,128)(2,1)} %give.1), channel_id=1, source_target_pairs={{0,1},{1,0},{2,3},{3,2},{4,5},{5,4},{6,7},{7,6},{8,9},{9,8},{10,11... | collective-permute-start | bytes 786440 | tf_op jit(solution)/shard_map/ppermute | solution.py:218
  47.8 0.0 collective-permute-done.swapped
  47.8 0.0 collective-permute-done.2.gate_swapped
  47.8 0.0 collective-permute-done.4.up_swapped
  47.8 0.0 copy-start
  47.8 0.7 copy-done
  48.5 0.0 all-to-all-done
  48.5 0.0 copy-start.1
  48.5 0.9 %copy-done.1 = bf16[64,2048]{1,0:T(8,128)(2,1)S(1)} copy-done((bf16[64,2048]{1,0:T(8,128)(2,1)S(1)}, bf16[64,2048]{1,0:T(8,128)(2,1)}, u32[]{:S(2)}) %copy-start.1) | copy-done | bytes 262168
  49.5 1.0 %hidden.1.h_own = bf16[128,256]{1,0:T(8,128)(2,1)S(1)} custom-call(bf16[256,1024]{1,0:T(8,128)(2,1)S(1)} %bitcast.10, bf16[2,64,2048]{2,1,0:T(8,128)(2,1)S(1)} %get-tuple-element.19.mine, bf16[2,64,2048]{2,1,0:T(8,128)(2,1)S(1)} %collective-permute-done.swapped, bf16[2,64,2048]{2,1,0:T(8,128)(2,1)S(1)} %collective-permute-done.1.both.gate, ...), custom_call_target="tpu_custom_call" | custom-call | tf_op jit(solution)/shard_map/hidden/pallas_call | solution.py:283
  50.5 0.1 collective-permute-start.5
  50.6 2.7 %collective-permute-start.6 = (bf16[128,256]{1,0:T(8,128)(2,1)S(1)}, bf16[128,256]{1,0:T(8,128)(2,1)S(1)}, u32[]{:S(2)}, u32[]{:S(2)}) collective-permute-start(bf16[128,256]{1,0:T(8,128)(2,1)S(1)} %hidden.1.h_own), channel_id=1, source_target_pairs={{0,6},{1,7},{2,4},{3,5},{4,2},{5,3},{6,0},{7,1},{8,14},{9,15},{10,... | collective-permute-start | bytes 196616 | tf_op jit(solution)/shard_map/ppermute | solution.py:218
  53.4 1.1 %collective-permute-start.7 = (bf16[128,256]{1,0:T(8,128)(2,1)S(1)}, bf16[128,256]{1,0:T(8,128)(2,1)S(1)}, u32[]{:S(2)}, u32[]{:S(2)}) collective-permute-start(bf16[128,256]{1,0:T(8,128)(2,1)S(1)} %hidden.1.h_own), channel_id=1, source_target_pairs={{0,4},{1,5},{2,6},{3,7},{4,0},{5,1},{6,2},{7,3},{8,12},{9,13},{10,... | collective-permute-start | bytes 196616 | tf_op jit(solution)/shard_map/ppermute | solution.py:218
  54.5 0.0 collective-permute-done.11.other
  54.5 0.0 collective-permute-done.5.h_first
  54.5 0.9 collective-permute-done.6.h_second
  55.4 2.6 %collective-permute-done.7.h_third = bf16[128,256]{1,0:T(8,128)(2,1)S(1)} collective-permute-done((bf16[128,256]{1,0:T(8,128)(2,1)S(1)}, bf16[128,256]{1,0:T(8,128)(2,1)S(1)}, u32[]{:S(2)}, u32[]{:S(2)}) %collective-permute-start.7) | collective-permute-done | bytes 65568 | tf_op jit(solution)/shard_map/ppermute | solution.py:218
  58.0 1.4 %down.3 = f32[256,512]{1,0:T(8,128)S(1)} custom-call(bf16[128,256]{1,0:T(8,128)(2,1)S(1)} %hidden.1.h_own, bf16[128,256]{1,0:T(8,128)(2,1)S(1)} %collective-permute-done.5.h_first, bf16[128,256]{1,0:T(8,128)(2,1)S(1)} %collective-permute-done.6.h_second, bf16[128,256]{1,0:T(8,128)(2,1)S(1)} %collective-permute-done.7.h_third, ...), custom_call_target="tpu_custom_call" | custom-call | tf_op jit(solution)/shard_map/down/pallas_call | solution.py:301
  59.4 24.4 %all_to_all.10 = f32[32,8,512]{2,1,0:T(8,128)S(1)} all-to-all(f32[32,8,512]{2,1,0:T(8,128)S(1)} %bitcast.11), channel_id=1, replica_groups=mesh['ep'=32,'tp'=8] {'ep'}, dimensions={0} | all-to-all | bytes 1048576 | tf_op jit(solution)/shard_map/all_to_all | solution.py:309
  83.8 0.3 combine.1
  84.1 3.5 %collective-permute-start.12 = (f32[64,256]{1,0:T(8,128)S(1)}, f32[64,256]{1,0:T(8,128)S(1)}, u32[]{:S(2)}, u32[]{:S(2)}) collective-permute-start(f32[64,256]{1,0:T(8,128)S(1)} %get-tuple-element.26), channel_id=1, source_target_pairs={{0,1},{1,0},{2,3},{3,2},{4,5},{5,4},{6,7},{7,6},{8,9},{9,8},{10,11... | collective-permute-start | bytes 196616 | tf_op jit(solution)/shard_map/ppermute | solution.py:321
  87.6 0.9 %collective-permute-done.12 = f32[64,256]{1,0:T(8,128)S(1)} collective-permute-done((f32[64,256]{1,0:T(8,128)S(1)}, f32[64,256]{1,0:T(8,128)S(1)}, u32[]{:S(2)}, u32[]{:S(2)}) %collective-permute-start.12) | collective-permute-done | bytes 65568 | tf_op jit(solution)/shard_map/ppermute | solution.py:321
  88.5 0.6 add_convert_fusion
  (2 shorter events, 0.0 us)
Async XLA Ops:
  2.5 46.1 %all-to-all-start = ((bf16[32,8,1024]{2,1,0:T(8,128)(2,1)}), bf16[32,8,1024]{2,1,0:T(8,128)(2,1)S(1)}, u32[]{:S(2)}, u32[]{:S(2)}) async-start(bf16[32,8,1024]{2,1,0:T(8,128)(2,1)} %bitcast.4), calls=%async_computation | async-start | bytes 1048576 | tf_op jit(solution)/shard_map/all_to_all | solution.py:244
  14.3 14.2 %collective-permute-start.1 = (bf16[2,64,2048]{2,1,0:T(8,128)(2,1)}, bf16[2,64,2048]{2,1,0:T(8,128)(2,1)S(1)}, u32[]{:S(2)}, u32[]{:S(2)}) collective-permute-start(bf16[2,64,2048]{2,1,0:T(8,128)(2,1)} %bitcast.6.gate), channel_id=1, source_target_pairs={{0,6},{1,7},{2,4},{3,5},{4,2},{5,3},{6,0},{7,1},{8,14},{9,15},{10,... | collective-permute-start | bytes 1572872 | tf_op jit(solution)/shard_map/ppermute | solution.py:218
  17.1 25.4 %collective-permute-start.3 = (bf16[2,64,2048]{2,1,0:T(8,128)(2,1)}, bf16[2,64,2048]{2,1,0:T(8,128)(2,1)S(1)}, u32[]{:S(2)}, u32[]{:S(2)}) collective-permute-start(bf16[2,64,2048]{2,1,0:T(8,128)(2,1)} %bitcast.7.up), channel_id=1, source_target_pairs={{0,6},{1,7},{2,4},{3,5},{4,2},{5,3},{6,0},{7,1},{8,14},{9,15},{10,... | collective-permute-start | bytes 1572872 | tf_op jit(solution)/shard_map/ppermute | solution.py:218
  18.5 29.3 %collective-permute-start = (bf16[2,64,2048]{2,1,0:T(8,128)(2,1)S(1)}, bf16[2,64,2048]{2,1,0:T(8,128)(2,1)S(1)}, u32[]{:S(2)}, u32[]{:S(2)}) collective-permute-start(bf16[2,64,2048]{2,1,0:T(8,128)(2,1)S(1)} %get-tuple-element.20), channel_id=1, source_target_pairs={{0,1},{1,0},{2,3},{3,2},{4,5},{5,4},{6,7},{7,6},{8,9},{9,8},{10,11... | collective-permute-start | bytes 1572872 | tf_op jit(solution)/shard_map/ppermute | solution.py:218
  21.0 24.6 %collective-permute-start.8 = (bf16[2,64,512]{2,1,0:T(8,128)(2,1)S(1)}, bf16[2,64,512]{2,1,0:T(8,128)(2,1)S(1)}, u32[]{:S(2)}, u32[]{:S(2)}) collective-permute-start(bf16[2,64,512]{2,1,0:T(8,128)(2,1)S(1)} %get-tuple-element.22), channel_id=1, source_target_pairs={{0,2},{1,3},{2,0},{3,1},{4,6},{5,7},{6,4},{7,5},{8,10},{9,11},{10,... | collective-permute-start | bytes 393224 | tf_op jit(solution)/shard_map/ppermute | solution.py:218
  21.2 24.5 %collective-permute-start.9 = (bf16[2,64,512]{2,1,0:T(8,128)(2,1)S(1)}, bf16[2,64,512]{2,1,0:T(8,128)(2,1)S(1)}, u32[]{:S(2)}, u32[]{:S(2)}) collective-permute-start(bf16[2,64,512]{2,1,0:T(8,128)(2,1)S(1)} %get-tuple-element.23), channel_id=1, source_target_pairs={{0,6},{1,7},{2,4},{3,5},{4,2},{5,3},{6,0},{7,1},{8,14},{9,15},{10,... | collective-permute-start | bytes 393224 | tf_op jit(solution)/shard_map/ppermute | solution.py:218
  28.5 17.3 %collective-permute-start.10 = (bf16[2,64,512]{2,1,0:T(8,128)(2,1)S(1)}, bf16[2,64,512]{2,1,0:T(8,128)(2,1)S(1)}, u32[]{:S(2)}, u32[]{:S(2)}) collective-permute-start(bf16[2,64,512]{2,1,0:T(8,128)(2,1)S(1)} %get-tuple-element.24), channel_id=1, source_target_pairs={{0,4},{1,5},{2,6},{3,7},{4,0},{5,1},{6,2},{7,3},{8,12},{9,13},{10,... | collective-permute-start | bytes 393224 | tf_op jit(solution)/shard_map/ppermute | solution.py:218
  42.5 5.3 %collective-permute-start.2 = (bf16[64,2048]{1,0:T(8,128)(2,1)S(1)}, bf16[64,2048]{1,0:T(8,128)(2,1)S(1)}, u32[]{:S(2)}, u32[]{:S(2)}) collective-permute-start(bf16[64,2048]{1,0:T(8,128)(2,1)S(1)} %shard_map.82), channel_id=1, source_target_pairs={{0,1},{1,0},{2,3},{3,2},{4,5},{5,4},{6,7},{7,6},{8,9},{9,8},{10,11... | collective-permute-start | bytes 786440 | tf_op jit(solution)/shard_map/ppermute | solution.py:218
  45.7 2.2 %collective-permute-start.4 = (bf16[64,2048]{1,0:T(8,128)(2,1)S(1)}, bf16[64,2048]{1,0:T(8,128)(2,1)S(1)}, u32[]{:S(2)}, u32[]{:S(2)}) collective-permute-start(bf16[64,2048]{1,0:T(8,128)(2,1)S(1)} %shard_map.83), channel_id=1, source_target_pairs={{0,1},{1,0},{2,3},{3,2},{4,5},{5,4},{6,7},{7,6},{8,9},{9,8},{10,11... | collective-permute-start | bytes 786440 | tf_op jit(solution)/shard_map/ppermute | solution.py:218
  46.5 8.0 %collective-permute-start.11 = (bf16[4,64,512]{2,1,0:T(8,128)(2,1)}, bf16[4,64,512]{2,1,0:T(8,128)(2,1)}, u32[]{:S(2)}, u32[]{:S(2)}) collective-permute-start(bf16[4,64,512]{2,1,0:T(8,128)(2,1)} %give.1), channel_id=1, source_target_pairs={{0,1},{1,0},{2,3},{3,2},{4,5},{5,4},{6,7},{7,6},{8,9},{9,8},{10,11... | collective-permute-start | bytes 786440 | tf_op jit(solution)/shard_map/ppermute | solution.py:218
  47.8 0.7 copy-start
  48.5 1.0 %copy-start.1 = (bf16[64,2048]{1,0:T(8,128)(2,1)S(1)}, bf16[64,2048]{1,0:T(8,128)(2,1)}, u32[]{:S(2)}) copy-start(bf16[64,2048]{1,0:T(8,128)(2,1)} %copy-done) | copy-start | bytes 786436
  50.5 4.0 %collective-permute-start.5 = (bf16[128,256]{1,0:T(8,128)(2,1)S(1)}, bf16[128,256]{1,0:T(8,128)(2,1)S(1)}, u32[]{:S(2)}, u32[]{:S(2)}) collective-permute-start(bf16[128,256]{1,0:T(8,128)(2,1)S(1)} %hidden.1.h_own), channel_id=1, source_target_pairs={{0,2},{1,3},{2,0},{3,1},{4,6},{5,7},{6,4},{7,5},{8,10},{9,11},{10,... | collective-permute-start | bytes 196616 | tf_op jit(solution)/shard_map/ppermute | solution.py:218
  50.6 4.7 %collective-permute-start.6 = (bf16[128,256]{1,0:T(8,128)(2,1)S(1)}, bf16[128,256]{1,0:T(8,128)(2,1)S(1)}, u32[]{:S(2)}, u32[]{:S(2)}) collective-permute-start(bf16[128,256]{1,0:T(8,128)(2,1)S(1)} %hidden.1.h_own), channel_id=1, source_target_pairs={{0,6},{1,7},{2,4},{3,5},{4,2},{5,3},{6,0},{7,1},{8,14},{9,15},{10,... | collective-permute-start | bytes 196616 | tf_op jit(solution)/shard_map/ppermute | solution.py:218
  53.4 4.6 %collective-permute-start.7 = (bf16[128,256]{1,0:T(8,128)(2,1)S(1)}, bf16[128,256]{1,0:T(8,128)(2,1)S(1)}, u32[]{:S(2)}, u32[]{:S(2)}) collective-permute-start(bf16[128,256]{1,0:T(8,128)(2,1)S(1)} %hidden.1.h_own), channel_id=1, source_target_pairs={{0,4},{1,5},{2,6},{3,7},{4,0},{5,1},{6,2},{7,3},{8,12},{9,13},{10,... | collective-permute-start | bytes 196616 | tf_op jit(solution)/shard_map/ppermute | solution.py:218
  84.1 4.4 %collective-permute-start.12 = (f32[64,256]{1,0:T(8,128)S(1)}, f32[64,256]{1,0:T(8,128)S(1)}, u32[]{:S(2)}, u32[]{:S(2)}) collective-permute-start(f32[64,256]{1,0:T(8,128)S(1)} %get-tuple-element.26), channel_id=1, source_target_pairs={{0,1},{1,0},{2,3},{3,2},{4,5},{5,4},{6,7},{7,6},{8,9},{9,8},{10,11... | collective-permute-start | bytes 196616 | tf_op jit(solution)/shard_map/ppermute | solution.py:321

commit v3 on v2

--- a/solution.py
+++ b/solution.py
@@ -57,11 +57,10 @@
     return copies
 
 
-def ours_kernel(gate, up, mine, giving, sems):
-    _, core = position()
-    pairs = [(ref.at[core], mine.at[i]) for i, ref in enumerate((gate, up))]
-    pairs += [(ref.at[1 - core], giving.at[i]) for i, ref in enumerate((gate, up))]
-    for copy in copy_all(pairs, sems):
+def expert_kernel(gate, up, out, sems, *, own):
+    _, core = position()
+    which = core if own else 1 - core
+    for copy in copy_all([(ref.at[which], out.at[i]) for i, ref in enumerate((gate, up))], sems):
         copy.wait()
 
 
@@ -110,13 +109,15 @@
     select_lo[...] = (factor - high.astype(jnp.float32)).astype(jnp.bfloat16)
 
 
-def pieces_kernel(down, own, first, second, third, sems):
+def pieces_kernel(down, kept, sent, sems):
     y, _ = position()
-    share = own.shape[-1]
+    share = kept.shape[-1]
+    near, same, across = others(y)
     pairs = []
-    for chip, piece in zip((y, *others(y)), (own, first, second, third)):
-        columns = pl.ds(pl.multiple_of(chip * share, share), share)
-        pairs.append((down.at[:, :, columns], piece))
+    for chips, out in (((y, same), kept), ((near, across), sent)):
+        for i, chip in enumerate(chips):
+            columns = pl.ds(pl.multiple_of(chip * share, share), share)
+            pairs.append((down.at[:, :, columns], out.at[:, i]))
     for copy in copy_all(pairs, sems):
         copy.wait()
 
@@ -150,14 +151,22 @@
     hidden[...] = result.astype(jnp.bfloat16)
 
 
-def give_kernel(own, first, second, third, giving):
-    _, core = position()
-    for i, ref in enumerate((own, first, second, third)):
-        giving[i] = ref[1 - core]
-
-
-def down_kernel(h_own, h_first, h_second, h_third, own, first, second, third, other, out, *, slots):
-    y, core = position()
+def give_kernel(kept, near, giving):
+    _, core = position()
+    giving[0] = kept[1 - core]
+    giving[1] = near[1 - core]
+
+
+def join_kernel(kept, near, other, mine, sent):
+    _, core = position()
+    units = kept.shape[2]
+    for i, out in enumerate((mine, sent)):
+        for j, value in enumerate((kept[core, i], other[0, i], near[core, i], other[1, i])):
+            out[j * units : (j + 1) * units, :] = value
+
+
+def down_kernel(h_own, h_first, h_second, h_third, mine, same, out, *, slots):
+    y, _ = position()
     row_half, _ = part(y)
     rows = out.shape[0]
     kept = h_own.shape[0]
@@ -168,16 +177,13 @@
     half = jnp.where(j < kept, row_half, 1 - row_half)
     place = (i // count) * slots + half * count + i % count
     spread = jnp.where(r == place, 1.0, 0.0).astype(jnp.bfloat16)
-    total = None
-    for a, b, w0, o0, w1, o1 in (
-        (h_own, h_second, own, 0, second, 2),
-        (h_first, h_third, first, 1, third, 3),
-    ):
+    picked = []
+    for a, b in ((h_own, h_second), (h_first, h_third)):
         across = jnp.concatenate([b[:, units:], b[:, :units]], axis=1)
-        h = dot_nn(spread, jnp.concatenate([a[...], across])).astype(jnp.bfloat16)
-        w = jnp.concatenate([w0[core], other[o0], w1[core], other[o1]])
-        product = dot_nn(h, w)
-        total = product if total is None else total + product
+        picked.append(dot_nn(spread, jnp.concatenate([a[...], across])).astype(jnp.bfloat16))
+    (h_y, h_same), (h_near, h_across) = ((p[:, :units], p[:, units:]) for p in picked)
+    total = dot_nn(jnp.concatenate([h_y, h_near], axis=1), mine[...])
+    total = total + dot_nn(jnp.concatenate([h_same, h_across], axis=1), same[...])
     out[...] = total
 
 
@@ -245,15 +251,17 @@
         packed.reshape(ep_size, slots, features // 2), "ep", split_axis=0, concat_axis=0, tiled=True
     ).reshape(rows, features // 2)
 
-    mine, giving = pl.pallas_call(
-        ours_kernel,
-        out_shape=(pltpu.VMEM((2, units, features), jnp.bfloat16),) * 2,
-        in_specs=[anywhere] * 2,
-        out_specs=(VMEM,) * 2,
-        scratch_shapes=[pltpu.SemaphoreType.DMA((4,))],
-        compiler_params=PARAMS,
-        name="ours",
-    )(gate_t, up_t)
+    def expert_weights(own):
+        return pl.pallas_call(
+            functools.partial(expert_kernel, own=own),
+            out_shape=pltpu.VMEM((2, units, features), jnp.bfloat16),
+            in_specs=[anywhere] * 2,
+            out_specs=VMEM,
+            scratch_shapes=[pltpu.SemaphoreType.DMA((2,))],
+            compiler_params=PARAMS,
+        )(gate_t, up_t)
+
+    giving, mine = expert_weights(False), expert_weights(True)
     swapped = ppermute(giving, swap)
 
     def passed_on(both):
@@ -268,17 +276,36 @@
 
     gate_swapped, up_swapped = passed_on(gate_both), passed_on(up_both)
 
-    pieces = pl.pallas_call(
+    halves = pltpu.VMEM((2, 2, units, share), jnp.bfloat16)
+    whole = pltpu.VMEM((4 * units, share), jnp.bfloat16)
+    d_kept, d_sent = pl.pallas_call(
         pieces_kernel,
-        out_shape=(pltpu.VMEM((2, units, share), jnp.bfloat16),) * chips,
+        out_shape=(halves, halves),
         in_specs=[anywhere],
-        out_specs=(VMEM,) * chips,
-        scratch_shapes=[pltpu.SemaphoreType.DMA((chips,))],
+        out_specs=(VMEM, VMEM),
+        scratch_shapes=[pltpu.SemaphoreType.DMA((4,))],
         compiler_params=PARAMS,
         name="pieces",
     )(*off_chip(expert_down))
-    downs = [ppermute(p, pairs) for p, pairs in zip(pieces[1:], (near, same, across))]
-    downs = on_chip(pieces[0], *downs)
+    d_near = ppermute(d_sent, near)
+    d_giving = pl.pallas_call(
+        give_kernel,
+        out_shape=halves,
+        in_specs=[VMEM] * 2,
+        out_specs=VMEM,
+        compiler_params=PARAMS,
+        name="give",
+    )(*on_chip(d_kept, d_near))
+    d_other = ppermute(d_giving, swap)
+    d_mine, d_passing = pl.pallas_call(
+        join_kernel,
+        out_shape=(whole, whole),
+        in_specs=[VMEM] * 3,
+        out_specs=(VMEM, VMEM),
+        compiler_params=PARAMS,
+        name="join",
+    )(*on_chip(d_kept, d_near, d_other))
+    d_same = ppermute(d_passing, same)
 
     hidden = pl.pallas_call(
         functools.partial(hidden_kernel, slots=slots),
@@ -289,23 +316,14 @@
         name="hidden",
     )(*on_chip(arrived, mine, swapped, gate_both, gate_swapped, up_both, up_swapped))
     hiddens = [hidden] + [ppermute(hidden, pairs) for pairs in (near, same, across)]
-    d_giving = pl.pallas_call(
-        give_kernel,
-        out_shape=pltpu.VMEM((chips, units, share), jnp.bfloat16),
-        in_specs=[VMEM] * chips,
-        out_specs=VMEM,
-        compiler_params=PARAMS,
-        name="give",
-    )(*downs)
-    d_other = ppermute(d_giving, swap)
     result = pl.pallas_call(
         functools.partial(down_kernel, slots=slots),
         out_shape=pltpu.VMEM((rows, share), jnp.float32),
-        in_specs=[VMEM] * (2 * chips + 1),
+        in_specs=[VMEM] * (chips + 2),
         out_specs=VMEM,
         compiler_params=PARAMS,
         name="down",
-    )(*on_chip(*hiddens), *downs, *on_chip(d_other))
+    )(*on_chip(*hiddens, d_mine, d_same))
     returned = lax.all_to_all(
         result.reshape(ep_size, slots, share), "ep", split_axis=0, concat_axis=0, tiled=True
     ).reshape(rows, share)

time: 89.4 us -> 84.8 us (0.949)
  waiting for transfers between devices: 21.4 us -> 16.5 us
  starting transfers between devices: 32.7 us -> 33.9 us
  blocking collectives: 24.4 us -> 23.4 us
    ppermute x12 -> x11, waiting for transfers between devices: 20.5 us -> 15.6 us  [ppermute(): return lax.ppermute(array, 'tp', pairs)]
    all_to_all x1, blocking collectives: 24.4 us -> 23.4 us  [per_device(): lax.all_to_all(result.reshape(ep_size, slots, share), 'ep', split_axis=0,...]
    pallas_call x1, Pallas kernels: 1.37 us -> 0.43 us  [per_device(): pl.pallas_call(functools.partial(down_kernel, slots=slots), out_shape=plt...]
    pallas_call x3 -> x5, Pallas kernels: 3.08 us -> 3.99 us  [the longest x2 2.1 us: expert_weights(): pl.pallas_call(functools.partial(expert_kernel, own=own), out_shape=pltpu...]
    ppermute x12 -> x11, starting transfers between devices: 17.3 us -> 18.1 us  [ppermute(): return lax.ppermute(array, 'tp', pairs)]
  transfers between devices with their start and end apart: 14 -> 13, of which waited for: 5 -> 5; matrix products, arithmetic and copies ran while one was open for 0% -> 0% of each run, Pallas kernels for 5% -> 6%
where the time goes in v3:
time: 84.8 us; the launch traced here: 84.5 us
  starting transfers between devices  33.9 us (40%)
  blocking collectives  23.4 us (28%)
  waiting for transfers between devices  16.5 us (19%)
  Pallas kernels  8.21 us (10%)
  local copies, waits for them, and re-layouts  1.64 us (2%)
    all_to_all x1, blocking collectives, per_device(): lax.all_to_all(result.reshape(ep_size, slots, share), 'ep', split_axis=0,...  23.4 us
    ppermute x11, starting transfers between devices, ppermute(): return lax.ppermute(array, 'tp', pairs)  18.1 us
    ppermute x11, waiting for transfers between devices, ppermute(): return lax.ppermute(array, 'tp', pairs)  15.6 us
    all_to_all x1, starting transfers between devices, per_device(): lax.all_to_all(packed.reshape(ep_size, slots, features // 2), 'ep', split...  12 us
    ppermute x1, starting transfers between devices, per_device(): mixed_out = kept + lax.ppermute(sent, 'tp', swap)  3.8 us
    pallas_call x1, Pallas kernels, per_device(): pl.pallas_call(functools.partial(pack_kernel, slots=slots), out_shape=(pl...  2.45 us
    pallas_call x2, Pallas kernels, expert_weights(): pl.pallas_call(functools.partial(expert_kernel, own=own), out_shape=pltpu...  2.1 us
  transfers between devices with their start and end apart: 13, of which 5 were waited for; matrix products, arithmetic and copies ran while one was open for 0% of the time, Pallas kernels for 6%

profile of v3, /device:TPU:1, one launch (start us, length us, event | category | flops | bytes accessed | tf_op | source)
XLA Modules:
  0.0 84.5 jit_solution(14752827672835216398)
XLA Ops:
  0.0 2.5 %pack.1 = (bf16[256,1024]{1,0:T(8,128)(2,1)}, bf16[256,64]{1,0:T(8,128)(2,1)S(1)}, bf16[256,64]{1,0:T(8,128)(2,1)S(1)}) custom-call(bf16[64,2048]{1,0:T(8,128)(2,1)} %tokens.1, f32[1,2048]{1,0:T(1,128)} %bitcast.16, f32[1,2048]{1,0:T(1,128)} %bitcast.17, s32[4,64]{1,0:T(4,128)} %bitcast.18, f32[4,64]{1,0:T(4,128)} %bitcast.19), custom_call_target="tpu_custom_call" | custom-call | tf_op jit(solution)/shard_map/pack/pallas_call | solution.py:230
  2.5 0.0 copy-start.2
  2.5 12.0 %all-to-all-start = ((bf16[32,8,1024]{2,1,0:T(8,128)(2,1)}), bf16[32,8,1024]{2,1,0:T(8,128)(2,1)S(1)}, u32[]{:S(2)}, u32[]{:S(2)}) async-start(bf16[32,8,1024]{2,1,0:T(8,128)(2,1)} %bitcast.4), calls=%async_computation | async-start | bytes 1048576 | tf_op jit(solution)/shard_map/all_to_all | solution.py:250
  14.4 0.0 copy-done.2
  14.5 2.8 %collective-permute-start.1 = (bf16[2,64,2048]{2,1,0:T(8,128)(2,1)S(1)}, bf16[2,64,2048]{2,1,0:T(8,128)(2,1)S(1)}, u32[]{:S(2)}, u32[]{:S(2)}) collective-permute-start(bf16[2,64,2048]{2,1,0:T(8,128)(2,1)S(1)} %bitcast.15), channel_id=1, source_target_pairs={{0,6},{1,7},{2,4},{3,5},{4,2},{5,3},{6,0},{7,1},{8,14},{9,15},{10,... | collective-permute-start | bytes 1572872 | tf_op jit(solution)/shard_map/ppermute | solution.py:224
  17.3 0.1 collective-permute-start.3
  17.4 1.1 %pieces.1 = (bf16[2,2,64,512]{3,2,1,0:T(8,128)(2,1)S(1)}, bf16[2,2,64,512]{3,2,1,0:T(8,128)(2,1)S(1)}) custom-call(bf16[2,64,2048]{2,1,0:T(8,128)(2,1)} %down.2), custom_call_target="tpu_custom_call" | custom-call | tf_op jit(solution)/shard_map/pieces/pallas_call | solution.py:281
  18.5 0.1 collective-permute-start.8
  18.6 1.1 %shard_map.83 = bf16[2,64,2048]{2,1,0:T(8,128)(2,1)S(1)} custom-call(bf16[2,64,2048]{2,1,0:T(8,128)(2,1)} %bitcast.13, bf16[2,64,2048]{2,1,0:T(8,128)(2,1)} %bitcast.7.up), custom_call_target="tpu_custom_call" | custom-call | tf_op jit(solution)/shard_map/pallas_call | solution.py:255
  19.7 1.8 %collective-permute-start = (bf16[2,64,2048]{2,1,0:T(8,128)(2,1)S(1)}, bf16[2,64,2048]{2,1,0:T(8,128)(2,1)S(1)}, u32[]{:S(2)}, u32[]{:S(2)}) collective-permute-start(bf16[2,64,2048]{2,1,0:T(8,128)(2,1)S(1)} %shard_map.83), channel_id=1, source_target_pairs={{0,1},{1,0},{2,3},{3,2},{4,5},{5,4},{6,7},{7,6},{8,9},{9,8},{10,11... | collective-permute-start | bytes 1572872 | tf_op jit(solution)/shard_map/ppermute | solution.py:224
  21.5 3.6 %collective-permute-done.8.near = bf16[2,2,64,512]{3,2,1,0:T(8,128)(2,1)S(1)} collective-permute-done((bf16[2,2,64,512]{3,2,1,0:T(8,128)(2,1)S(1)}, bf16[2,2,64,512]{3,2,1,0:T(8,128)(2,1)S(1)}, u32[]{:S(2)}, u32[]{:S(2)}) %collective-permute-start.8) | collective-permute-done | bytes 262176 | tf_op jit(solution)/shard_map/ppermute | solution.py:224
  25.1 2.3 %collective-permute-start.9 = (bf16[2,2,64,512]{3,2,1,0:T(8,128)(2,1)S(1)}, bf16[2,2,64,512]{3,2,1,0:T(8,128)(2,1)S(1)}, u32[]{:S(2)}, u32[]{:S(2)}) collective-permute-start(bf16[2,2,64,512]{3,2,1,0:T(8,128)(2,1)S(1)} %give.1), channel_id=1, source_target_pairs={{0,1},{1,0},{2,3},{3,2},{4,5},{5,4},{6,7},{7,6},{8,9},{9,8},{10,11... | collective-permute-start | bytes 786440 | tf_op jit(solution)/shard_map/ppermute | solution.py:224
  27.4 1.0 %collective-permute-done.1.both.gate = bf16[2,64,2048]{2,1,0:T(8,128)(2,1)S(1)} collective-permute-done((bf16[2,64,2048]{2,1,0:T(8,128)(2,1)S(1)}, bf16[2,64,2048]{2,1,0:T(8,128)(2,1)S(1)}, u32[]{:S(2)}, u32[]{:S(2)}) %collective-permute-start.1) | collective-permute-done | bytes 524320 | tf_op jit(solution)/shard_map/ppermute | solution.py:224
  28.4 3.2 %collective-permute-start.2 = (bf16[64,2048]{1,0:T(8,128)(2,1)S(1)}, bf16[64,2048]{1,0:T(8,128)(2,1)S(1)}, u32[]{:S(2)}, u32[]{:S(2)}) collective-permute-start(bf16[64,2048]{1,0:T(8,128)(2,1)S(1)} %shard_map.84), channel_id=1, source_target_pairs={{0,1},{1,0},{2,3},{3,2},{4,5},{5,4},{6,7},{7,6},{8,9},{9,8},{10,11... | collective-permute-start | bytes 786440 | tf_op jit(solution)/shard_map/ppermute | solution.py:224
  31.6 8.0 %collective-permute-done.3.both.up = bf16[2,64,2048]{2,1,0:T(8,128)(2,1)S(1)} collective-permute-done((bf16[2,64,2048]{2,1,0:T(8,128)(2,1)}, bf16[2,64,2048]{2,1,0:T(8,128)(2,1)S(1)}, u32[]{:S(2)}, u32[]{:S(2)}) %collective-permute-start.3) | collective-permute-done | bytes 524320 | tf_op jit(solution)/shard_map/ppermute | solution.py:224
  39.7 1.8 %collective-permute-start.4 = (bf16[64,2048]{1,0:T(8,128)(2,1)S(1)}, bf16[64,2048]{1,0:T(8,128)(2,1)S(1)}, u32[]{:S(2)}, u32[]{:S(2)}) collective-permute-start(bf16[64,2048]{1,0:T(8,128)(2,1)S(1)} %shard_map.85), channel_id=1, source_target_pairs={{0,1},{1,0},{2,3},{3,2},{4,5},{5,4},{6,7},{7,6},{8,9},{9,8},{10,11... | collective-permute-start | bytes 786440 | tf_op jit(solution)/shard_map/ppermute | solution.py:224
  41.5 0.0 collective-permute-done.9.other
  41.5 0.7 join.1
  42.2 2.7 %collective-permute-start.10 = (bf16[256,512]{1,0:T(8,128)(2,1)}, bf16[256,512]{1,0:T(8,128)(2,1)S(1)}, u32[]{:S(2)}, u32[]{:S(2)}) collective-permute-start(bf16[256,512]{1,0:T(8,128)(2,1)} %get-tuple-element.20), channel_id=1, source_target_pairs={{0,6},{1,7},{2,4},{3,5},{4,2},{5,3},{6,0},{7,1},{8,14},{9,15},{10,... | collective-permute-start | bytes 786440 | tf_op jit(solution)/shard_map/ppermute | solution.py:224
  44.9 1.0 %shard_map.82.mine = bf16[2,64,2048]{2,1,0:T(8,128)(2,1)S(1)} custom-call(bf16[2,64,2048]{2,1,0:T(8,128)(2,1)} %bitcast.14, bf16[2,64,2048]{2,1,0:T(8,128)(2,1)} %bitcast.7.up), custom_call_target="tpu_custom_call" | custom-call | tf_op jit(solution)/shard_map/pallas_call | solution.py:255
  46.0 0.0 collective-permute-done.swapped
  46.0 0.0 collective-permute-done.2.gate_swapped
  46.0 0.0 collective-permute-done.4.up_swapped
  46.0 0.0 copy-start
  46.0 0.7 copy-done
  46.7 0.0 all-to-all-done
  46.7 0.0 copy-start.1
  46.7 0.9 %copy-done.1 = bf16[64,2048]{1,0:T(8,128)(2,1)S(1)} copy-done((bf16[64,2048]{1,0:T(8,128)(2,1)S(1)}, bf16[64,2048]{1,0:T(8,128)(2,1)}, u32[]{:S(2)}) %copy-start.1) | copy-done | bytes 262168
  47.7 1.0 %hidden.1.h_own = bf16[128,256]{1,0:T(8,128)(2,1)S(1)} custom-call(bf16[256,1024]{1,0:T(8,128)(2,1)S(1)} %bitcast.10, bf16[2,64,2048]{2,1,0:T(8,128)(2,1)S(1)} %shard_map.82.mine, bf16[2,64,2048]{2,1,0:T(8,128)(2,1)S(1)} %collective-permute-done.swapped, bf16[2,64,2048]{2,1,0:T(8,128)(2,1)S(1)} %collective-permute-done.1.both.gate, ...), custom_call_target="tpu_custom_call" | custom-call | tf_op jit(solution)/shard_map/hidden/pallas_call | solution.py:310
  48.7 0.1 collective-permute-start.5
  48.8 0.1 collective-permute-start.6
  48.9 3.1 %collective-permute-start.7 = (bf16[128,256]{1,0:T(8,128)(2,1)S(1)}, bf16[128,256]{1,0:T(8,128)(2,1)S(1)}, u32[]{:S(2)}, u32[]{:S(2)}) collective-permute-start(bf16[128,256]{1,0:T(8,128)(2,1)S(1)} %hidden.1.h_own), channel_id=1, source_target_pairs={{0,4},{1,5},{2,6},{3,7},{4,0},{5,1},{6,2},{7,3},{8,12},{9,13},{10,... | collective-permute-start | bytes 196616 | tf_op jit(solution)/shard_map/ppermute | solution.py:224
  52.0 0.0 collective-permute-done.10.same
  52.0 0.0 collective-permute-done.5.h_first
  52.0 3.0 %collective-permute-done.6.h_second = bf16[128,256]{1,0:T(8,128)(2,1)S(1)} collective-permute-done((bf16[128,256]{1,0:T(8,128)(2,1)S(1)}, bf16[128,256]{1,0:T(8,128)(2,1)S(1)}, u32[]{:S(2)}, u32[]{:S(2)}) %collective-permute-start.6) | collective-permute-done | bytes 65568 | tf_op jit(solution)/shard_map/ppermute | solution.py:224
  55.0 0.0 collective-permute-done.7.h_third
  55.0 0.4 down.3
  55.5 23.4 %all_to_all.10 = f32[32,8,512]{2,1,0:T(8,128)S(1)} all-to-all(f32[32,8,512]{2,1,0:T(8,128)S(1)} %bitcast.12), channel_id=1, replica_groups=mesh['ep'=32,'tp'=8] {'ep'}, dimensions={0} | all-to-all | bytes 1048576 | tf_op jit(solution)/shard_map/all_to_all | solution.py:327
  78.9 0.3 combine.1
  79.1 3.8 %collective-permute-start.11 = (f32[64,256]{1,0:T(8,128)S(1)}, f32[64,256]{1,0:T(8,128)S(1)}, u32[]{:S(2)}, u32[]{:S(2)}) collective-permute-start(f32[64,256]{1,0:T(8,128)S(1)} %get-tuple-element.22), channel_id=1, source_target_pairs={{0,1},{1,0},{2,3},{3,2},{4,5},{5,4},{6,7},{7,6},{8,9},{9,8},{10,11... | collective-permute-start | bytes 196616 | tf_op jit(solution)/shard_map/ppermute | solution.py:339
  82.9 0.9 %collective-permute-done.11 = f32[64,256]{1,0:T(8,128)S(1)} collective-permute-done((f32[64,256]{1,0:T(8,128)S(1)}, f32[64,256]{1,0:T(8,128)S(1)}, u32[]{:S(2)}, u32[]{:S(2)}) %collective-permute-start.11) | collective-permute-done | bytes 65568 | tf_op jit(solution)/shard_map/ppermute | solution.py:339
  83.8 0.6 add_convert_fusion
  (3 shorter events, 0.1 us)
Async XLA Ops:
  2.5 12.0 %copy-start.2 = (bf16[2,2048,64]{1,2,0:T(8,128)(2,1)S(1)}, bf16[2,2048,64]{1,2,0:T(8,128)(2,1)}, u32[]{:S(2)}) copy-start(bf16[2,2048,64]{1,2,0:T(8,128)(2,1)} %param.13) | copy-start | bytes 1572868
  2.5 44.2 %all-to-all-start = ((bf16[32,8,1024]{2,1,0:T(8,128)(2,1)}), bf16[32,8,1024]{2,1,0:T(8,128)(2,1)S(1)}, u32[]{:S(2)}, u32[]{:S(2)}) async-start(bf16[32,8,1024]{2,1,0:T(8,128)(2,1)} %bitcast.4), calls=%async_computation | async-start | bytes 1048576 | tf_op jit(solution)/shard_map/all_to_all | solution.py:250
  14.5 13.9 %collective-permute-start.1 = (bf16[2,64,2048]{2,1,0:T(8,128)(2,1)S(1)}, bf16[2,64,2048]{2,1,0:T(8,128)(2,1)S(1)}, u32[]{:S(2)}, u32[]{:S(2)}) collective-permute-start(bf16[2,64,2048]{2,1,0:T(8,128)(2,1)S(1)} %bitcast.15), channel_id=1, source_target_pairs={{0,6},{1,7},{2,4},{3,5},{4,2},{5,3},{6,0},{7,1},{8,14},{9,15},{10,... | collective-permute-start | bytes 1572872 | tf_op jit(solution)/shard_map/ppermute | solution.py:224
  17.3 22.4 %collective-permute-start.3 = (bf16[2,64,2048]{2,1,0:T(8,128)(2,1)}, bf16[2,64,2048]{2,1,0:T(8,128)(2,1)S(1)}, u32[]{:S(2)}, u32[]{:S(2)}) collective-permute-start(bf16[2,64,2048]{2,1,0:T(8,128)(2,1)} %bitcast.7.up), channel_id=1, source_target_pairs={{0,6},{1,7},{2,4},{3,5},{4,2},{5,3},{6,0},{7,1},{8,14},{9,15},{10,... | collective-permute-start | bytes 1572872 | tf_op jit(solution)/shard_map/ppermute | solution.py:224
  18.5 6.6 %collective-permute-start.8 = (bf16[2,2,64,512]{3,2,1,0:T(8,128)(2,1)S(1)}, bf16[2,2,64,512]{3,2,1,0:T(8,128)(2,1)S(1)}, u32[]{:S(2)}, u32[]{:S(2)}) collective-permute-start(bf16[2,2,64,512]{3,2,1,0:T(8,128)(2,1)S(1)} %get-tuple-element.18), channel_id=1, source_target_pairs={{0,2},{1,3},{2,0},{3,1},{4,6},{5,7},{6,4},{7,5},{8,10},{9,11},{10,... | collective-permute-start | bytes 786440 | tf_op jit(solution)/shard_map/ppermute | solution.py:224
  19.7 26.3 %collective-permute-start = (bf16[2,64,2048]{2,1,0:T(8,128)(2,1)S(1)}, bf16[2,64,2048]{2,1,0:T(8,128)(2,1)S(1)}, u32[]{:S(2)}, u32[]{:S(2)}) collective-permute-start(bf16[2,64,2048]{2,1,0:T(8,128)(2,1)S(1)} %shard_map.83), channel_id=1, source_target_pairs={{0,1},{1,0},{2,3},{3,2},{4,5},{5,4},{6,7},{7,6},{8,9},{9,8},{10,11... | collective-permute-start | bytes 1572872 | tf_op jit(solution)/shard_map/ppermute | solution.py:224
  25.1 16.4 %collective-permute-start.9 = (bf16[2,2,64,512]{3,2,1,0:T(8,128)(2,1)S(1)}, bf16[2,2,64,512]{3,2,1,0:T(8,128)(2,1)S(1)}, u32[]{:S(2)}, u32[]{:S(2)}) collective-permute-start(bf16[2,2,64,512]{3,2,1,0:T(8,128)(2,1)S(1)} %give.1), channel_id=1, source_target_pairs={{0,1},{1,0},{2,3},{3,2},{4,5},{5,4},{6,7},{7,6},{8,9},{9,8},{10,11... | collective-permute-start | bytes 786440 | tf_op jit(solution)/shard_map/ppermute | solution.py:224
  28.4 17.6 %collective-permute-start.2 = (bf16[64,2048]{1,0:T(8,128)(2,1)S(1)}, bf16[64,2048]{1,0:T(8,128)(2,1)S(1)}, u32[]{:S(2)}, u32[]{:S(2)}) collective-permute-start(bf16[64,2048]{1,0:T(8,128)(2,1)S(1)} %shard_map.84), channel_id=1, source_target_pairs={{0,1},{1,0},{2,3},{3,2},{4,5},{5,4},{6,7},{7,6},{8,9},{9,8},{10,11... | collective-permute-start | bytes 786440 | tf_op jit(solution)/shard_map/ppermute | solution.py:224
  39.7 6.3 %collective-permute-start.4 = (bf16[64,2048]{1,0:T(8,128)(2,1)S(1)}, bf16[64,2048]{1,0:T(8,128)(2,1)S(1)}, u32[]{:S(2)}, u32[]{:S(2)}) collective-permute-start(bf16[64,2048]{1,0:T(8,128)(2,1)S(1)} %shard_map.85), channel_id=1, source_target_pairs={{0,1},{1,0},{2,3},{3,2},{4,5},{5,4},{6,7},{7,6},{8,9},{9,8},{10,11... | collective-permute-start | bytes 786440 | tf_op jit(solution)/shard_map/ppermute | solution.py:224
  42.2 9.8 %collective-permute-start.10 = (bf16[256,512]{1,0:T(8,128)(2,1)}, bf16[256,512]{1,0:T(8,128)(2,1)S(1)}, u32[]{:S(2)}, u32[]{:S(2)}) collective-permute-start(bf16[256,512]{1,0:T(8,128)(2,1)} %get-tuple-element.20), channel_id=1, source_target_pairs={{0,6},{1,7},{2,4},{3,5},{4,2},{5,3},{6,0},{7,1},{8,14},{9,15},{10,... | collective-permute-start | bytes 786440 | tf_op jit(solution)/shard_map/ppermute | solution.py:224
  46.0 0.7 copy-start
  46.7 1.0 %copy-start.1 = (bf16[64,2048]{1,0:T(8,128)(2,1)S(1)}, bf16[64,2048]{1,0:T(8,128)(2,1)}, u32[]{:S(2)}) copy-start(bf16[64,2048]{1,0:T(8,128)(2,1)} %copy-done) | copy-start | bytes 786436
  48.7 3.3 %collective-permute-start.5 = (bf16[128,256]{1,0:T(8,128)(2,1)S(1)}, bf16[128,256]{1,0:T(8,128)(2,1)S(1)}, u32[]{:S(2)}, u32[]{:S(2)}) collective-permute-start(bf16[128,256]{1,0:T(8,128)(2,1)S(1)} %hidden.1.h_own), channel_id=1, source_target_pairs={{0,2},{1,3},{2,0},{3,1},{4,6},{5,7},{6,4},{7,5},{8,10},{9,11},{10,... | collective-permute-start | bytes 196616 | tf_op jit(solution)/shard_map/ppermute | solution.py:224
  48.8 6.2 %collective-permute-start.6 = (bf16[128,256]{1,0:T(8,128)(2,1)S(1)}, bf16[128,256]{1,0:T(8,128)(2,1)S(1)}, u32[]{:S(2)}, u32[]{:S(2)}) collective-permute-start(bf16[128,256]{1,0:T(8,128)(2,1)S(1)} %hidden.1.h_own), channel_id=1, source_target_pairs={{0,6},{1,7},{2,4},{3,5},{4,2},{5,3},{6,0},{7,1},{8,14},{9,15},{10,... | collective-permute-start | bytes 196616 | tf_op jit(solution)/shard_map/ppermute | solution.py:224
  48.9 6.1 %collective-permute-start.7 = (bf16[128,256]{1,0:T(8,128)(2,1)S(1)}, bf16[128,256]{1,0:T(8,128)(2,1)S(1)}, u32[]{:S(2)}, u32[]{:S(2)}) collective-permute-start(bf16[128,256]{1,0:T(8,128)(2,1)S(1)} %hidden.1.h_own), channel_id=1, source_target_pairs={{0,4},{1,5},{2,6},{3,7},{4,0},{5,1},{6,2},{7,3},{8,12},{9,13},{10,... | collective-permute-start | bytes 196616 | tf_op jit(solution)/shard_map/ppermute | solution.py:224
  79.1 4.7 %collective-permute-start.11 = (f32[64,256]{1,0:T(8,128)S(1)}, f32[64,256]{1,0:T(8,128)S(1)}, u32[]{:S(2)}, u32[]{:S(2)}) collective-permute-start(f32[64,256]{1,0:T(8,128)S(1)} %get-tuple-element.22), channel_id=1, source_target_pairs={{0,1},{1,0},{2,3},{3,2},{4,5},{5,4},{6,7},{7,6},{8,9},{9,8},{10,11... | collective-permute-start | bytes 196616 | tf_op jit(solution)/shard_map/ppermute | solution.py:339

commit v4 on v3

--- a/solution.py
+++ b/solution.py
@@ -57,10 +57,9 @@
     return copies
 
 
-def expert_kernel(gate, up, out, sems, *, own):
-    _, core = position()
-    which = core if own else 1 - core
-    for copy in copy_all([(ref.at[which], out.at[i]) for i, ref in enumerate((gate, up))], sems):
+def theirs_kernel(gate, up, out, sems):
+    _, core = position()
+    for copy in copy_all([(ref.at[1 - core], out.at[i]) for i, ref in enumerate((gate, up))], sems):
         copy.wait()
 
 
@@ -126,22 +125,37 @@
     return lax.bitwise_xor(y, 1), 3 - y, lax.bitwise_xor(y, 2)
 
 
-def hidden_kernel(arrived, mine, swapped, gate, gate_swapped, up, up_swapped, hidden, *, slots):
-    _, core = position()
+def hidden_kernel(
+    own_gate, own_up, swapped, arrived, gate, gate_swapped, up, up_swapped, hidden, local, sems, *, slots
+):
+    _, core = position()
+    copies = copy_all(
+        [
+            (own_gate.at[core], local.at[0]),
+            (swapped.at[0], local.at[1]),
+            (own_up.at[core], local.at[2]),
+            (swapped.at[1], local.at[3]),
+        ],
+        sems,
+    )
     rows, width = arrived.shape
     kept = rows // 2
     count = slots // 2
     i, j = iota((kept, rows), 0), iota((kept, rows), 1)
     source = (i // count) * slots + i % count
-    total = None
     values = arrived[...]
+    xs = []
     for q in range(2):
         pick = jnp.where(j == source + q * count, 1.0, 0.0).astype(jnp.bfloat16)
-        x = dot_nn(pick, values).astype(jnp.bfloat16)
+        xs.append(dot_nn(pick, values).astype(jnp.bfloat16))
+    for copy in copies:
+        copy.wait()
+    total = None
+    for q, x in enumerate(xs):
         at = slice(q * width, (q + 1) * width)
         w = jnp.concatenate(
-            [mine[0, :, at], swapped[0, :, at], gate[core, :, at], gate_swapped[:, at]]
-            + [mine[1, :, at], swapped[1, :, at], up[core, :, at], up_swapped[:, at]]
+            [local[0, :, at], local[1, :, at], gate[core, :, at], gate_swapped[:, at]]
+            + [local[2, :, at], local[3, :, at], up[core, :, at], up_swapped[:, at]]
         )
         product = dot_nt(x, w)
         total = product if total is None else total + product
@@ -251,17 +265,15 @@
         packed.reshape(ep_size, slots, features // 2), "ep", split_axis=0, concat_axis=0, tiled=True
     ).reshape(rows, features // 2)
 
-    def expert_weights(own):
-        return pl.pallas_call(
-            functools.partial(expert_kernel, own=own),
-            out_shape=pltpu.VMEM((2, units, features), jnp.bfloat16),
-            in_specs=[anywhere] * 2,
-            out_specs=VMEM,
-            scratch_shapes=[pltpu.SemaphoreType.DMA((2,))],
-            compiler_params=PARAMS,
-        )(gate_t, up_t)
-
-    giving, mine = expert_weights(False), expert_weights(True)
+    giving = pl.pallas_call(
+        theirs_kernel,
+        out_shape=pltpu.VMEM((2, units, features), jnp.bfloat16),
+        in_specs=[anywhere] * 2,
+        out_specs=VMEM,
+        scratch_shapes=[pltpu.SemaphoreType.DMA((2,))],
+        compiler_params=PARAMS,
+        name="theirs",
+    )(gate_t, up_t)
     swapped = ppermute(giving, swap)
 
     def passed_on(both):
@@ -310,11 +322,20 @@
     hidden = pl.pallas_call(
         functools.partial(hidden_kernel, slots=slots),
         out_shape=pltpu.VMEM((rows // 2, 2 * CORES * units), jnp.bfloat16),
-        in_specs=[VMEM] * 7,
+        in_specs=[anywhere] * 3 + [VMEM] * 5,
         out_specs=VMEM,
+        scratch_shapes=[
+            pltpu.VMEM((4, units, features), jnp.bfloat16),
+            pltpu.SemaphoreType.DMA((4,)),
+        ],
         compiler_params=PARAMS,
         name="hidden",
-    )(*on_chip(arrived, mine, swapped, gate_both, gate_swapped, up_both, up_swapped))
+    )(
+        gate_t,
+        up_t,
+        *off_chip(swapped),
+        *on_chip(arrived, gate_both, gate_swapped, up_both, up_swapped),
+    )
     hiddens = [hidden] + [ppermute(hidden, pairs) for pairs in (near, same, across)]
     result = pl.pallas_call(
         functools.partial(down_kernel, slots=slots),

time: 84.8 us -> 83.3 us (0.982)
  the two profiles are of different devices: /device:TPU:1 before, /device:TPU:25 now
where the time goes in v4:
time: 83.3 us; the launch traced here: 82.7 us
  starting transfers between devices  30.4 us (36%)
  blocking collectives  24.5 us (29%)
  waiting for transfers between devices  18.6 us (22%)
  Pallas kernels  7.59 us (9%)
    all_to_all x1, blocking collectives, per_device(): lax.all_to_all(result.reshape(ep_size, slots, share), 'ep', split_axis=0,...  24.5 us
    ppermute x11, waiting for transfers between devices, ppermute(): return lax.ppermute(array, 'tp', pairs)  17.7 us
    ppermute x11, starting transfers between devices, ppermute(): return lax.ppermute(array, 'tp', pairs)  15.9 us
    all_to_all x1, starting transfers between devices, per_device(): lax.all_to_all(packed.reshape(ep_size, slots, features // 2), 'ep', split...  11.2 us
    ppermute x1, starting transfers between devices, per_device(): mixed_out = kept + lax.ppermute(sent, 'tp', swap)  3.29 us
    pallas_call x1, Pallas kernels, per_device(): pl.pallas_call(functools.partial(pack_kernel, slots=slots), out_shape=(pl...  2.45 us
    pallas_call x1, Pallas kernels, per_device(): pl.pallas_call(functools.partial(hidden_kernel, slots=slots), out_shape=p...  2.15 us
  transfers between devices with their start and end apart: 13, of which 7 were waited for; matrix products, arithmetic and copies ran while one was open for 0% of the time, Pallas kernels for 5%

profile of v4, /device:TPU:25, one launch (start us, length us, event | category | flops | bytes accessed | tf_op | source)
XLA Modules:
  0.0 82.7 jit_solution(5422194770587192454)
XLA Ops:
  0.0 2.5 %pack.1 = (bf16[256,1024]{1,0:T(8,128)(2,1)}, bf16[256,64]{1,0:T(8,128)(2,1)S(1)}, bf16[256,64]{1,0:T(8,128)(2,1)S(1)}) custom-call(bf16[64,2048]{1,0:T(8,128)(2,1)} %tokens.1, f32[1,2048]{1,0:T(1,128)} %bitcast.19, f32[1,2048]{1,0:T(1,128)} %bitcast.20, s32[4,64]{1,0:T(4,128)} %bitcast.21, f32[4,64]{1,0:T(4,128)} %bitcast.22), custom_call_target="tpu_custom_call" | custom-call | tf_op jit(solution)/shard_map/pack/pallas_call | solution.py:244
  2.5 0.0 copy-start
  2.5 0.0 copy-start.1
  2.5 11.2 %all-to-all-start = ((bf16[32,8,1024]{2,1,0:T(8,128)(2,1)}), bf16[32,8,1024]{2,1,0:T(8,128)(2,1)S(1)}, u32[]{:S(2)}, u32[]{:S(2)}) async-start(bf16[32,8,1024]{2,1,0:T(8,128)(2,1)} %bitcast.6), calls=%async_computation | async-start | bytes 1048576 | tf_op jit(solution)/shard_map/all_to_all | solution.py:264
  13.6 0.0 copy-done
  13.6 0.1 collective-permute-start.1
  13.7 0.0 copy-done.1
  13.8 2.7 %collective-permute-start.3 = (bf16[2,64,2048]{2,1,0:T(8,128)(2,1)S(1)}, bf16[2,64,2048]{2,1,0:T(8,128)(2,1)S(1)}, u32[]{:S(2)}, u32[]{:S(2)}) collective-permute-start(bf16[2,64,2048]{2,1,0:T(8,128)(2,1)S(1)} %bitcast.18), channel_id=1, source_target_pairs={{0,6},{1,7},{2,4},{3,5},{4,2},{5,3},{6,0},{7,1},{8,14},{9,15},{10,... | collective-permute-start | bytes 1572872 | tf_op jit(solution)/shard_map/ppermute | solution.py:238
  16.4 1.1 %pieces.1 = (bf16[2,2,64,512]{3,2,1,0:T(8,128)(2,1)S(1)}, bf16[2,2,64,512]{3,2,1,0:T(8,128)(2,1)S(1)}) custom-call(bf16[2,64,2048]{2,1,0:T(8,128)(2,1)} %down.2), custom_call_target="tpu_custom_call" | custom-call | tf_op jit(solution)/shard_map/pieces/pallas_call | solution.py:293
  17.5 0.1 collective-permute-start.8
  17.6 1.1 %theirs.1 = bf16[2,64,2048]{2,1,0:T(8,128)(2,1)S(1)} custom-call(bf16[2,64,2048]{2,1,0:T(8,128)(2,1)} %bitcast.13, bf16[2,64,2048]{2,1,0:T(8,128)(2,1)} %bitcast.16), custom_call_target="tpu_custom_call" | custom-call | tf_op jit(solution)/shard_map/theirs/pallas_call | solution.py:268
  18.7 1.6 %collective-permute-start = (bf16[2,64,2048]{2,1,0:T(8,128)(2,1)S(1)}, bf16[2,64,2048]{2,1,0:T(8,128)(2,1)S(1)}, u32[]{:S(2)}, u32[]{:S(2)}) collective-permute-start(bf16[2,64,2048]{2,1,0:T(8,128)(2,1)S(1)} %theirs.1), channel_id=1, source_target_pairs={{0,1},{1,0},{2,3},{3,2},{4,5},{5,4},{6,7},{7,6},{8,9},{9,8},{10,11... | collective-permute-start | bytes 1572872 | tf_op jit(solution)/shard_map/ppermute | solution.py:238
  20.3 3.7 %collective-permute-done.8.near = bf16[2,2,64,512]{3,2,1,0:T(8,128)(2,1)S(1)} collective-permute-done((bf16[2,2,64,512]{3,2,1,0:T(8,128)(2,1)S(1)}, bf16[2,2,64,512]{3,2,1,0:T(8,128)(2,1)S(1)}, u32[]{:S(2)}, u32[]{:S(2)}) %collective-permute-start.8) | collective-permute-done | bytes 262176 | tf_op jit(solution)/shard_map/ppermute | solution.py:238
  24.0 2.5 %collective-permute-start.9 = (bf16[2,2,64,512]{3,2,1,0:T(8,128)(2,1)S(1)}, bf16[2,2,64,512]{3,2,1,0:T(8,128)(2,1)S(1)}, u32[]{:S(2)}, u32[]{:S(2)}) collective-permute-start(bf16[2,2,64,512]{3,2,1,0:T(8,128)(2,1)S(1)} %give.1), channel_id=1, source_target_pairs={{0,1},{1,0},{2,3},{3,2},{4,5},{5,4},{6,7},{7,6},{8,9},{9,8},{10,11... | collective-permute-start | bytes 786440 | tf_op jit(solution)/shard_map/ppermute | solution.py:238
  26.5 1.0 %collective-permute-done.1.both.gate = bf16[2,64,2048]{2,1,0:T(8,128)(2,1)S(1)} collective-permute-done((bf16[2,64,2048]{2,1,0:T(8,128)(2,1)S(1)}, bf16[2,64,2048]{2,1,0:T(8,128)(2,1)S(1)}, u32[]{:S(2)}, u32[]{:S(2)}) %collective-permute-start.1) | collective-permute-done | bytes 524320 | tf_op jit(solution)/shard_map/ppermute | solution.py:238
  27.5 3.3 %collective-permute-start.2 = (bf16[64,2048]{1,0:T(8,128)(2,1)S(1)}, bf16[64,2048]{1,0:T(8,128)(2,1)S(1)}, u32[]{:S(2)}, u32[]{:S(2)}) collective-permute-start(bf16[64,2048]{1,0:T(8,128)(2,1)S(1)} %shard_map.82), channel_id=1, source_target_pairs={{0,1},{1,0},{2,3},{3,2},{4,5},{5,4},{6,7},{7,6},{8,9},{9,8},{10,11... | collective-permute-start | bytes 786440 | tf_op jit(solution)/shard_map/ppermute | solution.py:238
  30.8 7.9 %collective-permute-done.3.both.up = bf16[2,64,2048]{2,1,0:T(8,128)(2,1)S(1)} collective-permute-done((bf16[2,64,2048]{2,1,0:T(8,128)(2,1)S(1)}, bf16[2,64,2048]{2,1,0:T(8,128)(2,1)S(1)}, u32[]{:S(2)}, u32[]{:S(2)}) %collective-permute-start.3) | collective-permute-done | bytes 524320 | tf_op jit(solution)/shard_map/ppermute | solution.py:238
  38.7 1.9 %collective-permute-start.4 = (bf16[64,2048]{1,0:T(8,128)(2,1)S(1)}, bf16[64,2048]{1,0:T(8,128)(2,1)S(1)}, u32[]{:S(2)}, u32[]{:S(2)}) collective-permute-start(bf16[64,2048]{1,0:T(8,128)(2,1)S(1)} %shard_map.83), channel_id=1, source_target_pairs={{0,1},{1,0},{2,3},{3,2},{4,5},{5,4},{6,7},{7,6},{8,9},{9,8},{10,11... | collective-permute-start | bytes 786440 | tf_op jit(solution)/shard_map/ppermute | solution.py:238
  40.6 0.0 collective-permute-done.9.other
  40.7 0.1 collective-permute-start.10
  40.8 0.0 collective-permute-done.swapped
  40.8 0.0 copy-start.2
  40.8 0.0 collective-permute-done.2.gate_swapped
  40.8 0.8 copy-done.2
  41.6 0.2 collective-permute-done.4.up_swapped
  41.8 0.0 all-to-all-done
  41.8 2.2 %hidden.1.h_own = bf16[128,256]{1,0:T(8,128)(2,1)S(1)} custom-call(bf16[2,64,2048]{2,1,0:T(8,128)(2,1)} %bitcast.14, bf16[2,64,2048]{2,1,0:T(8,128)(2,1)} %bitcast.17, bf16[2,64,2048]{2,1,0:T(8,128)(2,1)} %copy-done.2, bf16[256,1024]{1,0:T(8,128)(2,1)S(1)} %bitcast.10, bf16[2,64,2048]{2,1,0:T(8,128)(2,1)S(1)} %collective-permute-done.1.both.gate, ...), custom_call_target="tpu_custom_call" | custom-call | tf_op jit(solution)/shard_map/hidden/pallas_call | solution.py:322
  44.0 0.1 collective-permute-start.5
  44.1 2.5 %collective-permute-start.6 = (bf16[128,256]{1,0:T(8,128)(2,1)S(1)}, bf16[128,256]{1,0:T(8,128)(2,1)S(1)}, u32[]{:S(2)}, u32[]{:S(2)}) collective-permute-start(bf16[128,256]{1,0:T(8,128)(2,1)S(1)} %hidden.1.h_own), channel_id=1, source_target_pairs={{0,6},{1,7},{2,4},{3,5},{4,2},{5,3},{6,0},{7,1},{8,14},{9,15},{10,... | collective-permute-start | bytes 196616 | tf_op jit(solution)/shard_map/ppermute | solution.py:238
  46.6 1.1 %collective-permute-start.7 = (bf16[128,256]{1,0:T(8,128)(2,1)S(1)}, bf16[128,256]{1,0:T(8,128)(2,1)S(1)}, u32[]{:S(2)}, u32[]{:S(2)}) collective-permute-start(bf16[128,256]{1,0:T(8,128)(2,1)S(1)} %hidden.1.h_own), channel_id=1, source_target_pairs={{0,4},{1,5},{2,6},{3,7},{4,0},{5,1},{6,2},{7,3},{8,12},{9,13},{10,... | collective-permute-start | bytes 196616 | tf_op jit(solution)/shard_map/ppermute | solution.py:238
  47.7 2.1 %collective-permute-done.10.same = bf16[256,512]{1,0:T(8,128)(2,1)S(1)} collective-permute-done((bf16[256,512]{1,0:T(8,128)(2,1)S(1)}, bf16[256,512]{1,0:T(8,128)(2,1)S(1)}, u32[]{:S(2)}, u32[]{:S(2)}) %collective-permute-start.10) | collective-permute-done | bytes 262176 | tf_op jit(solution)/shard_map/ppermute | solution.py:238
  49.8 0.0 collective-permute-done.5.h_first
  49.8 2.8 %collective-permute-done.6.h_second = bf16[128,256]{1,0:T(8,128)(2,1)S(1)} collective-permute-done((bf16[128,256]{1,0:T(8,128)(2,1)S(1)}, bf16[128,256]{1,0:T(8,128)(2,1)S(1)}, u32[]{:S(2)}, u32[]{:S(2)}) %collective-permute-start.6) | collective-permute-done | bytes 65568 | tf_op jit(solution)/shard_map/ppermute | solution.py:238
  52.6 0.0 collective-permute-done.7.h_third
  52.6 0.4 down.3
  53.0 24.5 %all_to_all.10 = f32[32,8,512]{2,1,0:T(8,128)S(1)} all-to-all(f32[32,8,512]{2,1,0:T(8,128)S(1)} %bitcast.12), channel_id=1, replica_groups=mesh['ep'=32,'tp'=8] {'ep'}, dimensions={0} | all-to-all | bytes 1048576 | tf_op jit(solution)/shard_map/all_to_all | solution.py:348
  77.6 0.3 combine.1
  77.8 3.3 %collective-permute-start.11 = (f32[64,256]{1,0:T(8,128)S(1)}, f32[64,256]{1,0:T(8,128)S(1)}, u32[]{:S(2)}, u32[]{:S(2)}) collective-permute-start(f32[64,256]{1,0:T(8,128)S(1)} %get-tuple-element.22), channel_id=1, source_target_pairs={{0,1},{1,0},{2,3},{3,2},{4,5},{5,4},{6,7},{7,6},{8,9},{9,8},{10,11... | collective-permute-start | bytes 196616 | tf_op jit(solution)/shard_map/ppermute | solution.py:360
  81.1 0.9 %collective-permute-done.11 = f32[64,256]{1,0:T(8,128)S(1)} collective-permute-done((f32[64,256]{1,0:T(8,128)S(1)}, f32[64,256]{1,0:T(8,128)S(1)}, u32[]{:S(2)}, u32[]{:S(2)}) %collective-permute-start.11) | collective-permute-done | bytes 65568 | tf_op jit(solution)/shard_map/ppermute | solution.py:360
  82.0 0.6 add_convert_fusion
  (4 shorter events, 0.1 us)
Async XLA Ops:
  2.5 11.2 %copy-start = (bf16[2,2048,64]{1,2,0:T(8,128)(2,1)S(1)}, bf16[2,2048,64]{1,2,0:T(8,128)(2,1)}, u32[]{:S(2)}) copy-start(bf16[2,2048,64]{1,2,0:T(8,128)(2,1)} %param.13) | copy-start | bytes 1572868
  2.5 11.3 %copy-start.1 = (bf16[2,2048,64]{1,2,0:T(8,128)(2,1)S(1)}, bf16[2,2048,64]{1,2,0:T(8,128)(2,1)}, u32[]{:S(2)}) copy-start(bf16[2,2048,64]{1,2,0:T(8,128)(2,1)} %param.14) | copy-start | bytes 1572868
  2.5 39.3 %all-to-all-start = ((bf16[32,8,1024]{2,1,0:T(8,128)(2,1)}), bf16[32,8,1024]{2,1,0:T(8,128)(2,1)S(1)}, u32[]{:S(2)}, u32[]{:S(2)}) async-start(bf16[32,8,1024]{2,1,0:T(8,128)(2,1)} %bitcast.6), calls=%async_computation | async-start | bytes 1048576 | tf_op jit(solution)/shard_map/all_to_all | solution.py:264
  13.6 13.8 %collective-permute-start.1 = (bf16[2,64,2048]{2,1,0:T(8,128)(2,1)S(1)}, bf16[2,64,2048]{2,1,0:T(8,128)(2,1)S(1)}, u32[]{:S(2)}, u32[]{:S(2)}) collective-permute-start(bf16[2,64,2048]{2,1,0:T(8,128)(2,1)S(1)} %bitcast.15), channel_id=1, source_target_pairs={{0,6},{1,7},{2,4},{3,5},{4,2},{5,3},{6,0},{7,1},{8,14},{9,15},{10,... | collective-permute-start | bytes 1572872 | tf_op jit(solution)/shard_map/ppermute | solution.py:238
  13.8 24.9 %collective-permute-start.3 = (bf16[2,64,2048]{2,1,0:T(8,128)(2,1)S(1)}, bf16[2,64,2048]{2,1,0:T(8,128)(2,1)S(1)}, u32[]{:S(2)}, u32[]{:S(2)}) collective-permute-start(bf16[2,64,2048]{2,1,0:T(8,128)(2,1)S(1)} %bitcast.18), channel_id=1, source_target_pairs={{0,6},{1,7},{2,4},{3,5},{4,2},{5,3},{6,0},{7,1},{8,14},{9,15},{10,... | collective-permute-start | bytes 1572872 | tf_op jit(solution)/shard_map/ppermute | solution.py:238
  17.5 6.4 %collective-permute-start.8 = (bf16[2,2,64,512]{3,2,1,0:T(8,128)(2,1)S(1)}, bf16[2,2,64,512]{3,2,1,0:T(8,128)(2,1)S(1)}, u32[]{:S(2)}, u32[]{:S(2)}) collective-permute-start(bf16[2,2,64,512]{3,2,1,0:T(8,128)(2,1)S(1)} %get-tuple-element.18), channel_id=1, source_target_pairs={{0,2},{1,3},{2,0},{3,1},{4,6},{5,7},{6,4},{7,5},{8,10},{9,11},{10,... | collective-permute-start | bytes 786440 | tf_op jit(solution)/shard_map/ppermute | solution.py:238
  18.7 22.1 %collective-permute-start = (bf16[2,64,2048]{2,1,0:T(8,128)(2,1)S(1)}, bf16[2,64,2048]{2,1,0:T(8,128)(2,1)S(1)}, u32[]{:S(2)}, u32[]{:S(2)}) collective-permute-start(bf16[2,64,2048]{2,1,0:T(8,128)(2,1)S(1)} %theirs.1), channel_id=1, source_target_pairs={{0,1},{1,0},{2,3},{3,2},{4,5},{5,4},{6,7},{7,6},{8,9},{9,8},{10,11... | collective-permute-start | bytes 1572872 | tf_op jit(solution)/shard_map/ppermute | solution.py:238
  24.0 16.6 %collective-permute-start.9 = (bf16[2,2,64,512]{3,2,1,0:T(8,128)(2,1)S(1)}, bf16[2,2,64,512]{3,2,1,0:T(8,128)(2,1)S(1)}, u32[]{:S(2)}, u32[]{:S(2)}) collective-permute-start(bf16[2,2,64,512]{3,2,1,0:T(8,128)(2,1)S(1)} %give.1), channel_id=1, source_target_pairs={{0,1},{1,0},{2,3},{3,2},{4,5},{5,4},{6,7},{7,6},{8,9},{9,8},{10,11... | collective-permute-start | bytes 786440 | tf_op jit(solution)/shard_map/ppermute | solution.py:238
  27.5 13.3 %collective-permute-start.2 = (bf16[64,2048]{1,0:T(8,128)(2,1)S(1)}, bf16[64,2048]{1,0:T(8,128)(2,1)S(1)}, u32[]{:S(2)}, u32[]{:S(2)}) collective-permute-start(bf16[64,2048]{1,0:T(8,128)(2,1)S(1)} %shard_map.82), channel_id=1, source_target_pairs={{0,1},{1,0},{2,3},{3,2},{4,5},{5,4},{6,7},{7,6},{8,9},{9,8},{10,11... | collective-permute-start | bytes 786440 | tf_op jit(solution)/shard_map/ppermute | solution.py:238
  38.7 3.1 %collective-permute-start.4 = (bf16[64,2048]{1,0:T(8,128)(2,1)S(1)}, bf16[64,2048]{1,0:T(8,128)(2,1)S(1)}, u32[]{:S(2)}, u32[]{:S(2)}) collective-permute-start(bf16[64,2048]{1,0:T(8,128)(2,1)S(1)} %shard_map.83), channel_id=1, source_target_pairs={{0,1},{1,0},{2,3},{3,2},{4,5},{5,4},{6,7},{7,6},{8,9},{9,8},{10,11... | collective-permute-start | bytes 786440 | tf_op jit(solution)/shard_map/ppermute | solution.py:238
  40.7 9.1 %collective-permute-start.10 = (bf16[256,512]{1,0:T(8,128)(2,1)S(1)}, bf16[256,512]{1,0:T(8,128)(2,1)S(1)}, u32[]{:S(2)}, u32[]{:S(2)}) collective-permute-start(bf16[256,512]{1,0:T(8,128)(2,1)S(1)} %get-tuple-element.20), channel_id=1, source_target_pairs={{0,6},{1,7},{2,4},{3,5},{4,2},{5,3},{6,0},{7,1},{8,14},{9,15},{10,... | collective-permute-start | bytes 786440 | tf_op jit(solution)/shard_map/ppermute | solution.py:238
  40.8 0.8 copy-start.2
  44.0 5.9 %collective-permute-start.5 = (bf16[128,256]{1,0:T(8,128)(2,1)S(1)}, bf16[128,256]{1,0:T(8,128)(2,1)S(1)}, u32[]{:S(2)}, u32[]{:S(2)}) collective-permute-start(bf16[128,256]{1,0:T(8,128)(2,1)S(1)} %hidden.1.h_own), channel_id=1, source_target_pairs={{0,2},{1,3},{2,0},{3,1},{4,6},{5,7},{6,4},{7,5},{8,10},{9,11},{10,... | collective-permute-start | bytes 196616 | tf_op jit(solution)/shard_map/ppermute | solution.py:238
  44.1 8.6 %collective-permute-start.6 = (bf16[128,256]{1,0:T(8,128)(2,1)S(1)}, bf16[128,256]{1,0:T(8,128)(2,1)S(1)}, u32[]{:S(2)}, u32[]{:S(2)}) collective-permute-start(bf16[128,256]{1,0:T(8,128)(2,1)S(1)} %hidden.1.h_own), channel_id=1, source_target_pairs={{0,6},{1,7},{2,4},{3,5},{4,2},{5,3},{6,0},{7,1},{8,14},{9,15},{10,... | collective-permute-start | bytes 196616 | tf_op jit(solution)/shard_map/ppermute | solution.py:238
  46.6 6.0 %collective-permute-start.7 = (bf16[128,256]{1,0:T(8,128)(2,1)S(1)}, bf16[128,256]{1,0:T(8,128)(2,1)S(1)}, u32[]{:S(2)}, u32[]{:S(2)}) collective-permute-start(bf16[128,256]{1,0:T(8,128)(2,1)S(1)} %hidden.1.h_own), channel_id=1, source_target_pairs={{0,4},{1,5},{2,6},{3,7},{4,0},{5,1},{6,2},{7,3},{8,12},{9,13},{10,... | collective-permute-start | bytes 196616 | tf_op jit(solution)/shard_map/ppermute | solution.py:238
  77.8 4.2 %collective-permute-start.11 = (f32[64,256]{1,0:T(8,128)S(1)}, f32[64,256]{1,0:T(8,128)S(1)}, u32[]{:S(2)}, u32[]{:S(2)}) collective-permute-start(f32[64,256]{1,0:T(8,128)S(1)} %get-tuple-element.22), channel_id=1, source_target_pairs={{0,1},{1,0},{2,3},{3,2},{4,5},{5,4},{6,7},{7,6},{8,9},{9,8},{10,11... | collective-permute-start | bytes 196616 | tf_op jit(solution)/shard_map/ppermute | solution.py:360

commit v5 on v4

--- a/solution.py
+++ b/solution.py
@@ -253,8 +253,8 @@
         compiler_params=PARAMS,
         name="pack",
     )(
+        *on_chip(tokens),
         *off_chip(
-            tokens,
             norm_gain.reshape(1, features),
             norm_shift.reshape(1, features),
             expert_ids.T,
@@ -336,7 +336,8 @@
         *off_chip(swapped),
         *on_chip(arrived, gate_both, gate_swapped, up_both, up_swapped),
     )
-    hiddens = [hidden] + [ppermute(hidden, pairs) for pairs in (near, same, across)]
+    h_across = ppermute(hidden, across)
+    hiddens = [hidden, ppermute(hidden, near), ppermute(hidden, same), h_across]
     result = pl.pallas_call(
         functools.partial(down_kernel, slots=slots),
         out_shape=pltpu.VMEM((rows, share), jnp.float32),

time: 83.3 us -> 84.1 us (level)
  local copies, waits for them, and re-layouts: 0.78 us -> 1.73 us
    unnamed x6 -> x8, local copies, waits for them, and re-layouts: 0.78 us -> 1.73 us
where the time goes in v5:
time: 84.1 us; the launch traced here: 83.4 us
  starting transfers between devices  30.4 us (36%)
  blocking collectives  24.5 us (29%)
  waiting for transfers between devices  18.7 us (22%)
  Pallas kernels  7.34 us (9%)
  local copies, waits for them, and re-layouts  1.73 us (2%)
    all_to_all x1, blocking collectives, per_device(): lax.all_to_all(result.reshape(ep_size, slots, share), 'ep', split_axis=0,...  24.5 us
    ppermute x11, waiting for transfers between devices, ppermute(): return lax.ppermute(array, 'tp', pairs)  17.8 us
    ppermute x11, starting transfers between devices, ppermute(): return lax.ppermute(array, 'tp', pairs)  15.9 us
    all_to_all x1, starting transfers between devices, per_device(): lax.all_to_all(packed.reshape(ep_size, slots, features // 2), 'ep', split...  11.2 us
    ppermute x1, starting transfers between devices, per_device(): mixed_out = kept + lax.ppermute(sent, 'tp', swap)  3.29 us
    pallas_call x1, Pallas kernels, per_device(): pl.pallas_call(functools.partial(pack_kernel, slots=slots), out_shape=(pl...  2.21 us
    pallas_call x1, Pallas kernels, per_device(): pl.pallas_call(functools.partial(hidden_kernel, slots=slots), out_shape=p...  2.14 us
    unnamed x8, local copies, waits for them, and re-layouts  1.73 us
  transfers between devices with their start and end apart: 13, of which 7 were waited for; matrix products, arithmetic and copies ran while one was open for 0% of the time, Pallas kernels for 5%

profile of v5, /device:TPU:25, one launch (start us, length us, event | category | flops | bytes accessed | tf_op | source)
XLA Modules:
  0.0 83.4 jit_solution(12476996325780024714)
XLA Ops:
  0.0 0.0 copy-start
  0.0 0.9 %copy-done = bf16[64,2048]{1,0:T(8,128)(2,1)S(1)} copy-done((bf16[64,2048]{1,0:T(8,128)(2,1)S(1)}, bf16[64,2048]{1,0:T(8,128)(2,1)}, u32[]{:S(2)}) %copy-start) | copy-done | bytes 262168
  1.0 2.2 %pack.1 = (bf16[256,1024]{1,0:T(8,128)(2,1)}, bf16[256,64]{1,0:T(8,128)(2,1)S(1)}, bf16[256,64]{1,0:T(8,128)(2,1)S(1)}) custom-call(bf16[64,2048]{1,0:T(8,128)(2,1)S(1)} %copy-done, f32[1,2048]{1,0:T(1,128)} %bitcast.19, f32[1,2048]{1,0:T(1,128)} %bitcast.20, s32[4,64]{1,0:T(4,128)} %bitcast.21, f32[4,64]{1,0:T(4,128)} %bitcast.22), custom_call_target="tpu_custom_call" | custom-call | tf_op jit(solution)/shard_map/pack/pallas_call | solution.py:244
  3.2 0.0 copy-start.1
  3.2 0.0 copy-start.2
  3.2 11.2 %all-to-all-start = ((bf16[32,8,1024]{2,1,0:T(8,128)(2,1)}), bf16[32,8,1024]{2,1,0:T(8,128)(2,1)S(1)}, u32[]{:S(2)}, u32[]{:S(2)}) async-start(bf16[32,8,1024]{2,1,0:T(8,128)(2,1)} %bitcast.6), calls=%async_computation | async-start | bytes 1048576 | tf_op jit(solution)/shard_map/all_to_all | solution.py:264
  14.3 0.0 copy-done.1
  14.3 0.1 collective-permute-start.1
  14.4 0.0 copy-done.2
  14.5 2.7 %collective-permute-start.3 = (bf16[2,64,2048]{2,1,0:T(8,128)(2,1)S(1)}, bf16[2,64,2048]{2,1,0:T(8,128)(2,1)S(1)}, u32[]{:S(2)}, u32[]{:S(2)}) collective-permute-start(bf16[2,64,2048]{2,1,0:T(8,128)(2,1)S(1)} %bitcast.18), channel_id=1, source_target_pairs={{0,6},{1,7},{2,4},{3,5},{4,2},{5,3},{6,0},{7,1},{8,14},{9,15},{10,... | collective-permute-start | bytes 1572872 | tf_op jit(solution)/shard_map/ppermute | solution.py:238
  17.1 1.1 %pieces.1 = (bf16[2,2,64,512]{3,2,1,0:T(8,128)(2,1)S(1)}, bf16[2,2,64,512]{3,2,1,0:T(8,128)(2,1)S(1)}) custom-call(bf16[2,64,2048]{2,1,0:T(8,128)(2,1)} %down.2), custom_call_target="tpu_custom_call" | custom-call | tf_op jit(solution)/shard_map/pieces/pallas_call | solution.py:293
  18.3 0.1 collective-permute-start.8
  18.4 1.1 %theirs.1 = bf16[2,64,2048]{2,1,0:T(8,128)(2,1)S(1)} custom-call(bf16[2,64,2048]{2,1,0:T(8,128)(2,1)} %bitcast.13, bf16[2,64,2048]{2,1,0:T(8,128)(2,1)} %bitcast.16), custom_call_target="tpu_custom_call" | custom-call | tf_op jit(solution)/shard_map/theirs/pallas_call | solution.py:268
  19.4 1.6 %collective-permute-start = (bf16[2,64,2048]{2,1,0:T(8,128)(2,1)S(1)}, bf16[2,64,2048]{2,1,0:T(8,128)(2,1)S(1)}, u32[]{:S(2)}, u32[]{:S(2)}) collective-permute-start(bf16[2,64,2048]{2,1,0:T(8,128)(2,1)S(1)} %theirs.1), channel_id=1, source_target_pairs={{0,1},{1,0},{2,3},{3,2},{4,5},{5,4},{6,7},{7,6},{8,9},{9,8},{10,11... | collective-permute-start | bytes 1572872 | tf_op jit(solution)/shard_map/ppermute | solution.py:238
  21.0 3.7 %collective-permute-done.8.near = bf16[2,2,64,512]{3,2,1,0:T(8,128)(2,1)S(1)} collective-permute-done((bf16[2,2,64,512]{3,2,1,0:T(8,128)(2,1)S(1)}, bf16[2,2,64,512]{3,2,1,0:T(8,128)(2,1)S(1)}, u32[]{:S(2)}, u32[]{:S(2)}) %collective-permute-start.8) | collective-permute-done | bytes 262176 | tf_op jit(solution)/shard_map/ppermute | solution.py:238
  24.7 2.5 %collective-permute-start.9 = (bf16[2,2,64,512]{3,2,1,0:T(8,128)(2,1)S(1)}, bf16[2,2,64,512]{3,2,1,0:T(8,128)(2,1)S(1)}, u32[]{:S(2)}, u32[]{:S(2)}) collective-permute-start(bf16[2,2,64,512]{3,2,1,0:T(8,128)(2,1)S(1)} %give.1), channel_id=1, source_target_pairs={{0,1},{1,0},{2,3},{3,2},{4,5},{5,4},{6,7},{7,6},{8,9},{9,8},{10,11... | collective-permute-start | bytes 786440 | tf_op jit(solution)/shard_map/ppermute | solution.py:238
  27.2 1.0 %collective-permute-done.1.both.gate = bf16[2,64,2048]{2,1,0:T(8,128)(2,1)S(1)} collective-permute-done((bf16[2,64,2048]{2,1,0:T(8,128)(2,1)S(1)}, bf16[2,64,2048]{2,1,0:T(8,128)(2,1)S(1)}, u32[]{:S(2)}, u32[]{:S(2)}) %collective-permute-start.1) | collective-permute-done | bytes 524320 | tf_op jit(solution)/shard_map/ppermute | solution.py:238
  28.2 3.3 %collective-permute-start.2 = (bf16[64,2048]{1,0:T(8,128)(2,1)S(1)}, bf16[64,2048]{1,0:T(8,128)(2,1)S(1)}, u32[]{:S(2)}, u32[]{:S(2)}) collective-permute-start(bf16[64,2048]{1,0:T(8,128)(2,1)S(1)} %shard_map.82), channel_id=1, source_target_pairs={{0,1},{1,0},{2,3},{3,2},{4,5},{5,4},{6,7},{7,6},{8,9},{9,8},{10,11... | collective-permute-start | bytes 786440 | tf_op jit(solution)/shard_map/ppermute | solution.py:238
  31.5 7.9 %collective-permute-done.3.both.up = bf16[2,64,2048]{2,1,0:T(8,128)(2,1)S(1)} collective-permute-done((bf16[2,64,2048]{2,1,0:T(8,128)(2,1)S(1)}, bf16[2,64,2048]{2,1,0:T(8,128)(2,1)S(1)}, u32[]{:S(2)}, u32[]{:S(2)}) %collective-permute-start.3) | collective-permute-done | bytes 524320 | tf_op jit(solution)/shard_map/ppermute | solution.py:238
  39.4 1.9 %collective-permute-start.4 = (bf16[64,2048]{1,0:T(8,128)(2,1)S(1)}, bf16[64,2048]{1,0:T(8,128)(2,1)S(1)}, u32[]{:S(2)}, u32[]{:S(2)}) collective-permute-start(bf16[64,2048]{1,0:T(8,128)(2,1)S(1)} %shard_map.83), channel_id=1, source_target_pairs={{0,1},{1,0},{2,3},{3,2},{4,5},{5,4},{6,7},{7,6},{8,9},{9,8},{10,11... | collective-permute-start | bytes 786440 | tf_op jit(solution)/shard_map/ppermute | solution.py:238
  41.3 0.0 collective-permute-done.9.other
  41.4 0.1 collective-permute-start.10
  41.5 0.0 collective-permute-done.swapped
  41.5 0.0 copy-start.3
  41.5 0.0 collective-permute-done.2.gate_swapped
  41.5 0.8 copy-done.3
  42.3 0.2 collective-permute-done.4.up_swapped
  42.5 0.0 all-to-all-done
  42.5 2.1 %hidden.1.h_own = bf16[128,256]{1,0:T(8,128)(2,1)S(1)} custom-call(bf16[2,64,2048]{2,1,0:T(8,128)(2,1)} %bitcast.14, bf16[2,64,2048]{2,1,0:T(8,128)(2,1)} %bitcast.17, bf16[2,64,2048]{2,1,0:T(8,128)(2,1)} %copy-done.3, bf16[256,1024]{1,0:T(8,128)(2,1)S(1)} %bitcast.10, bf16[2,64,2048]{2,1,0:T(8,128)(2,1)S(1)} %collective-permute-done.1.both.gate, ...), custom_call_target="tpu_custom_call" | custom-call | tf_op jit(solution)/shard_map/hidden/pallas_call | solution.py:322
  44.6 0.1 collective-permute-start.5
  44.7 2.5 %collective-permute-start.6 = (bf16[128,256]{1,0:T(8,128)(2,1)S(1)}, bf16[128,256]{1,0:T(8,128)(2,1)S(1)}, u32[]{:S(2)}, u32[]{:S(2)}) collective-permute-start(bf16[128,256]{1,0:T(8,128)(2,1)S(1)} %hidden.1.h_own), channel_id=1, source_target_pairs={{0,6},{1,7},{2,4},{3,5},{4,2},{5,3},{6,0},{7,1},{8,14},{9,15},{10,... | collective-permute-start | bytes 196616 | tf_op jit(solution)/shard_map/ppermute | solution.py:238
  47.3 1.1 %collective-permute-start.7 = (bf16[128,256]{1,0:T(8,128)(2,1)S(1)}, bf16[128,256]{1,0:T(8,128)(2,1)S(1)}, u32[]{:S(2)}, u32[]{:S(2)}) collective-permute-start(bf16[128,256]{1,0:T(8,128)(2,1)S(1)} %hidden.1.h_own), channel_id=1, source_target_pairs={{0,4},{1,5},{2,6},{3,7},{4,0},{5,1},{6,2},{7,3},{8,12},{9,13},{10,... | collective-permute-start | bytes 196616 | tf_op jit(solution)/shard_map/ppermute | solution.py:238
  48.4 2.1 %collective-permute-done.10.same = bf16[256,512]{1,0:T(8,128)(2,1)S(1)} collective-permute-done((bf16[256,512]{1,0:T(8,128)(2,1)S(1)}, bf16[256,512]{1,0:T(8,128)(2,1)S(1)}, u32[]{:S(2)}, u32[]{:S(2)}) %collective-permute-start.10) | collective-permute-done | bytes 262176 | tf_op jit(solution)/shard_map/ppermute | solution.py:238
  50.5 0.0 collective-permute-done.5.h_first
  50.5 2.8 %collective-permute-done.6.h_second = bf16[128,256]{1,0:T(8,128)(2,1)S(1)} collective-permute-done((bf16[128,256]{1,0:T(8,128)(2,1)S(1)}, bf16[128,256]{1,0:T(8,128)(2,1)S(1)}, u32[]{:S(2)}, u32[]{:S(2)}) %collective-permute-start.6) | collective-permute-done | bytes 65568 | tf_op jit(solution)/shard_map/ppermute | solution.py:238
  53.3 0.0 collective-permute-done.7.h_third
  53.3 0.4 down.3
  53.8 24.5 %all_to_all.10 = f32[32,8,512]{2,1,0:T(8,128)S(1)} all-to-all(f32[32,8,512]{2,1,0:T(8,128)S(1)} %bitcast.12), channel_id=1, replica_groups=mesh['ep'=32,'tp'=8] {'ep'}, dimensions={0} | all-to-all | bytes 1048576 | tf_op jit(solution)/shard_map/all_to_all | solution.py:349
  78.3 0.3 combine.1
  78.5 3.3 %collective-permute-start.11 = (f32[64,256]{1,0:T(8,128)S(1)}, f32[64,256]{1,0:T(8,128)S(1)}, u32[]{:S(2)}, u32[]{:S(2)}) collective-permute-start(f32[64,256]{1,0:T(8,128)S(1)} %get-tuple-element.22), channel_id=1, source_target_pairs={{0,1},{1,0},{2,3},{3,2},{4,5},{5,4},{6,7},{7,6},{8,9},{9,8},{10,11... | collective-permute-start | bytes 196616 | tf_op jit(solution)/shard_map/ppermute | solution.py:361
  81.8 0.9 %collective-permute-done.11 = f32[64,256]{1,0:T(8,128)S(1)} collective-permute-done((f32[64,256]{1,0:T(8,128)S(1)}, f32[64,256]{1,0:T(8,128)S(1)}, u32[]{:S(2)}, u32[]{:S(2)}) %collective-permute-start.11) | collective-permute-done | bytes 65568 | tf_op jit(solution)/shard_map/ppermute | solution.py:361
  82.7 0.6 add_convert_fusion
  (4 shorter events, 0.1 us)
Async XLA Ops:
  0.0 0.9 %copy-start = (bf16[64,2048]{1,0:T(8,128)(2,1)S(1)}, bf16[64,2048]{1,0:T(8,128)(2,1)}, u32[]{:S(2)}) copy-start(bf16[64,2048]{1,0:T(8,128)(2,1)} %tokens.1) | copy-start | bytes 786436
  3.2 11.2 %copy-start.1 = (bf16[2,2048,64]{1,2,0:T(8,128)(2,1)S(1)}, bf16[2,2048,64]{1,2,0:T(8,128)(2,1)}, u32[]{:S(2)}) copy-start(bf16[2,2048,64]{1,2,0:T(8,128)(2,1)} %param.13) | copy-start | bytes 1572868
  3.2 11.3 %copy-start.2 = (bf16[2,2048,64]{1,2,0:T(8,128)(2,1)S(1)}, bf16[2,2048,64]{1,2,0:T(8,128)(2,1)}, u32[]{:S(2)}) copy-start(bf16[2,2048,64]{1,2,0:T(8,128)(2,1)} %param.14) | copy-start | bytes 1572868
  3.2 39.3 %all-to-all-start = ((bf16[32,8,1024]{2,1,0:T(8,128)(2,1)}), bf16[32,8,1024]{2,1,0:T(8,128)(2,1)S(1)}, u32[]{:S(2)}, u32[]{:S(2)}) async-start(bf16[32,8,1024]{2,1,0:T(8,128)(2,1)} %bitcast.6), calls=%async_computation | async-start | bytes 1048576 | tf_op jit(solution)/shard_map/all_to_all | solution.py:264
  14.3 13.8 %collective-permute-start.1 = (bf16[2,64,2048]{2,1,0:T(8,128)(2,1)S(1)}, bf16[2,64,2048]{2,1,0:T(8,128)(2,1)S(1)}, u32[]{:S(2)}, u32[]{:S(2)}) collective-permute-start(bf16[2,64,2048]{2,1,0:T(8,128)(2,1)S(1)} %bitcast.15), channel_id=1, source_target_pairs={{0,6},{1,7},{2,4},{3,5},{4,2},{5,3},{6,0},{7,1},{8,14},{9,15},{10,... | collective-permute-start | bytes 1572872 | tf_op jit(solution)/shard_map/ppermute | solution.py:238
  14.5 25.0 %collective-permute-start.3 = (bf16[2,64,2048]{2,1,0:T(8,128)(2,1)S(1)}, bf16[2,64,2048]{2,1,0:T(8,128)(2,1)S(1)}, u32[]{:S(2)}, u32[]{:S(2)}) collective-permute-start(bf16[2,64,2048]{2,1,0:T(8,128)(2,1)S(1)} %bitcast.18), channel_id=1, source_target_pairs={{0,6},{1,7},{2,4},{3,5},{4,2},{5,3},{6,0},{7,1},{8,14},{9,15},{10,... | collective-permute-start | bytes 1572872 | tf_op jit(solution)/shard_map/ppermute | solution.py:238
  18.3 6.4 %collective-permute-start.8 = (bf16[2,2,64,512]{3,2,1,0:T(8,128)(2,1)S(1)}, bf16[2,2,64,512]{3,2,1,0:T(8,128)(2,1)S(1)}, u32[]{:S(2)}, u32[]{:S(2)}) collective-permute-start(bf16[2,2,64,512]{3,2,1,0:T(8,128)(2,1)S(1)} %get-tuple-element.18), channel_id=1, source_target_pairs={{0,2},{1,3},{2,0},{3,1},{4,6},{5,7},{6,4},{7,5},{8,10},{9,11},{10,... | collective-permute-start | bytes 786440 | tf_op jit(solution)/shard_map/ppermute | solution.py:238
  19.4 22.1 %collective-permute-start = (bf16[2,64,2048]{2,1,0:T(8,128)(2,1)S(1)}, bf16[2,64,2048]{2,1,0:T(8,128)(2,1)S(1)}, u32[]{:S(2)}, u32[]{:S(2)}) collective-permute-start(bf16[2,64,2048]{2,1,0:T(8,128)(2,1)S(1)} %theirs.1), channel_id=1, source_target_pairs={{0,1},{1,0},{2,3},{3,2},{4,5},{5,4},{6,7},{7,6},{8,9},{9,8},{10,11... | collective-permute-start | bytes 1572872 | tf_op jit(solution)/shard_map/ppermute | solution.py:238
  24.7 16.6 %collective-permute-start.9 = (bf16[2,2,64,512]{3,2,1,0:T(8,128)(2,1)S(1)}, bf16[2,2,64,512]{3,2,1,0:T(8,128)(2,1)S(1)}, u32[]{:S(2)}, u32[]{:S(2)}) collective-permute-start(bf16[2,2,64,512]{3,2,1,0:T(8,128)(2,1)S(1)} %give.1), channel_id=1, source_target_pairs={{0,1},{1,0},{2,3},{3,2},{4,5},{5,4},{6,7},{7,6},{8,9},{9,8},{10,11... | collective-permute-start | bytes 786440 | tf_op jit(solution)/shard_map/ppermute | solution.py:238
  28.2 13.3 %collective-permute-start.2 = (bf16[64,2048]{1,0:T(8,128)(2,1)S(1)}, bf16[64,2048]{1,0:T(8,128)(2,1)S(1)}, u32[]{:S(2)}, u32[]{:S(2)}) collective-permute-start(bf16[64,2048]{1,0:T(8,128)(2,1)S(1)} %shard_map.82), channel_id=1, source_target_pairs={{0,1},{1,0},{2,3},{3,2},{4,5},{5,4},{6,7},{7,6},{8,9},{9,8},{10,11... | collective-permute-start | bytes 786440 | tf_op jit(solution)/shard_map/ppermute | solution.py:238
  39.4 3.1 %collective-permute-start.4 = (bf16[64,2048]{1,0:T(8,128)(2,1)S(1)}, bf16[64,2048]{1,0:T(8,128)(2,1)S(1)}, u32[]{:S(2)}, u32[]{:S(2)}) collective-permute-start(bf16[64,2048]{1,0:T(8,128)(2,1)S(1)} %shard_map.83), channel_id=1, source_target_pairs={{0,1},{1,0},{2,3},{3,2},{4,5},{5,4},{6,7},{7,6},{8,9},{9,8},{10,11... | collective-permute-start | bytes 786440 | tf_op jit(solution)/shard_map/ppermute | solution.py:238
  41.4 9.1 %collective-permute-start.10 = (bf16[256,512]{1,0:T(8,128)(2,1)S(1)}, bf16[256,512]{1,0:T(8,128)(2,1)S(1)}, u32[]{:S(2)}, u32[]{:S(2)}) collective-permute-start(bf16[256,512]{1,0:T(8,128)(2,1)S(1)} %get-tuple-element.20), channel_id=1, source_target_pairs={{0,6},{1,7},{2,4},{3,5},{4,2},{5,3},{6,0},{7,1},{8,14},{9,15},{10,... | collective-permute-start | bytes 786440 | tf_op jit(solution)/shard_map/ppermute | solution.py:238
  41.5 0.8 copy-start.3
  44.6 5.9 %collective-permute-start.5 = (bf16[128,256]{1,0:T(8,128)(2,1)S(1)}, bf16[128,256]{1,0:T(8,128)(2,1)S(1)}, u32[]{:S(2)}, u32[]{:S(2)}) collective-permute-start(bf16[128,256]{1,0:T(8,128)(2,1)S(1)} %hidden.1.h_own), channel_id=1, source_target_pairs={{0,2},{1,3},{2,0},{3,1},{4,6},{5,7},{6,4},{7,5},{8,10},{9,11},{10,... | collective-permute-start | bytes 196616 | tf_op jit(solution)/shard_map/ppermute | solution.py:238
  44.7 8.6 %collective-permute-start.6 = (bf16[128,256]{1,0:T(8,128)(2,1)S(1)}, bf16[128,256]{1,0:T(8,128)(2,1)S(1)}, u32[]{:S(2)}, u32[]{:S(2)}) collective-permute-start(bf16[128,256]{1,0:T(8,128)(2,1)S(1)} %hidden.1.h_own), channel_id=1, source_target_pairs={{0,6},{1,7},{2,4},{3,5},{4,2},{5,3},{6,0},{7,1},{8,14},{9,15},{10,... | collective-permute-start | bytes 196616 | tf_op jit(solution)/shard_map/ppermute | solution.py:238
  47.3 6.0 %collective-permute-start.7 = (bf16[128,256]{1,0:T(8,128)(2,1)S(1)}, bf16[128,256]{1,0:T(8,128)(2,1)S(1)}, u32[]{:S(2)}, u32[]{:S(2)}) collective-permute-start(bf16[128,256]{1,0:T(8,128)(2,1)S(1)} %hidden.1.h_own), channel_id=1, source_target_pairs={{0,4},{1,5},{2,6},{3,7},{4,0},{5,1},{6,2},{7,3},{8,12},{9,13},{10,... | collective-permute-start | bytes 196616 | tf_op jit(solution)/shard_map/ppermute | solution.py:238
  78.5 4.2 %collective-permute-start.11 = (f32[64,256]{1,0:T(8,128)S(1)}, f32[64,256]{1,0:T(8,128)S(1)}, u32[]{:S(2)}, u32[]{:S(2)}) collective-permute-start(f32[64,256]{1,0:T(8,128)S(1)} %get-tuple-element.22), channel_id=1, source_target_pairs={{0,1},{1,0},{2,3},{3,2},{4,5},{5,4},{6,7},{7,6},{8,9},{9,8},{10,11... | collective-permute-start | bytes 196616 | tf_op jit(solution)/shard_map/ppermute | solution.py:361

commit v6 on v4

--- a/solution.py
+++ b/solution.py
@@ -11,6 +11,9 @@
 GROUPS = 4
 CORES = 2
 EPSILON = 1e-05
+LANES = 128
+HEADROOM = 13.0
+TINY = 1e-30
 
 VMEM = pl.BlockSpec(memory_space=pltpu.VMEM)
 PARAMS = pltpu.CompilerParams(vmem_limit_bytes=12 * 1024 * 1024)
@@ -198,12 +201,17 @@
     (h_y, h_same), (h_near, h_across) = ((p[:, :units], p[:, units:]) for p in picked)
     total = dot_nn(jnp.concatenate([h_y, h_near], axis=1), mine[...])
     total = total + dot_nn(jnp.concatenate([h_same, h_across], axis=1), same[...])
-    out[...] = total
+    largest = jnp.max(jnp.abs(total), axis=1, keepdims=True)
+    exponent = jnp.ceil(jnp.log2(jnp.maximum(largest, TINY)))
+    width = total.shape[1]
+    out[:, :width] = total * jnp.exp2(HEADROOM - exponent)
+    out[:, width:] = jnp.broadcast_to(exponent, (rows, out.shape[1] - width))
 
 
 def combine_kernel(select_hi, select_lo, returned, kept, sent):
     _, core = position()
-    values = returned[...]
+    width = CORES * kept.shape[1]
+    values = returned[:, :width] * jnp.exp2(returned[:, width : width + 1] - HEADROOM)
     high = values.astype(jnp.bfloat16)
     low = (values - high.astype(jnp.float32)).astype(jnp.bfloat16)
     total = dot_tn(select_hi[...], high) + dot_tn(select_lo[...], high)
@@ -339,15 +347,15 @@
     hiddens = [hidden] + [ppermute(hidden, pairs) for pairs in (near, same, across)]
     result = pl.pallas_call(
         functools.partial(down_kernel, slots=slots),
-        out_shape=pltpu.VMEM((rows, share), jnp.float32),
+        out_shape=pltpu.VMEM((rows, share + LANES), jnp.float32),
         in_specs=[VMEM] * (chips + 2),
         out_specs=VMEM,
         compiler_params=PARAMS,
         name="down",
     )(*on_chip(*hiddens, d_mine, d_same))
-    returned = lax.all_to_all(
-        result.reshape(ep_size, slots, share), "ep", split_axis=0, concat_axis=0, tiled=True
-    ).reshape(rows, share)
+    wire = result.astype(jnp.float16).reshape(ep_size, slots, share + LANES)
+    returned = lax.all_to_all(wire, "ep", split_axis=0, concat_axis=0, tiled=True)
+    returned = returned.astype(jnp.float32).reshape(rows, share + LANES)
     half = pltpu.VMEM((tok_rows, share // CORES), jnp.float32)
     kept, sent = pl.pallas_call(
         combine_kernel,

time: 83.3 us -> 80 us (0.960)
  blocking collectives: 24.5 us -> 21.6 us
  starting transfers between devices: 30.4 us -> 29.4 us
    all_to_all x1, blocking collectives: 24.5 us -> 21.6 us  [per_device(): lax.all_to_all(wire, 'ep', split_axis=0, concat_axis=0, tiled=True)]
    ppermute x1, starting transfers between devices: 3.29 us -> 2.27 us  [per_device(): mixed_out = kept + lax.ppermute(sent, 'tp', swap)]
  transfers between devices with their start and end apart: 13 -> 13, of which waited for: 7 -> 7; matrix products, arithmetic and copies ran while one was open for 0% -> 0% of each run, Pallas kernels for 5% -> 6%
where the time goes in v6:
time: 80 us; the launch traced here: 79 us
  starting transfers between devices  29.4 us (37%)
  blocking collectives  21.6 us (27%)
  waiting for transfers between devices  18.6 us (23%)
  Pallas kernels  7.75 us (10%)
    all_to_all x1, blocking collectives, per_device(): lax.all_to_all(wire, 'ep', split_axis=0, concat_axis=0, tiled=True)  21.6 us
    ppermute x11, waiting for transfers between devices, ppermute(): return lax.ppermute(array, 'tp', pairs)  17.7 us
    ppermute x11, starting transfers between devices, ppermute(): return lax.ppermute(array, 'tp', pairs)  15.9 us
    all_to_all x1, starting transfers between devices, per_device(): lax.all_to_all(packed.reshape(ep_size, slots, features // 2), 'ep', split...  11.2 us
    pallas_call x1, Pallas kernels, per_device(): pl.pallas_call(functools.partial(pack_kernel, slots=slots), out_shape=(pl...  2.45 us
    ppermute x1, starting transfers between devices, per_device(): mixed_out = kept + lax.ppermute(sent, 'tp', swap)  2.27 us
    pallas_call x1, Pallas kernels, per_device(): pl.pallas_call(functools.partial(hidden_kernel, slots=slots), out_shape=p...  2.15 us
  transfers between devices with their start and end apart: 13, of which 7 were waited for; matrix products, arithmetic and copies ran while one was open for 0% of the time, Pallas kernels for 6%

profile of v6, /device:TPU:25, one launch (start us, length us, event | category | flops | bytes accessed | tf_op | source)
XLA Modules:
  0.0 79.0 jit_solution(18269450263010743264)
XLA Ops:
  0.0 2.5 %pack.1 = (bf16[256,1024]{1,0:T(8,128)(2,1)}, bf16[256,64]{1,0:T(8,128)(2,1)S(1)}, bf16[256,64]{1,0:T(8,128)(2,1)S(1)}) custom-call(bf16[64,2048]{1,0:T(8,128)(2,1)} %tokens.1, f32[1,2048]{1,0:T(1,128)} %bitcast.20, f32[1,2048]{1,0:T(1,128)} %bitcast.21, s32[4,64]{1,0:T(4,128)} %bitcast.22, f32[4,64]{1,0:T(4,128)} %bitcast.23), custom_call_target="tpu_custom_call" | custom-call | tf_op jit(solution)/shard_map/pack/pallas_call | solution.py:252
  2.5 0.0 copy-start
  2.5 0.0 copy-start.1
  2.5 11.2 %all-to-all-start = ((bf16[32,8,1024]{2,1,0:T(8,128)(2,1)}), bf16[32,8,1024]{2,1,0:T(8,128)(2,1)S(1)}, u32[]{:S(2)}, u32[]{:S(2)}) async-start(bf16[32,8,1024]{2,1,0:T(8,128)(2,1)} %bitcast.6), calls=%async_computation | async-start | bytes 1048576 | tf_op jit(solution)/shard_map/all_to_all | solution.py:272
  13.6 0.0 copy-done
  13.6 0.1 collective-permute-start.1
  13.7 0.0 copy-done.1
  13.8 2.7 %collective-permute-start.3 = (bf16[2,64,2048]{2,1,0:T(8,128)(2,1)S(1)}, bf16[2,64,2048]{2,1,0:T(8,128)(2,1)S(1)}, u32[]{:S(2)}, u32[]{:S(2)}) collective-permute-start(bf16[2,64,2048]{2,1,0:T(8,128)(2,1)S(1)} %bitcast.19), channel_id=1, source_target_pairs={{0,6},{1,7},{2,4},{3,5},{4,2},{5,3},{6,0},{7,1},{8,14},{9,15},{10,... | collective-permute-start | bytes 1572872 | tf_op jit(solution)/shard_map/ppermute | solution.py:246
  16.4 1.1 %pieces.1 = (bf16[2,2,64,512]{3,2,1,0:T(8,128)(2,1)S(1)}, bf16[2,2,64,512]{3,2,1,0:T(8,128)(2,1)S(1)}) custom-call(bf16[2,64,2048]{2,1,0:T(8,128)(2,1)} %down.2), custom_call_target="tpu_custom_call" | custom-call | tf_op jit(solution)/shard_map/pieces/pallas_call | solution.py:301
  17.5 0.1 collective-permute-start.8
  17.6 1.1 %theirs.1 = bf16[2,64,2048]{2,1,0:T(8,128)(2,1)S(1)} custom-call(bf16[2,64,2048]{2,1,0:T(8,128)(2,1)} %bitcast.14, bf16[2,64,2048]{2,1,0:T(8,128)(2,1)} %bitcast.17), custom_call_target="tpu_custom_call" | custom-call | tf_op jit(solution)/shard_map/theirs/pallas_call | solution.py:276
  18.7 1.6 %collective-permute-start = (bf16[2,64,2048]{2,1,0:T(8,128)(2,1)S(1)}, bf16[2,64,2048]{2,1,0:T(8,128)(2,1)S(1)}, u32[]{:S(2)}, u32[]{:S(2)}) collective-permute-start(bf16[2,64,2048]{2,1,0:T(8,128)(2,1)S(1)} %theirs.1), channel_id=1, source_target_pairs={{0,1},{1,0},{2,3},{3,2},{4,5},{5,4},{6,7},{7,6},{8,9},{9,8},{10,11... | collective-permute-start | bytes 1572872 | tf_op jit(solution)/shard_map/ppermute | solution.py:246
  20.3 3.7 %collective-permute-done.8.near = bf16[2,2,64,512]{3,2,1,0:T(8,128)(2,1)S(1)} collective-permute-done((bf16[2,2,64,512]{3,2,1,0:T(8,128)(2,1)S(1)}, bf16[2,2,64,512]{3,2,1,0:T(8,128)(2,1)S(1)}, u32[]{:S(2)}, u32[]{:S(2)}) %collective-permute-start.8) | collective-permute-done | bytes 262176 | tf_op jit(solution)/shard_map/ppermute | solution.py:246
  24.0 2.5 %collective-permute-start.9 = (bf16[2,2,64,512]{3,2,1,0:T(8,128)(2,1)S(1)}, bf16[2,2,64,512]{3,2,1,0:T(8,128)(2,1)S(1)}, u32[]{:S(2)}, u32[]{:S(2)}) collective-permute-start(bf16[2,2,64,512]{3,2,1,0:T(8,128)(2,1)S(1)} %give.1), channel_id=1, source_target_pairs={{0,1},{1,0},{2,3},{3,2},{4,5},{5,4},{6,7},{7,6},{8,9},{9,8},{10,11... | collective-permute-start | bytes 786440 | tf_op jit(solution)/shard_map/ppermute | solution.py:246
  26.5 1.0 %collective-permute-done.1.both.gate = bf16[2,64,2048]{2,1,0:T(8,128)(2,1)S(1)} collective-permute-done((bf16[2,64,2048]{2,1,0:T(8,128)(2,1)S(1)}, bf16[2,64,2048]{2,1,0:T(8,128)(2,1)S(1)}, u32[]{:S(2)}, u32[]{:S(2)}) %collective-permute-start.1) | collective-permute-done | bytes 524320 | tf_op jit(solution)/shard_map/ppermute | solution.py:246
  27.5 3.3 %collective-permute-start.2 = (bf16[64,2048]{1,0:T(8,128)(2,1)S(1)}, bf16[64,2048]{1,0:T(8,128)(2,1)S(1)}, u32[]{:S(2)}, u32[]{:S(2)}) collective-permute-start(bf16[64,2048]{1,0:T(8,128)(2,1)S(1)} %shard_map.82), channel_id=1, source_target_pairs={{0,1},{1,0},{2,3},{3,2},{4,5},{5,4},{6,7},{7,6},{8,9},{9,8},{10,11... | collective-permute-start | bytes 786440 | tf_op jit(solution)/shard_map/ppermute | solution.py:246
  30.8 7.9 %collective-permute-done.3.both.up = bf16[2,64,2048]{2,1,0:T(8,128)(2,1)S(1)} collective-permute-done((bf16[2,64,2048]{2,1,0:T(8,128)(2,1)S(1)}, bf16[2,64,2048]{2,1,0:T(8,128)(2,1)S(1)}, u32[]{:S(2)}, u32[]{:S(2)}) %collective-permute-start.3) | collective-permute-done | bytes 524320 | tf_op jit(solution)/shard_map/ppermute | solution.py:246
  38.7 1.9 %collective-permute-start.4 = (bf16[64,2048]{1,0:T(8,128)(2,1)S(1)}, bf16[64,2048]{1,0:T(8,128)(2,1)S(1)}, u32[]{:S(2)}, u32[]{:S(2)}) collective-permute-start(bf16[64,2048]{1,0:T(8,128)(2,1)S(1)} %shard_map.83), channel_id=1, source_target_pairs={{0,1},{1,0},{2,3},{3,2},{4,5},{5,4},{6,7},{7,6},{8,9},{9,8},{10,11... | collective-permute-start | bytes 786440 | tf_op jit(solution)/shard_map/ppermute | solution.py:246
  40.6 0.0 collective-permute-done.9.other
  40.7 0.1 collective-permute-start.10
  40.8 0.0 collective-permute-done.swapped
  40.8 0.0 copy-start.2
  40.8 0.0 collective-permute-done.2.gate_swapped
  40.8 0.8 copy-done.2
  41.6 0.2 collective-permute-done.4.up_swapped
  41.8 0.0 all-to-all-done
  41.8 2.2 %hidden.1.h_own = bf16[128,256]{1,0:T(8,128)(2,1)S(1)} custom-call(bf16[2,64,2048]{2,1,0:T(8,128)(2,1)} %bitcast.15, bf16[2,64,2048]{2,1,0:T(8,128)(2,1)} %bitcast.18, bf16[2,64,2048]{2,1,0:T(8,128)(2,1)} %copy-done.2, bf16[256,1024]{1,0:T(8,128)(2,1)S(1)} %bitcast.13, bf16[2,64,2048]{2,1,0:T(8,128)(2,1)S(1)} %collective-permute-done.1.both.gate, ...), custom_call_target="tpu_custom_call" | custom-call | tf_op jit(solution)/shard_map/hidden/pallas_call | solution.py:330
  44.0 0.1 collective-permute-start.5
  44.1 2.5 %collective-permute-start.6 = (bf16[128,256]{1,0:T(8,128)(2,1)S(1)}, bf16[128,256]{1,0:T(8,128)(2,1)S(1)}, u32[]{:S(2)}, u32[]{:S(2)}) collective-permute-start(bf16[128,256]{1,0:T(8,128)(2,1)S(1)} %hidden.1.h_own), channel_id=1, source_target_pairs={{0,6},{1,7},{2,4},{3,5},{4,2},{5,3},{6,0},{7,1},{8,14},{9,15},{10,... | collective-permute-start | bytes 196616 | tf_op jit(solution)/shard_map/ppermute | solution.py:246
  46.6 1.1 %collective-permute-start.7 = (bf16[128,256]{1,0:T(8,128)(2,1)S(1)}, bf16[128,256]{1,0:T(8,128)(2,1)S(1)}, u32[]{:S(2)}, u32[]{:S(2)}) collective-permute-start(bf16[128,256]{1,0:T(8,128)(2,1)S(1)} %hidden.1.h_own), channel_id=1, source_target_pairs={{0,4},{1,5},{2,6},{3,7},{4,0},{5,1},{6,2},{7,3},{8,12},{9,13},{10,... | collective-permute-start | bytes 196616 | tf_op jit(solution)/shard_map/ppermute | solution.py:246
  47.7 2.1 %collective-permute-done.10.same = bf16[256,512]{1,0:T(8,128)(2,1)S(1)} collective-permute-done((bf16[256,512]{1,0:T(8,128)(2,1)S(1)}, bf16[256,512]{1,0:T(8,128)(2,1)S(1)}, u32[]{:S(2)}, u32[]{:S(2)}) %collective-permute-start.10) | collective-permute-done | bytes 262176 | tf_op jit(solution)/shard_map/ppermute | solution.py:246
  49.8 0.0 collective-permute-done.5.h_first
  49.8 2.8 %collective-permute-done.6.h_second = bf16[128,256]{1,0:T(8,128)(2,1)S(1)} collective-permute-done((bf16[128,256]{1,0:T(8,128)(2,1)S(1)}, bf16[128,256]{1,0:T(8,128)(2,1)S(1)}, u32[]{:S(2)}, u32[]{:S(2)}) %collective-permute-start.6) | collective-permute-done | bytes 65568 | tf_op jit(solution)/shard_map/ppermute | solution.py:246
  52.6 0.0 collective-permute-done.7.h_third
  52.6 0.5 down.3
  53.2 21.6 %all_to_all.10 = f16[32,8,640]{2,1,0:T(8,128)(2,1)S(1)} all-to-all(f16[32,8,640]{2,1,0:T(8,128)(2,1)S(1)} %convert_bitcast_fusion), channel_id=1, replica_groups=mesh['ep'=32,'tp'=8] {'ep'}, dimensions={0} | all-to-all | bytes 655360 | tf_op jit(solution)/shard_map/all_to_all | solution.py:357
  74.9 0.3 combine.1
  75.2 2.3 %collective-permute-start.11 = (f32[64,256]{1,0:T(8,128)S(1)}, f32[64,256]{1,0:T(8,128)S(1)}, u32[]{:S(2)}, u32[]{:S(2)}) collective-permute-start(f32[64,256]{1,0:T(8,128)S(1)} %get-tuple-element.22), channel_id=1, source_target_pairs={{0,1},{1,0},{2,3},{3,2},{4,5},{5,4},{6,7},{7,6},{8,9},{9,8},{10,11... | collective-permute-start | bytes 196616 | tf_op jit(solution)/shard_map/ppermute | solution.py:368
  77.5 0.9 %collective-permute-done.11 = f32[64,256]{1,0:T(8,128)S(1)} collective-permute-done((f32[64,256]{1,0:T(8,128)S(1)}, f32[64,256]{1,0:T(8,128)S(1)}, u32[]{:S(2)}, u32[]{:S(2)}) %collective-permute-start.11) | collective-permute-done | bytes 65568 | tf_op jit(solution)/shard_map/ppermute | solution.py:368
  78.4 0.6 add_convert_fusion
  (6 shorter events, 0.2 us)
Async XLA Ops:
  2.5 11.2 %copy-start = (bf16[2,2048,64]{1,2,0:T(8,128)(2,1)S(1)}, bf16[2,2048,64]{1,2,0:T(8,128)(2,1)}, u32[]{:S(2)}) copy-start(bf16[2,2048,64]{1,2,0:T(8,128)(2,1)} %param.13) | copy-start | bytes 1572868
  2.5 11.3 %copy-start.1 = (bf16[2,2048,64]{1,2,0:T(8,128)(2,1)S(1)}, bf16[2,2048,64]{1,2,0:T(8,128)(2,1)}, u32[]{:S(2)}) copy-start(bf16[2,2048,64]{1,2,0:T(8,128)(2,1)} %param.14) | copy-start | bytes 1572868
  2.5 39.3 %all-to-all-start = ((bf16[32,8,1024]{2,1,0:T(8,128)(2,1)}), bf16[32,8,1024]{2,1,0:T(8,128)(2,1)S(1)}, u32[]{:S(2)}, u32[]{:S(2)}) async-start(bf16[32,8,1024]{2,1,0:T(8,128)(2,1)} %bitcast.6), calls=%async_computation | async-start | bytes 1048576 | tf_op jit(solution)/shard_map/all_to_all | solution.py:272
  13.6 13.8 %collective-permute-start.1 = (bf16[2,64,2048]{2,1,0:T(8,128)(2,1)S(1)}, bf16[2,64,2048]{2,1,0:T(8,128)(2,1)S(1)}, u32[]{:S(2)}, u32[]{:S(2)}) collective-permute-start(bf16[2,64,2048]{2,1,0:T(8,128)(2,1)S(1)} %bitcast.16), channel_id=1, source_target_pairs={{0,6},{1,7},{2,4},{3,5},{4,2},{5,3},{6,0},{7,1},{8,14},{9,15},{10,... | collective-permute-start | bytes 1572872 | tf_op jit(solution)/shard_map/ppermute | solution.py:246
  13.8 24.9 %collective-permute-start.3 = (bf16[2,64,2048]{2,1,0:T(8,128)(2,1)S(1)}, bf16[2,64,2048]{2,1,0:T(8,128)(2,1)S(1)}, u32[]{:S(2)}, u32[]{:S(2)}) collective-permute-start(bf16[2,64,2048]{2,1,0:T(8,128)(2,1)S(1)} %bitcast.19), channel_id=1, source_target_pairs={{0,6},{1,7},{2,4},{3,5},{4,2},{5,3},{6,0},{7,1},{8,14},{9,15},{10,... | collective-permute-start | bytes 1572872 | tf_op jit(solution)/shard_map/ppermute | solution.py:246
  17.5 6.4 %collective-permute-start.8 = (bf16[2,2,64,512]{3,2,1,0:T(8,128)(2,1)S(1)}, bf16[2,2,64,512]{3,2,1,0:T(8,128)(2,1)S(1)}, u32[]{:S(2)}, u32[]{:S(2)}) collective-permute-start(bf16[2,2,64,512]{3,2,1,0:T(8,128)(2,1)S(1)} %get-tuple-element.18), channel_id=1, source_target_pairs={{0,2},{1,3},{2,0},{3,1},{4,6},{5,7},{6,4},{7,5},{8,10},{9,11},{10,... | collective-permute-start | bytes 786440 | tf_op jit(solution)/shard_map/ppermute | solution.py:246
  18.7 22.1 %collective-permute-start = (bf16[2,64,2048]{2,1,0:T(8,128)(2,1)S(1)}, bf16[2,64,2048]{2,1,0:T(8,128)(2,1)S(1)}, u32[]{:S(2)}, u32[]{:S(2)}) collective-permute-start(bf16[2,64,2048]{2,1,0:T(8,128)(2,1)S(1)} %theirs.1), channel_id=1, source_target_pairs={{0,1},{1,0},{2,3},{3,2},{4,5},{5,4},{6,7},{7,6},{8,9},{9,8},{10,11... | collective-permute-start | bytes 1572872 | tf_op jit(solution)/shard_map/ppermute | solution.py:246
  24.0 16.6 %collective-permute-start.9 = (bf16[2,2,64,512]{3,2,1,0:T(8,128)(2,1)S(1)}, bf16[2,2,64,512]{3,2,1,0:T(8,128)(2,1)S(1)}, u32[]{:S(2)}, u32[]{:S(2)}) collective-permute-start(bf16[2,2,64,512]{3,2,1,0:T(8,128)(2,1)S(1)} %give.1), channel_id=1, source_target_pairs={{0,1},{1,0},{2,3},{3,2},{4,5},{5,4},{6,7},{7,6},{8,9},{9,8},{10,11... | collective-permute-start | bytes 786440 | tf_op jit(solution)/shard_map/ppermute | solution.py:246
  27.5 13.3 %collective-permute-start.2 = (bf16[64,2048]{1,0:T(8,128)(2,1)S(1)}, bf16[64,2048]{1,0:T(8,128)(2,1)S(1)}, u32[]{:S(2)}, u32[]{:S(2)}) collective-permute-start(bf16[64,2048]{1,0:T(8,128)(2,1)S(1)} %shard_map.82), channel_id=1, source_target_pairs={{0,1},{1,0},{2,3},{3,2},{4,5},{5,4},{6,7},{7,6},{8,9},{9,8},{10,11... | collective-permute-start | bytes 786440 | tf_op jit(solution)/shard_map/ppermute | solution.py:246
  38.7 3.1 %collective-permute-start.4 = (bf16[64,2048]{1,0:T(8,128)(2,1)S(1)}, bf16[64,2048]{1,0:T(8,128)(2,1)S(1)}, u32[]{:S(2)}, u32[]{:S(2)}) collective-permute-start(bf16[64,2048]{1,0:T(8,128)(2,1)S(1)} %shard_map.83), channel_id=1, source_target_pairs={{0,1},{1,0},{2,3},{3,2},{4,5},{5,4},{6,7},{7,6},{8,9},{9,8},{10,11... | collective-permute-start | bytes 786440 | tf_op jit(solution)/shard_map/ppermute | solution.py:246
  40.7 9.1 %collective-permute-start.10 = (bf16[256,512]{1,0:T(8,128)(2,1)S(1)}, bf16[256,512]{1,0:T(8,128)(2,1)S(1)}, u32[]{:S(2)}, u32[]{:S(2)}) collective-permute-start(bf16[256,512]{1,0:T(8,128)(2,1)S(1)} %get-tuple-element.20), channel_id=1, source_target_pairs={{0,6},{1,7},{2,4},{3,5},{4,2},{5,3},{6,0},{7,1},{8,14},{9,15},{10,... | collective-permute-start | bytes 786440 | tf_op jit(solution)/shard_map/ppermute | solution.py:246
  40.8 0.8 %copy-start.2 = (bf16[2,64,2048]{2,1,0:T(8,128)(2,1)}, bf16[2,64,2048]{2,1,0:T(8,128)(2,1)S(1)}, u32[]{:S(2)}) copy-start(bf16[2,64,2048]{2,1,0:T(8,128)(2,1)S(1)} %collective-permute-done.swapped) | copy-start | bytes 1572868
  44.0 5.9 %collective-permute-start.5 = (bf16[128,256]{1,0:T(8,128)(2,1)S(1)}, bf16[128,256]{1,0:T(8,128)(2,1)S(1)}, u32[]{:S(2)}, u32[]{:S(2)}) collective-permute-start(bf16[128,256]{1,0:T(8,128)(2,1)S(1)} %hidden.1.h_own), channel_id=1, source_target_pairs={{0,2},{1,3},{2,0},{3,1},{4,6},{5,7},{6,4},{7,5},{8,10},{9,11},{10,... | collective-permute-start | bytes 196616 | tf_op jit(solution)/shard_map/ppermute | solution.py:246
  44.1 8.6 %collective-permute-start.6 = (bf16[128,256]{1,0:T(8,128)(2,1)S(1)}, bf16[128,256]{1,0:T(8,128)(2,1)S(1)}, u32[]{:S(2)}, u32[]{:S(2)}) collective-permute-start(bf16[128,256]{1,0:T(8,128)(2,1)S(1)} %hidden.1.h_own), channel_id=1, source_target_pairs={{0,6},{1,7},{2,4},{3,5},{4,2},{5,3},{6,0},{7,1},{8,14},{9,15},{10,... | collective-permute-start | bytes 196616 | tf_op jit(solution)/shard_map/ppermute | solution.py:246
  46.6 6.0 %collective-permute-start.7 = (bf16[128,256]{1,0:T(8,128)(2,1)S(1)}, bf16[128,256]{1,0:T(8,128)(2,1)S(1)}, u32[]{:S(2)}, u32[]{:S(2)}) collective-permute-start(bf16[128,256]{1,0:T(8,128)(2,1)S(1)} %hidden.1.h_own), channel_id=1, source_target_pairs={{0,4},{1,5},{2,6},{3,7},{4,0},{5,1},{6,2},{7,3},{8,12},{9,13},{10,... | collective-permute-start | bytes 196616 | tf_op jit(solution)/shard_map/ppermute | solution.py:246
  75.2 3.2 %collective-permute-start.11 = (f32[64,256]{1,0:T(8,128)S(1)}, f32[64,256]{1,0:T(8,128)S(1)}, u32[]{:S(2)}, u32[]{:S(2)}) collective-permute-start(f32[64,256]{1,0:T(8,128)S(1)} %get-tuple-element.22), channel_id=1, source_target_pairs={{0,1},{1,0},{2,3},{3,2},{4,5},{5,4},{6,7},{7,6},{8,9},{9,8},{10,11... | collective-permute-start | bytes 196616 | tf_op jit(solution)/shard_map/ppermute | solution.py:368

commit v7 on v6

--- a/solution.py
+++ b/solution.py
@@ -44,11 +44,6 @@
     return lax.dot_general(a, b, (((0,), (0,)), ((), ())), preferred_element_type=jnp.float32)
 
 
-def part(y):
-    high = lax.shift_right_logical(y, 1)
-    return high, lax.bitwise_and(lax.bitwise_xor(y, high), 1)
-
-
 def iota(shape, dimension):
     return lax.broadcasted_iota(jnp.int32, shape, dimension)
 
@@ -73,7 +68,7 @@
 
 def pack_kernel(tokens, gain, shift, ids, weights, packed, select_hi, select_lo, *, slots):
     y, core = position()
-    row_half, _ = part(y)
+    row_half = lax.bitwise_and(y, 1)
     top_count, rows = ids.shape
     total = packed.shape[0]
     experts = total // slots
@@ -183,8 +178,8 @@
 
 
 def down_kernel(h_own, h_first, h_second, h_third, mine, same, out, *, slots):
-    y, _ = position()
-    row_half, _ = part(y)
+    y, core = position()
+    row_half = lax.bitwise_and(y, 1)
     rows = out.shape[0]
     kept = h_own.shape[0]
     count = slots // 2
@@ -194,13 +189,21 @@
     half = jnp.where(j < kept, row_half, 1 - row_half)
     place = (i // count) * slots + half * count + i % count
     spread = jnp.where(r == place, 1.0, 0.0).astype(jnp.bfloat16)
-    picked = []
-    for a, b in ((h_own, h_second), (h_first, h_third)):
-        across = jnp.concatenate([b[:, units:], b[:, :units]], axis=1)
-        picked.append(dot_nn(spread, jnp.concatenate([a[...], across])).astype(jnp.bfloat16))
-    (h_y, h_same), (h_near, h_across) = ((p[:, :units], p[:, units:]) for p in picked)
-    total = dot_nn(jnp.concatenate([h_y, h_near], axis=1), mine[...])
-    total = total + dot_nn(jnp.concatenate([h_same, h_across], axis=1), same[...])
+    turn = lax.bitwise_xor(core, row_half) == 1
+    lower = iota((kept, units), 1) < units // 2
+
+    def passed(a, b):
+        a, b = a[:, units:], b[:, units:]
+        forward, backward = jnp.where(lower, a, b), jnp.where(lower, b, a)
+        return jnp.where(turn, forward, backward), jnp.where(turn, backward, forward)
+
+    for_own, for_third = passed(h_first[...], h_second[...])
+    for_first, for_second = passed(h_third[...], h_own[...])
+    tops = (h_own[:, :units], for_first, for_second, h_third[:, :units])
+    bottoms = (for_own, h_first[:, :units], h_second[:, :units], for_third)
+    pieces = jnp.concatenate([jnp.concatenate(tops, axis=1), jnp.concatenate(bottoms, axis=1)])
+    h = dot_nn(spread, pieces).astype(jnp.bfloat16)
+    total = dot_nn(h[:, : 2 * units], mine[...]) + dot_nn(h[:, 2 * units :], same[...])
     largest = jnp.max(jnp.abs(total), axis=1, keepdims=True)
     exponent = jnp.ceil(jnp.log2(jnp.maximum(largest, TINY)))
     width = total.shape[1]
@@ -240,14 +243,15 @@
     near = [(i, i ^ 2) for i in range(tp_size)]
     same = [(i, 6 - i // 2 * 2 + i % 2) for i in range(tp_size)]
     across = [(i, i ^ 4) for i in range(tp_size)]
+    turns = [(i, (i + (2 if i % 2 else -2)) % tp_size) for i in range(tp_size)]
     anywhere = pl.BlockSpec(memory_space=pl.ANY)
 
     def ppermute(array, pairs):
         return lax.ppermute(array, "tp", pairs)
 
     gate_t, up_t = off_chip(expert_gate.transpose(0, 2, 1), expert_up.transpose(0, 2, 1))
-    gate_both = ppermute(expert_gate.transpose(0, 2, 1), same)
-    up_both = ppermute(expert_up.transpose(0, 2, 1), same)
+    gate_both = ppermute(expert_gate.transpose(0, 2, 1), turns)
+    up_both = ppermute(expert_up.transpose(0, 2, 1), turns)
 
     packed, select_hi, select_lo = pl.pallas_call(
         functools.partial(pack_kernel, slots=slots),

time: 80 us -> 75.9 us (0.949)
  the two profiles are of different devices: /device:TPU:25 before, /device:TPU:1 now
where the time goes in v7:
time: 75.9 us; the launch traced here: 75.6 us
  starting transfers between devices  31.2 us (41%)
  blocking collectives  20 us (26%)
  waiting for transfers between devices  15 us (20%)
  Pallas kernels  7.74 us (10%)
  local copies, waits for them, and re-layouts  0.8 us (1%)
    all_to_all x1, blocking collectives, per_device(): lax.all_to_all(wire, 'ep', split_axis=0, concat_axis=0, tiled=True)  20 us
    ppermute x11, starting transfers between devices, ppermute(): return lax.ppermute(array, 'tp', pairs)  14.4 us
    ppermute x11, waiting for transfers between devices, ppermute(): return lax.ppermute(array, 'tp', pairs)  14.1 us
    all_to_all x1, starting transfers between devices, per_device(): lax.all_to_all(packed.reshape(ep_size, slots, features // 2), 'ep', split...  12 us
    ppermute x1, starting transfers between devices, per_device(): mixed_out = kept + lax.ppermute(sent, 'tp', swap)  4.83 us
    pallas_call x1, Pallas kernels, per_device(): pl.pallas_call(functools.partial(pack_kernel, slots=slots), out_shape=(pl...  2.45 us
    pallas_call x1, Pallas kernels, per_device(): pl.pallas_call(functools.partial(hidden_kernel, slots=slots), out_shape=p...  2.15 us
  transfers between devices with their start and end apart: 13, of which 6 were waited for; matrix products, arithmetic and copies ran while one was open for 0% of the time, Pallas kernels for 6%

profile of v7, /device:TPU:1, one launch (start us, length us, event | category | flops | bytes accessed | tf_op | source)
XLA Modules:
  0.0 75.6 jit_solution(15187625229733072184)
XLA Ops:
  0.0 2.5 %pack.1 = (bf16[256,1024]{1,0:T(8,128)(2,1)}, bf16[256,64]{1,0:T(8,128)(2,1)S(1)}, bf16[256,64]{1,0:T(8,128)(2,1)S(1)}) custom-call(bf16[64,2048]{1,0:T(8,128)(2,1)} %tokens.1, f32[1,2048]{1,0:T(1,128)} %bitcast.20, f32[1,2048]{1,0:T(1,128)} %bitcast.21, s32[4,64]{1,0:T(4,128)} %bitcast.22, f32[4,64]{1,0:T(4,128)} %bitcast.23), custom_call_target="tpu_custom_call" | custom-call | tf_op jit(solution)/shard_map/pack/pallas_call | solution.py:256
  2.5 0.0 copy-start
  2.5 0.0 copy-start.1
  2.5 12.0 %all-to-all-start = ((bf16[32,8,1024]{2,1,0:T(8,128)(2,1)}), bf16[32,8,1024]{2,1,0:T(8,128)(2,1)S(1)}, u32[]{:S(2)}, u32[]{:S(2)}) async-start(bf16[32,8,1024]{2,1,0:T(8,128)(2,1)} %bitcast.6), calls=%async_computation | async-start | bytes 1048576 | tf_op jit(solution)/shard_map/all_to_all | solution.py:276
  14.5 0.0 copy-done
  14.5 1.4 %collective-permute-start.1 = (bf16[2,64,2048]{2,1,0:T(8,128)(2,1)S(1)}, bf16[2,64,2048]{2,1,0:T(8,128)(2,1)S(1)}, u32[]{:S(2)}, u32[]{:S(2)}) collective-permute-start(bf16[2,64,2048]{2,1,0:T(8,128)(2,1)S(1)} %bitcast.16), channel_id=1, source_target_pairs={{0,6},{1,3},{2,0},{3,5},{4,2},{5,7},{6,4},{7,1},{8,14},{9,11},{10,... | collective-permute-start | bytes 1572872 | tf_op jit(solution)/shard_map/ppermute | solution.py:250
  15.8 0.0 copy-done.1
  15.8 1.3 %collective-permute-start.3 = (bf16[2,64,2048]{2,1,0:T(8,128)(2,1)S(1)}, bf16[2,64,2048]{2,1,0:T(8,128)(2,1)S(1)}, u32[]{:S(2)}, u32[]{:S(2)}) collective-permute-start(bf16[2,64,2048]{2,1,0:T(8,128)(2,1)S(1)} %bitcast.19), channel_id=1, source_target_pairs={{0,6},{1,3},{2,0},{3,5},{4,2},{5,7},{6,4},{7,1},{8,14},{9,11},{10,... | collective-permute-start | bytes 1572872 | tf_op jit(solution)/shard_map/ppermute | solution.py:250
  17.1 1.1 %pieces.1 = (bf16[2,2,64,512]{3,2,1,0:T(8,128)(2,1)S(1)}, bf16[2,2,64,512]{3,2,1,0:T(8,128)(2,1)S(1)}) custom-call(bf16[2,64,2048]{2,1,0:T(8,128)(2,1)} %down.2), custom_call_target="tpu_custom_call" | custom-call | tf_op jit(solution)/shard_map/pieces/pallas_call | solution.py:305
  18.3 1.1 %collective-permute-start.8 = (bf16[2,2,64,512]{3,2,1,0:T(8,128)(2,1)S(1)}, bf16[2,2,64,512]{3,2,1,0:T(8,128)(2,1)S(1)}, u32[]{:S(2)}, u32[]{:S(2)}) collective-permute-start(bf16[2,2,64,512]{3,2,1,0:T(8,128)(2,1)S(1)} %get-tuple-element.18), channel_id=1, source_target_pairs={{0,2},{1,3},{2,0},{3,1},{4,6},{5,7},{6,4},{7,5},{8,10},{9,11},{10,... | collective-permute-start | bytes 786440 | tf_op jit(solution)/shard_map/ppermute | solution.py:250
  19.4 1.0 %theirs.1 = bf16[2,64,2048]{2,1,0:T(8,128)(2,1)S(1)} custom-call(bf16[2,64,2048]{2,1,0:T(8,128)(2,1)} %bitcast.14, bf16[2,64,2048]{2,1,0:T(8,128)(2,1)} %bitcast.17), custom_call_target="tpu_custom_call" | custom-call | tf_op jit(solution)/shard_map/theirs/pallas_call | solution.py:280
  20.4 2.5 %collective-permute-start = (bf16[2,64,2048]{2,1,0:T(8,128)(2,1)S(1)}, bf16[2,64,2048]{2,1,0:T(8,128)(2,1)S(1)}, u32[]{:S(2)}, u32[]{:S(2)}) collective-permute-start(bf16[2,64,2048]{2,1,0:T(8,128)(2,1)S(1)} %theirs.1), channel_id=1, source_target_pairs={{0,1},{1,0},{2,3},{3,2},{4,5},{5,4},{6,7},{7,6},{8,9},{9,8},{10,11... | collective-permute-start | bytes 1572872 | tf_op jit(solution)/shard_map/ppermute | solution.py:250
  22.9 10.3 %collective-permute-done.8.near = bf16[2,2,64,512]{3,2,1,0:T(8,128)(2,1)S(1)} collective-permute-done((bf16[2,2,64,512]{3,2,1,0:T(8,128)(2,1)S(1)}, bf16[2,2,64,512]{3,2,1,0:T(8,128)(2,1)S(1)}, u32[]{:S(2)}, u32[]{:S(2)}) %collective-permute-start.8) | collective-permute-done | bytes 262176 | tf_op jit(solution)/shard_map/ppermute | solution.py:250
  33.2 2.8 %collective-permute-start.9 = (bf16[2,2,64,512]{3,2,1,0:T(8,128)(2,1)S(1)}, bf16[2,2,64,512]{3,2,1,0:T(8,128)(2,1)S(1)}, u32[]{:S(2)}, u32[]{:S(2)}) collective-permute-start(bf16[2,2,64,512]{3,2,1,0:T(8,128)(2,1)S(1)} %give.1), channel_id=1, source_target_pairs={{0,1},{1,0},{2,3},{3,2},{4,5},{5,4},{6,7},{7,6},{8,9},{9,8},{10,11... | collective-permute-start | bytes 786440 | tf_op jit(solution)/shard_map/ppermute | solution.py:250
  36.0 0.0 collective-permute-done.1.both.gate
  36.0 0.1 collective-permute-start.2
  36.2 0.0 collective-permute-done.3.both.up
  36.2 0.6 collective-permute-start.4
  36.8 0.4 collective-permute-done.9.other
  37.2 1.1 %collective-permute-start.10 = (bf16[256,512]{1,0:T(8,128)(2,1)S(1)}, bf16[256,512]{1,0:T(8,128)(2,1)S(1)}, u32[]{:S(2)}, u32[]{:S(2)}) collective-permute-start(bf16[256,512]{1,0:T(8,128)(2,1)S(1)} %get-tuple-element.20), channel_id=1, source_target_pairs={{0,6},{1,7},{2,4},{3,5},{4,2},{5,3},{6,0},{7,1},{8,14},{9,15},{10,... | collective-permute-start | bytes 786440 | tf_op jit(solution)/shard_map/ppermute | solution.py:250
  38.3 0.0 collective-permute-done.swapped
  38.3 0.0 copy-start.2
  38.3 0.0 collective-permute-done.2.gate_swapped
  38.3 0.8 %copy-done.2 = bf16[2,64,2048]{2,1,0:T(8,128)(2,1)} copy-done((bf16[2,64,2048]{2,1,0:T(8,128)(2,1)}, bf16[2,64,2048]{2,1,0:T(8,128)(2,1)S(1)}, u32[]{:S(2)}) %copy-start.2) | copy-done | bytes 524312
  39.1 0.0 collective-permute-done.4.up_swapped
  39.1 0.0 all-to-all-done
  39.1 2.1 %hidden.1.h_own = bf16[128,256]{1,0:T(8,128)(2,1)S(1)} custom-call(bf16[2,64,2048]{2,1,0:T(8,128)(2,1)} %bitcast.15, bf16[2,64,2048]{2,1,0:T(8,128)(2,1)} %bitcast.18, bf16[2,64,2048]{2,1,0:T(8,128)(2,1)} %copy-done.2, bf16[256,1024]{1,0:T(8,128)(2,1)S(1)} %bitcast.13, bf16[2,64,2048]{2,1,0:T(8,128)(2,1)S(1)} %collective-permute-done.1.both.gate, ...), custom_call_target="tpu_custom_call" | custom-call | tf_op jit(solution)/shard_map/hidden/pallas_call | solution.py:334
  41.3 1.7 %collective-permute-start.5 = (bf16[128,256]{1,0:T(8,128)(2,1)S(1)}, bf16[128,256]{1,0:T(8,128)(2,1)S(1)}, u32[]{:S(2)}, u32[]{:S(2)}) collective-permute-start(bf16[128,256]{1,0:T(8,128)(2,1)S(1)} %hidden.1.h_own), channel_id=1, source_target_pairs={{0,2},{1,3},{2,0},{3,1},{4,6},{5,7},{6,4},{7,5},{8,10},{9,11},{10,... | collective-permute-start | bytes 196616 | tf_op jit(solution)/shard_map/ppermute | solution.py:250
  42.9 0.6 collective-permute-start.6
  43.6 1.3 %collective-permute-start.7 = (bf16[128,256]{1,0:T(8,128)(2,1)S(1)}, bf16[128,256]{1,0:T(8,128)(2,1)S(1)}, u32[]{:S(2)}, u32[]{:S(2)}) collective-permute-start(bf16[128,256]{1,0:T(8,128)(2,1)S(1)} %hidden.1.h_own), channel_id=1, source_target_pairs={{0,4},{1,5},{2,6},{3,7},{4,0},{5,1},{6,2},{7,3},{8,12},{9,13},{10,... | collective-permute-start | bytes 196616 | tf_op jit(solution)/shard_map/ppermute | solution.py:250
  44.8 1.2 %collective-permute-done.10.same = bf16[256,512]{1,0:T(8,128)(2,1)S(1)} collective-permute-done((bf16[256,512]{1,0:T(8,128)(2,1)S(1)}, bf16[256,512]{1,0:T(8,128)(2,1)S(1)}, u32[]{:S(2)}, u32[]{:S(2)}) %collective-permute-start.10) | collective-permute-done | bytes 262176 | tf_op jit(solution)/shard_map/ppermute | solution.py:250
  46.0 0.0 collective-permute-done.5.h_first
  46.0 1.3 %collective-permute-done.6.h_second = bf16[128,256]{1,0:T(8,128)(2,1)S(1)} collective-permute-done((bf16[128,256]{1,0:T(8,128)(2,1)S(1)}, bf16[128,256]{1,0:T(8,128)(2,1)S(1)}, u32[]{:S(2)}, u32[]{:S(2)}) %collective-permute-start.6) | collective-permute-done | bytes 65568 | tf_op jit(solution)/shard_map/ppermute | solution.py:250
  47.3 0.9 %collective-permute-done.7.h_third = bf16[128,256]{1,0:T(8,128)(2,1)S(1)} collective-permute-done((bf16[128,256]{1,0:T(8,128)(2,1)S(1)}, bf16[128,256]{1,0:T(8,128)(2,1)S(1)}, u32[]{:S(2)}, u32[]{:S(2)}) %collective-permute-start.7) | collective-permute-done | bytes 65568 | tf_op jit(solution)/shard_map/ppermute | solution.py:250
  48.2 0.5 down.3
  48.8 20.0 %all_to_all.10 = f16[32,8,640]{2,1,0:T(8,128)(2,1)S(1)} all-to-all(f16[32,8,640]{2,1,0:T(8,128)(2,1)S(1)} %convert_bitcast_fusion), channel_id=1, replica_groups=mesh['ep'=32,'tp'=8] {'ep'}, dimensions={0} | all-to-all | bytes 655360 | tf_op jit(solution)/shard_map/all_to_all | solution.py:361
  68.9 0.3 combine.1
  69.2 4.8 %collective-permute-start.11 = (f32[64,256]{1,0:T(8,128)S(1)}, f32[64,256]{1,0:T(8,128)S(1)}, u32[]{:S(2)}, u32[]{:S(2)}) collective-permute-start(f32[64,256]{1,0:T(8,128)S(1)} %get-tuple-element.22), channel_id=1, source_target_pairs={{0,1},{1,0},{2,3},{3,2},{4,5},{5,4},{6,7},{7,6},{8,9},{9,8},{10,11... | collective-permute-start | bytes 196616 | tf_op jit(solution)/shard_map/ppermute | solution.py:372
  74.0 0.9 %collective-permute-done.11 = f32[64,256]{1,0:T(8,128)S(1)} collective-permute-done((f32[64,256]{1,0:T(8,128)S(1)}, f32[64,256]{1,0:T(8,128)S(1)}, u32[]{:S(2)}, u32[]{:S(2)}) %collective-permute-start.11) | collective-permute-done | bytes 65568 | tf_op jit(solution)/shard_map/ppermute | solution.py:372
  74.9 0.6 add_convert_fusion
  (6 shorter events, 0.2 us)
Async XLA Ops:
  2.5 12.0 %copy-start = (bf16[2,2048,64]{1,2,0:T(8,128)(2,1)S(1)}, bf16[2,2048,64]{1,2,0:T(8,128)(2,1)}, u32[]{:S(2)}) copy-start(bf16[2,2048,64]{1,2,0:T(8,128)(2,1)} %param.13) | copy-start | bytes 1572868
  2.5 13.4 %copy-start.1 = (bf16[2,2048,64]{1,2,0:T(8,128)(2,1)S(1)}, bf16[2,2048,64]{1,2,0:T(8,128)(2,1)}, u32[]{:S(2)}) copy-start(bf16[2,2048,64]{1,2,0:T(8,128)(2,1)} %param.14) | copy-start | bytes 1572868
  2.5 36.7 %all-to-all-start = ((bf16[32,8,1024]{2,1,0:T(8,128)(2,1)}), bf16[32,8,1024]{2,1,0:T(8,128)(2,1)S(1)}, u32[]{:S(2)}, u32[]{:S(2)}) async-start(bf16[32,8,1024]{2,1,0:T(8,128)(2,1)} %bitcast.6), calls=%async_computation | async-start | bytes 1048576 | tf_op jit(solution)/shard_map/all_to_all | solution.py:276
  14.5 21.6 %collective-permute-start.1 = (bf16[2,64,2048]{2,1,0:T(8,128)(2,1)S(1)}, bf16[2,64,2048]{2,1,0:T(8,128)(2,1)S(1)}, u32[]{:S(2)}, u32[]{:S(2)}) collective-permute-start(bf16[2,64,2048]{2,1,0:T(8,128)(2,1)S(1)} %bitcast.16), channel_id=1, source_target_pairs={{0,6},{1,3},{2,0},{3,5},{4,2},{5,7},{6,4},{7,1},{8,14},{9,11},{10,... | collective-permute-start | bytes 1572872 | tf_op jit(solution)/shard_map/ppermute | solution.py:250
  15.8 20.3 %collective-permute-start.3 = (bf16[2,64,2048]{2,1,0:T(8,128)(2,1)S(1)}, bf16[2,64,2048]{2,1,0:T(8,128)(2,1)S(1)}, u32[]{:S(2)}, u32[]{:S(2)}) collective-permute-start(bf16[2,64,2048]{2,1,0:T(8,128)(2,1)S(1)} %bitcast.19), channel_id=1, source_target_pairs={{0,6},{1,3},{2,0},{3,5},{4,2},{5,7},{6,4},{7,1},{8,14},{9,11},{10,... | collective-permute-start | bytes 1572872 | tf_op jit(solution)/shard_map/ppermute | solution.py:250
  18.3 14.9 %collective-permute-start.8 = (bf16[2,2,64,512]{3,2,1,0:T(8,128)(2,1)S(1)}, bf16[2,2,64,512]{3,2,1,0:T(8,128)(2,1)S(1)}, u32[]{:S(2)}, u32[]{:S(2)}) collective-permute-start(bf16[2,2,64,512]{3,2,1,0:T(8,128)(2,1)S(1)} %get-tuple-element.18), channel_id=1, source_target_pairs={{0,2},{1,3},{2,0},{3,1},{4,6},{5,7},{6,4},{7,5},{8,10},{9,11},{10,... | collective-permute-start | bytes 786440 | tf_op jit(solution)/shard_map/ppermute | solution.py:250
  20.4 17.9 %collective-permute-start = (bf16[2,64,2048]{2,1,0:T(8,128)(2,1)S(1)}, bf16[2,64,2048]{2,1,0:T(8,128)(2,1)S(1)}, u32[]{:S(2)}, u32[]{:S(2)}) collective-permute-start(bf16[2,64,2048]{2,1,0:T(8,128)(2,1)S(1)} %theirs.1), channel_id=1, source_target_pairs={{0,1},{1,0},{2,3},{3,2},{4,5},{5,4},{6,7},{7,6},{8,9},{9,8},{10,11... | collective-permute-start | bytes 1572872 | tf_op jit(solution)/shard_map/ppermute | solution.py:250
  33.2 4.0 %collective-permute-start.9 = (bf16[2,2,64,512]{3,2,1,0:T(8,128)(2,1)S(1)}, bf16[2,2,64,512]{3,2,1,0:T(8,128)(2,1)S(1)}, u32[]{:S(2)}, u32[]{:S(2)}) collective-permute-start(bf16[2,2,64,512]{3,2,1,0:T(8,128)(2,1)S(1)} %give.1), channel_id=1, source_target_pairs={{0,1},{1,0},{2,3},{3,2},{4,5},{5,4},{6,7},{7,6},{8,9},{9,8},{10,11... | collective-permute-start | bytes 786440 | tf_op jit(solution)/shard_map/ppermute | solution.py:250
  36.0 2.3 %collective-permute-start.2 = (bf16[64,2048]{1,0:T(8,128)(2,1)S(1)}, bf16[64,2048]{1,0:T(8,128)(2,1)S(1)}, u32[]{:S(2)}, u32[]{:S(2)}) collective-permute-start(bf16[64,2048]{1,0:T(8,128)(2,1)S(1)} %shard_map.82), channel_id=1, source_target_pairs={{0,1},{1,0},{2,3},{3,2},{4,5},{5,4},{6,7},{7,6},{8,9},{9,8},{10,11... | collective-permute-start | bytes 786440 | tf_op jit(solution)/shard_map/ppermute | solution.py:250
  36.2 2.9 %collective-permute-start.4 = (bf16[64,2048]{1,0:T(8,128)(2,1)S(1)}, bf16[64,2048]{1,0:T(8,128)(2,1)S(1)}, u32[]{:S(2)}, u32[]{:S(2)}) collective-permute-start(bf16[64,2048]{1,0:T(8,128)(2,1)S(1)} %shard_map.83), channel_id=1, source_target_pairs={{0,1},{1,0},{2,3},{3,2},{4,5},{5,4},{6,7},{7,6},{8,9},{9,8},{10,11... | collective-permute-start | bytes 786440 | tf_op jit(solution)/shard_map/ppermute | solution.py:250
  37.2 8.8 %collective-permute-start.10 = (bf16[256,512]{1,0:T(8,128)(2,1)S(1)}, bf16[256,512]{1,0:T(8,128)(2,1)S(1)}, u32[]{:S(2)}, u32[]{:S(2)}) collective-permute-start(bf16[256,512]{1,0:T(8,128)(2,1)S(1)} %get-tuple-element.20), channel_id=1, source_target_pairs={{0,6},{1,7},{2,4},{3,5},{4,2},{5,3},{6,0},{7,1},{8,14},{9,15},{10,... | collective-permute-start | bytes 786440 | tf_op jit(solution)/shard_map/ppermute | solution.py:250
  38.3 0.8 %copy-start.2 = (bf16[2,64,2048]{2,1,0:T(8,128)(2,1)}, bf16[2,64,2048]{2,1,0:T(8,128)(2,1)S(1)}, u32[]{:S(2)}) copy-start(bf16[2,64,2048]{2,1,0:T(8,128)(2,1)S(1)} %collective-permute-done.swapped) | copy-start | bytes 1572868
  41.3 4.7 %collective-permute-start.5 = (bf16[128,256]{1,0:T(8,128)(2,1)S(1)}, bf16[128,256]{1,0:T(8,128)(2,1)S(1)}, u32[]{:S(2)}, u32[]{:S(2)}) collective-permute-start(bf16[128,256]{1,0:T(8,128)(2,1)S(1)} %hidden.1.h_own), channel_id=1, source_target_pairs={{0,2},{1,3},{2,0},{3,1},{4,6},{5,7},{6,4},{7,5},{8,10},{9,11},{10,... | collective-permute-start | bytes 196616 | tf_op jit(solution)/shard_map/ppermute | solution.py:250
  42.9 4.3 %collective-permute-start.6 = (bf16[128,256]{1,0:T(8,128)(2,1)S(1)}, bf16[128,256]{1,0:T(8,128)(2,1)S(1)}, u32[]{:S(2)}, u32[]{:S(2)}) collective-permute-start(bf16[128,256]{1,0:T(8,128)(2,1)S(1)} %hidden.1.h_own), channel_id=1, source_target_pairs={{0,6},{1,7},{2,4},{3,5},{4,2},{5,3},{6,0},{7,1},{8,14},{9,15},{10,... | collective-permute-start | bytes 196616 | tf_op jit(solution)/shard_map/ppermute | solution.py:250
  43.6 4.6 %collective-permute-start.7 = (bf16[128,256]{1,0:T(8,128)(2,1)S(1)}, bf16[128,256]{1,0:T(8,128)(2,1)S(1)}, u32[]{:S(2)}, u32[]{:S(2)}) collective-permute-start(bf16[128,256]{1,0:T(8,128)(2,1)S(1)} %hidden.1.h_own), channel_id=1, source_target_pairs={{0,4},{1,5},{2,6},{3,7},{4,0},{5,1},{6,2},{7,3},{8,12},{9,13},{10,... | collective-permute-start | bytes 196616 | tf_op jit(solution)/shard_map/ppermute | solution.py:250
  69.2 5.7 %collective-permute-start.11 = (f32[64,256]{1,0:T(8,128)S(1)}, f32[64,256]{1,0:T(8,128)S(1)}, u32[]{:S(2)}, u32[]{:S(2)}) collective-permute-start(f32[64,256]{1,0:T(8,128)S(1)} %get-tuple-element.22), channel_id=1, source_target_pairs={{0,1},{1,0},{2,3},{3,2},{4,5},{5,4},{6,7},{7,6},{8,9},{9,8},{10,11... | collective-permute-start | bytes 196616 | tf_op jit(solution)/shard_map/ppermute | solution.py:372
